TPU v7x, 32 devices: a whole 2x2x4 slice. The times are simulated.
32 devices in a mesh: sp: 8 (over z, y), tp: 4 (over x, core).
Axes of the slice: x: 2, y: 2, z: 4, core: 2. Of those that a mesh axis runs over, the one named last changes fastest.
Arguments:
- stream_in: bfloat16 [6144, 2048], P(('sp', 'tp')), may hold values from -6 to 6
- query_wide: bfloat16 [6144, 512], P('sp', 'tp'), may hold values from -6 to 6
- key_wide: bfloat16 [6144, 512], P('sp', 'tp'), may hold values from -6 to 6
- value_wide: bfloat16 [6144, 512], P('sp', 'tp'), may hold values from -6 to 6
- gate_wide: bfloat16 [6144, 512], P('sp', 'tp'), may hold values from -6 to 6
- decay_wide: float32 [4, 6144], P('tp', 'sp'), may hold values from -2.3 to 0, as said below
- query_narrow: bfloat16 [6144, 512], P('sp', 'tp'), may hold values from -6 to 6
- key_narrow: bfloat16 [6144, 512], P('sp', 'tp'), may hold values from -6 to 6
- value_narrow: bfloat16 [6144, 512], P('sp', 'tp'), may hold values from -6 to 6
- gate_narrow: bfloat16 [6144, 512], P('sp', 'tp'), may hold values from -6 to 6
- decay_narrow: float32 [8, 6144], P('tp', 'sp'), may hold values from -2.3 to 0, as said below
- output_wide: bfloat16 [512, 2048], P('tp'), may hold values from -0.25 to 0.25
- output_narrow: bfloat16 [512, 2048], P('tp'), may hold values from -0.25 to 0.25
- norm_gain: bfloat16 [2048], replicated, may hold values from 0.099609375 to 1.8984375
- up_weight: bfloat16 [2048, 8192], P('sp', 'tp'), may hold values from -0.125 to 0.125
- down_weight: bfloat16 [8192, 2048], P('tp', 'sp'), may hold values from -0.0625 to 0.0625
Outputs:
- layer_out: bfloat16 [6144, 2048], P(('sp', 'tp'))
Inputs may be any that keep to these rules, and one draw needn't show every extreme that they name: `decay_wide`: each entry is the logarithm of one head's retention factor at one position. `decay_narrow`: each entry is the logarithm of one head's retention factor at one position.
All inputs are finite; a program needn't handle non-finite values.
Results may differ from a plain program's by a relative error of at most 0.02.
Values may be sent and summed in bfloat16 or wider, within the bound.
No kernel may reach another device: no remote copies, remote signals or barrier semaphores. Data moves between devices by JAX's collectives and lax.ppermute only.
A program may use at most 128 MiB of HBM per device.

v0:
```python
import functools

import jax
import jax.numpy as jnp
import numpy as np
from jax import lax
from jax.experimental import pallas as pl
from jax.experimental.pallas import tpu as pltpu
from jax.sharding import PartitionSpec as P


HDW = 128
HDN = 64
SPAN = 128

head_eps = 1e-05
norm_eps = 1e-06
rope_base = 10000.0


F32 = jnp.float32
BF16 = jnp.bfloat16
VM = pl.BlockSpec(memory_space=pltpu.VMEM)


def call(kernel, out_shape, count, flops, nbytes):
    return pl.pallas_call(
        kernel,
        out_shape=out_shape,
        in_specs=[VM] * count,
        out_specs=jax.tree.map(lambda _: VM, out_shape),
        cost_estimate=pl.CostEstimate(flops=flops, bytes_accessed=nbytes, transcendentals=0),
    )


def scalar_call(kernel, out_shape, count, flops, nbytes, scratch=()):
    return pl.pallas_call(
        kernel,
        out_shape=out_shape,
        in_specs=[pl.BlockSpec(memory_space=pltpu.SMEM)] + [VM] * count,
        out_specs=jax.tree.map(lambda _: VM, out_shape),
        scratch_shapes=scratch,
        cost_estimate=pl.CostEstimate(flops=flops, bytes_accessed=nbytes, transcendentals=0),
    )


def lane_rates(width, lanes):
    half = width // 2
    lane = np.arange(lanes) % width
    return rope_base ** (-(lane % half).astype(np.float64) / half), np.where(lane < half, -1.0, 1.0)


def offset_tables(length, width, lanes):
    rates, signs = lane_rates(width, lanes)
    angles = np.arange(length, dtype=np.float64)[:, None] * rates[None, :]
    return (
        jnp.asarray(np.cos(angles), F32),
        jnp.asarray(np.sin(angles) * signs[None, :], F32),
    )


def start_rows(places, length, lanes):
    starts = SPAN * np.arange(places * (length // SPAN), dtype=np.float64)[:, None]
    rows = []
    for width in (HDW, HDN):
        rates, signs = lane_rates(width, lanes)
        angle = starts * rates[None, :]
        rows += [np.cos(angle), np.sin(angle) * signs[None, :]]
    return jnp.asarray(np.stack(rows).reshape(4, places, length // SPAN, lanes), F32)


def lane_iota(shape):
    return lax.broadcasted_iota(jnp.int32, shape, 1)


def rotary(x, cos_at, sin_at, width):
    half = width // 2
    lanes = x.shape[1]
    if lanes == width:
        other = pltpu.roll(x, half, 1)
    else:
        other = jnp.where(
            lane_iota(x.shape) % width < half,
            pltpu.roll(x, lanes - half, 1),
            pltpu.roll(x, half, 1),
        )
    return x * cos_at + other * sin_at


def full_tables(cos_r, sin_r, rows, at):
    cos_all, sin_all = [], []
    for n in range(rows.shape[1]):
        cos_p, sin_p = rows[at, n : n + 1, :], rows[at + 1, n : n + 1, :]
        cos_all.append(cos_r * cos_p - sin_r * sin_p)
        sin_all.append(sin_r * cos_p + cos_r * sin_p)
    return jnp.concatenate(cos_all, axis=0), jnp.concatenate(sin_all, axis=0)


def by_head(low, high, lanes):
    rows = low.shape[0]
    return jnp.where(lane_iota((rows, lanes)) < HDN, low, high)


def state_kernel(kw, vw, kn, vn, dw, dn, rows, cwr, swr, cnr, snr, out, col, row):
    length, lanes = kw.shape
    head = lax.broadcasted_iota(jnp.int32, (8, length), 0)
    c = jnp.where(head == 0, dw[0:1, :], 0.0)
    for n in range(dn.shape[0]):
        c = jnp.where(head == n + 1, dn[n : n + 1, :], c)
    step = 1
    while step < length:
        c = c + jnp.where(lane_iota(c.shape) >= step, pltpu.roll(c, step, 1), 0.0)
        step *= 2
    row[...] = c
    c = c.T
    col[...] = c
    last = c[length - 1 : length, :]
    tail = jnp.exp(last - c)
    cos_w, sin_w = full_tables(cwr[...], swr[...], rows[...], 0)
    k = rotary(kw[...].astype(F32), cos_w, sin_w, HDW) * (HDW ** (-0.5)) * tail[:, 0:1]
    wide = lax.dot_general(
        k.astype(BF16), vw[...], (((0,), (0,)), ((), ())), preferred_element_type=F32
    )
    cos_n, sin_n = full_tables(cnr[...], snr[...], rows[...], 2)
    k = rotary(kn[...].astype(F32), cos_n, sin_n, HDN) * (HDN ** (-0.5))
    k = k * by_head(tail[:, 1:2], tail[:, 2:3], lanes)
    both = lax.dot_general(
        k.astype(BF16), vn[...], (((0,), (0,)), ((), ())), preferred_element_type=F32
    )
    narrow = jnp.where(lane_iota((HDN, lanes)) < HDN, both[:HDN], both[HDN:])
    total = jnp.exp(last)
    row_w = jnp.broadcast_to(total[:, 0:1], (8, lanes))
    row_n = jnp.broadcast_to(by_head(total[:, 1:2], total[:, 2:3], lanes), (8, lanes))
    out[...] = jnp.concatenate([wide, narrow, row_w, row_n], axis=0).astype(BF16)


def local_kernel(qw, kw, vw, qn, kn, vn, col, row, rows, cwr, swr, cnr, snr, ow, on, qws, qns):
    length, lanes = kw.shape
    size = 256 if length % 256 == 0 else 128
    blocks = length // size
    c = col[...]
    grown = jnp.exp(c)

    def turned(q, k, cos_r, sin_r, at, width):
        cos_at, sin_at = full_tables(cos_r[...], sin_r[...], rows[...], at)
        return (
            rotary(q[...].astype(F32), cos_at, sin_at, width),
            (rotary(k[...].astype(F32), cos_at, sin_at, width) * width ** (-0.5)).astype(BF16),
        )

    def attend(q, k, v, i, head):
        total = None
        for j in range(i + 1):
            scores = lax.dot_general(
                q, k[j * size : (j + 1) * size], (((1,), (1,)), ((), ())), preferred_element_type=F32
            )
            spread = c[i * size : (i + 1) * size, head : head + 1] - row[
                head : head + 1, j * size : (j + 1) * size
            ]
            factor = jnp.exp(jnp.minimum(spread, 0.0))
            if i == j:
                t = lax.broadcasted_iota(jnp.int32, (size, size), 0)
                s = lax.broadcasted_iota(jnp.int32, (size, size), 1)
                factor = jnp.where(t >= s, factor, 0.0)
            part = jnp.dot(
                (scores * factor).astype(BF16),
                v[j * size : (j + 1) * size, :],
                preferred_element_type=F32,
            )
            total = part if total is None else total + part
        return total

    q, k = turned(qw, kw, cwr, swr, 0, HDW)
    qws[...] = (q * grown[:, 0:1]).astype(BF16)
    q = q.astype(BF16)
    for i in range(blocks):
        ow[i * size : (i + 1) * size, :] = attend(q[i * size : (i + 1) * size], k, vw, i, 0)
    q, k = turned(qn, kn, cnr, snr, 2, HDN)
    qns[...] = (q * by_head(grown[:, 1:2], grown[:, 2:3], lanes)).astype(BF16)
    for i in range(blocks):
        part = q[i * size : (i + 1) * size]
        low = lane_iota(part.shape) < HDN
        first = attend(jnp.where(low, part, 0.0).astype(BF16), k, vn, i, 1)
        second = attend(jnp.where(low, 0.0, part).astype(BF16), k, vn, i, 2)
        on[i * size : (i + 1) * size, :] = jnp.where(low, first, second)


STATE = HDW + HDN


def decays(pack):
    lanes = pack.shape[1]
    return jnp.concatenate(
        [
            jnp.broadcast_to(pack[STATE : STATE + 1], (HDW, lanes)),
            jnp.broadcast_to(pack[STATE + 8 : STATE + 9], (HDN, lanes)),
        ],
        axis=0,
    )


def ordered(late, own, other):
    flag = late[0] == 1
    own, other = own[...].astype(F32), other[...].astype(F32)
    return jnp.where(flag, other, own), jnp.where(flag, own, other)


def pair_kernel(late, own, other, out):
    first, second = ordered(late, own, other)
    out[...] = jnp.concatenate(
        [first[:STATE] * decays(second) + second[:STATE], first[STATE:] * second[STATE:]], axis=0
    ).astype(BF16)


def finish_kernel(tp, late, own, other, ow, on, qws, qns, gw, gn, *refs):
    earlier, outs, out = refs[: -tp - 1], refs[-tp - 1 : -1], refs[-1]
    lanes = ow.shape[1]
    state, decay = None, None
    for got in earlier:
        got = got[...].astype(F32)
        state = got[:STATE] if state is None else state + got[:STATE] * decay
        decay = decays(got) if decay is None else decay * decays(got)
    first, _ = ordered(late, own, other)
    state = jnp.where(late[0] == 1, state * decays(first) + first[:STATE], state).astype(BF16)
    wide = ow[...] + jnp.dot(qws[...], state[0:HDW, :], preferred_element_type=F32)
    packed = state[HDW:STATE, :]
    low = lane_iota(packed.shape) < HDN
    zero = jnp.zeros_like(packed)
    square = jnp.concatenate(
        [jnp.where(low, packed, zero), jnp.where(low, zero, packed)], axis=0
    )
    narrow = on[...] + jnp.dot(qns[...], square, preferred_element_type=F32)

    def gated(normed, gate):
        g = gate[...].astype(F32)
        return (g / (1.0 + jnp.exp(-g)) * normed).astype(BF16)

    centre = wide - jnp.mean(wide, axis=1, keepdims=True)
    spread = jnp.mean(centre * centre, axis=1, keepdims=True)
    out[:, 0:lanes] = gated(centre * lax.rsqrt(spread + head_eps), gw)

    low = lane_iota(narrow.shape) < HDN

    def head_mean(x):
        first = jnp.sum(jnp.where(low, x, 0.0), axis=1, keepdims=True)
        second = jnp.sum(jnp.where(low, 0.0, x), axis=1, keepdims=True)
        return jnp.where(low, first, second) * (1.0 / HDN)

    centre = narrow - head_mean(narrow)
    out[:, lanes : 2 * lanes] = gated(
        centre * lax.rsqrt(head_mean(centre * centre) + head_eps), gn
    )
    piece = outs[0].shape[0]
    for m, rows in enumerate(outs):
        start = pl.multiple_of(late[1 + m] * piece, 16)
        rows[...] = out[pl.ds(start, piece), :]


def middle_kernel(stream, gain, wide, narrow, *refs):
    *inputs, middle, first, second = refs
    count = (len(inputs) + 1) // 2
    pieces, weights = inputs[:count], inputs[count:]
    lanes = wide.shape[0]
    own = pieces[0][...]
    total = jnp.dot(own[:, :lanes], wide[...], preferred_element_type=F32)
    total = total + jnp.dot(own[:, lanes:], narrow[...], preferred_element_type=F32)
    for piece, weight in zip(pieces[1:], weights):
        total = total + jnp.dot(piece[...], weight[...], preferred_element_type=F32)
    rounded = (stream[...].astype(F32) + total).astype(BF16)
    middle[...] = rounded
    x = rounded.astype(F32)
    scale = lax.rsqrt(jnp.mean(x * x, axis=-1, keepdims=True) + norm_eps)
    normed = (x * scale * gain[...].astype(F32)).astype(BF16)
    half = normed.shape[0] // 2
    first[...] = normed[:half]
    second[...] = normed[half:]


def up_kernel(at, own_a, own_b, x_a, y_a, y_b, x_b, *refs):
    *blocks, out, x = refs
    depth = blocks[0].shape[0]
    rows = own_a.shape[0]

    @pl.when(pl.program_id(0) == 0)
    def _():
        for n, piece in enumerate(
            (own_a, own_b, x_a, x_b.at[:rows], y_a.at[:rows], y_b, y_a.at[rows:], x_b.at[rows:])
        ):
            x[n * rows : (n + 1) * rows, :] = piece[...]

    total = None
    for n, block in enumerate(blocks):
        columns = pl.ds(pl.multiple_of(at[n] * depth, 128), depth)
        part = jnp.dot(x[:, columns], block[...], preferred_element_type=F32)
        total = part if total is None else total + part
    total = jnp.maximum(total, 0.0)
    out[...] = (total * total).astype(BF16)


def up_project(at, pieces, blocks):
    width = blocks[0].shape[1]
    rows, depth = sum(p.shape[0] for p in pieces), pieces[0].shape[1]
    tile = 512
    run = pl.pallas_call(
        up_kernel,
        out_shape=jax.ShapeDtypeStruct((rows, width), BF16),
        grid_spec=pltpu.PrefetchScalarGridSpec(
            num_scalar_prefetch=1,
            grid=(width // tile,),
            in_specs=[pl.BlockSpec(p.shape, lambda n, a: (0, 0)) for p in pieces]
            + [pl.BlockSpec((b.shape[0], tile), lambda n, a: (0, n)) for b in blocks],
            out_specs=pl.BlockSpec((rows, tile), lambda n, a: (0, n)),
            scratch_shapes=[pltpu.VMEM((rows, depth), BF16)],
        ),
        cost_estimate=pl.CostEstimate(
            flops=2 * rows * depth * width,
            bytes_accessed=2 * (rows * depth + depth * width + rows * width),
            transcendentals=0,
        ),
    )
    return run(at, *pieces, *blocks)


SIDE = 256


def place_kernel(at, middle, *refs):
    *parts, out = refs
    place = 0
    for n in range(0, len(parts), 4):
        group = parts[n : n + 4]
        for side in range(group[0].shape[1] // SIDE):
            here = slice(side * SIDE, (side + 1) * SIDE)
            columns = pl.ds(pl.multiple_of(at[place] * SIDE, 128), SIDE)
            place += 1
            total = middle[:, columns].astype(F32)
            for part in group:
                total = total + part[:, here].astype(F32)
            out[:, columns] = total.astype(BF16)


def last_kernel(at, out_in, middle, *refs):
    *parts, out = refs
    total = middle[...].astype(F32)
    for part in parts:
        total = total + part[...].astype(F32)
    out[...] = total.astype(BF16)


def place_last(at, out, middle, parts):
    rows = middle.shape[0]
    skip = middle.shape[1] // SIDE - parts[0].shape[1] // SIDE

    def column(n, a):
        return (0, a[skip + n])

    run = pl.pallas_call(
        last_kernel,
        out_shape=jax.ShapeDtypeStruct(middle.shape, BF16),
        grid_spec=pltpu.PrefetchScalarGridSpec(
            num_scalar_prefetch=1,
            grid=(parts[0].shape[1] // SIDE,),
            in_specs=[pl.BlockSpec(memory_space=pl.ANY), pl.BlockSpec((rows, SIDE), column)]
            + [pl.BlockSpec((rows, SIDE), lambda n, a: (0, n))] * len(parts),
            out_specs=pl.BlockSpec((rows, SIDE), column),
        ),
        input_output_aliases={1: 0},
        cost_estimate=pl.CostEstimate(
            flops=middle.size, bytes_accessed=4 * middle.size, transcendentals=0
        ),
    )
    return run(at, out, middle, *parts)


def exchange(array, axis, size, move):
    pairs = [(i, move(i)) for i in range(size)]
    return lax.ppermute(array, axis, [(i, j) for i, j in pairs if j is not None and 0 <= j < size])


def retention(tensors, sp, tp):
    (qw, kw, vw, gw, dw, qn, kn, vn, gn, dn) = tensors
    length, lanes = qw.shape
    rows = lax.dynamic_index_in_dim(
        start_rows(sp, length, lanes), lax.axis_index("sp"), 1, keepdims=False
    )
    tables = offset_tables(SPAN, HDW, lanes) + offset_tables(SPAN, HDN, lanes)
    sds = jax.ShapeDtypeStruct
    unit = length * lanes
    state, col, running = call(
        state_kernel,
        (sds((STATE + 16, lanes), BF16), sds((length, 8), F32), sds((8, length), F32)),
        11,
        4 * unit * lanes,
        24 * unit,
    )(kw, vw, kn, vn, dw, dn, rows, *tables)
    ow, on, qws, qns = call(
        local_kernel,
        (sds((length, lanes), F32),) * 2 + (sds((length, lanes), BF16),) * 2,
        13,
        8 * unit * length,
        40 * unit,
    )(qw, kw, vw, qn, kn, vn, col, running, rows, *tables)
    mine = lax.axis_index("tp")
    late = jnp.stack([lax.axis_index("sp") % 2] + [mine ^ m for m in range(tp)]).astype(jnp.int32)
    other = exchange(state, "sp", sp, lambda i: i ^ 1)
    pair = scalar_call(pair_kernel, sds(state.shape, BF16), 2, unit, 6 * state.size)(
        late, state, other
    )
    earlier = [exchange(pair, "sp", sp, lambda i: i + 2 * n) for n in range(1, sp // 2)]
    pieces = scalar_call(
        functools.partial(finish_kernel, tp),
        (sds((length // tp, 2 * lanes), BF16),) * tp,
        8 + len(earlier),
        4 * unit * lanes,
        24 * unit,
        [pltpu.VMEM((length, 2 * lanes), BF16)],
    )(late, state, other, ow, on, qws, qns, gw, gn, *earlier)
    return pieces, other


def to_middle(mixed, stream_in, output_wide, output_narrow, norm_gain, tp):
    weights = [jnp.concatenate([output_wide, output_narrow], axis=0)]
    pieces = [mixed[0]]
    for m in range(1, tp):
        low = m & (m - 1)
        weights.append(exchange(weights[low], "tp", tp, lambda i: i ^ (m ^ low)))
        pieces.append(exchange(mixed[m], "tp", tp, lambda i: i ^ m))
    sds = jax.ShapeDtypeStruct
    rows, depth = stream_in.shape
    return call(
        middle_kernel,
        (sds((rows, depth), BF16),) + (sds((rows // 2, depth), BF16),) * 2,
        3 + 2 * tp,
        2 * rows * mixed[0].shape[1] * tp * depth,
        8 * stream_in.size,
    )(stream_in, norm_gain[None, :], output_wide, output_narrow, *pieces, *weights[1:])


def tie(array, *after):
    return lax.optimization_barrier((array, *after))[0]


def plane_layer(tensors, stream_in, output_wide, output_narrow, norm_gain, up_weight, down_weight, sp, tp):
    z, y = lax.axis_index("sp") // 2, lax.axis_index("sp") % 2
    core = lax.axis_index("tp") % 2
    at_end = (z == 0) | (z == 3)

    def swap_y_core(array, after=()):
        def move(i):
            s, t = divmod(i, tp)
            return None if s & 1 == t & 1 else (s ^ 1) * tp + (t ^ 1)

        return exchange(tie(array, *after), ("sp", "tp"), sp * tp, move)

    def along_z(array, table):
        def move(i):
            return table[i // 2] * 2 + i % 2 if i // 2 in table else None

        return exchange(array, "sp", sp, move)

    def ends(array):
        return along_z(array, {0: 1, 1: 0, 2: 3, 3: 2})

    def middles(array):
        return along_z(array, {1: 2, 2: 1})

    def outwards(array):
        return along_z(array, {1: 0, 2: 3})

    def by_x(array):
        return exchange(array, "tp", tp, lambda i: i ^ 2)

    def by_y(array):
        return exchange(array, "sp", sp, lambda i: i ^ 1)

    def both_cores(slot):
        return [slot, exchange(slot, "tp", tp, lambda i: i ^ 1)]

    slots = [z, z ^ 1, (z + 2) % 4, (z ^ 1) ^ 2]
    order = jnp.stack([s * 2 + c for s in slots for c in (core, 1 - core)]).astype(jnp.int32)

    def own_block(block, after=()):
        return jnp.where(y == core, block, swap_y_core(block, after))

    up_own = own_block(up_weight)
    up_near, up_cross = ends(up_own), middles(up_own)

    mixed, other_state = retention(tensors, sp, tp)

    down_own = own_block(down_weight, (other_state,))
    down_near = ends(down_own)
    up_in = middles(up_near)
    up_out = outwards(up_cross)
    down_cross = middles(tie(down_own, up_near))
    up_last = outwards(up_in)

    middle, first, second = to_middle(mixed, stream_in, output_wide, output_narrow, norm_gain, tp)

    x_a, y_b = by_x(first), by_y(second)
    down_in = middles(tie(down_near, y_b))
    y_a = by_y(jnp.concatenate([first, x_a], axis=0))
    x_b = by_x(jnp.concatenate([second, y_b], axis=0))
    there = (y_a, x_b)

    down_out = outwards(down_cross)
    up_far = jnp.where(at_end, up_out, up_in)
    up_final = jnp.where(at_end, tie(up_last, *there), up_cross)
    down_last = outwards(tie(down_in, up_final))

    blocks = []
    for slot in (up_own, up_near, up_far, up_final):
        blocks += both_cores(slot)
    hidden = up_project(order, [first, second, x_a, y_a, y_b, x_b], blocks)

    def down(group):
        blocks = []
        for d in group:
            blocks += both_cores(d)
        part = jnp.dot(
            hidden, jnp.concatenate(blocks, axis=1), preferred_element_type=F32
        ).astype(BF16)
        rows = part.shape[0] // 4
        keep, to_x, to_y, across = (part[m * rows : (m + 1) * rows] for m in range(4))
        return [
            keep,
            exchange(across, ("sp", "tp"), sp * tp, lambda i: i ^ tp ^ 2),
            by_x(to_x),
            by_y(to_y),
        ]

    sums = down([down_own, down_near])
    down_far = jnp.where(at_end, tie(down_out, hidden), down_in)
    sums += down([down_far])
    out = scalar_call(
        place_kernel,
        jax.ShapeDtypeStruct(middle.shape, BF16),
        1 + len(sums),
        middle.size,
        8 * middle.size,
    )(order, middle, *sums)
    down_final = jnp.where(at_end, tie(down_last, out), down_cross)
    return place_last(order, out, middle, down([down_final]))


def group_feed_forward(middle, normed):
    def run(up_weight, down_weight):
        rows = lax.all_gather(normed, "tp", axis=0, tiled=True)
        up_sum = jnp.dot(
            rows, lax.all_gather(up_weight, "sp", axis=0, tiled=True), preferred_element_type=F32
        )
        hidden = jnp.square(jax.nn.relu(up_sum)).astype(BF16)
        down_sum = jnp.dot(
            hidden, lax.all_gather(down_weight, "sp", axis=1, tiled=True), preferred_element_type=F32
        )
        down_rows = lax.psum_scatter(
            down_sum.astype(BF16), "tp", scatter_dimension=0, tiled=True
        ).astype(F32)
        return (middle.astype(F32) + down_rows).astype(BF16)

    return run


def on_device(sp, tp, stream_in, *rest):
    *tensors, output_wide, output_narrow, norm_gain, up_weight, down_weight = rest
    if sp == 8 and tp == 4:
        return plane_layer(
            tensors, stream_in, output_wide, output_narrow, norm_gain, up_weight, down_weight, sp, tp
        )
    mixed, _ = retention(tensors, sp, tp)
    middle, first, second = to_middle(mixed, stream_in, output_wide, output_narrow, norm_gain, tp)
    normed = jnp.concatenate([first, second], axis=0)
    return group_feed_forward(middle, normed)(up_weight, down_weight)


def solution(mesh):
    split = P("sp", "tp")
    in_specs = (
        (P(("sp", "tp"), None),)
        + ((split,) * 4 + (P("tp", "sp"),)) * 2
        + (P("tp", None), P("tp", None), P(), split, P("tp", "sp"))
    )
    sp, tp = mesh.shape["sp"], mesh.shape["tp"]
    return jax.shard_map(
        functools.partial(on_device, sp, tp),
        mesh=mesh,
        in_specs=in_specs,
        out_specs=P(("sp", "tp"), None),
        check_vma=False,
    )
```

profile of v0, /device:TPU:0, one launch (start us, length us, event | category | flops | bytes accessed | tf_op | source)
XLA Modules:
  0.0 280.9 jit_solution(11573148695506773114)
XLA Ops:
  0.9 1.9 constant_dynamic-update-slice_fusion.1
  2.8 1.9 constant_dynamic-update-slice_fusion
  4.7 3.0 %collective-permute-start.8 = (bf16[256,2048]{1,0:T(8,128)(2,1)}, bf16[256,2048]{1,0:T(8,128)(2,1)}, u32[]{:S(2)}, u32[]{:S(2)}) collective-permute-start(bf16[256,2048]{1,0:T(8,128)(2,1)} %constant_dynamic-update-slice_fusion), channel_id=1, source_target_pairs={{0,2},{1,3},{2,0},{3,1},{4,6},{5,7},{6,4},{7,5},{8,10},{9,11},{10,... | collective-permute-start | bytes 3145736 | tf_op jit(solution)/shard_map/ppermute | solution.py:377
  7.7 1.3 broadcast_select_fusion.5.refs_0_
  9.0 1.6 collective-permute-start.16
  10.7 9.1 %collective-permute-start.7 = (bf16[256,2048]{1,0:T(8,128)(2,1)}, bf16[256,2048]{1,0:T(8,128)(2,1)S(1)}, u32[]{:S(2)}, u32[]{:S(2)}) collective-permute-start(bf16[256,2048]{1,0:T(8,128)(2,1)} %constant_dynamic-update-slice_fusion), channel_id=1, source_target_pairs={{0,1},{1,0},{2,3},{3,2},{4,5},{5,4},{6,7},{7,6},{8,9},{9,8},{10,11... | collective-permute-start | bytes 3145736 | tf_op jit(solution)/shard_map/ppermute | solution.py:377
  19.7 9.9 %collective-permute-done.8.refs_5_ = bf16[256,2048]{1,0:T(8,128)(2,1)} collective-permute-done((bf16[256,2048]{1,0:T(8,128)(2,1)}, bf16[256,2048]{1,0:T(8,128)(2,1)}, u32[]{:S(2)}, u32[]{:S(2)}) %collective-permute-start.8) | collective-permute-done | bytes 1048608 | tf_op jit(solution)/shard_map/ppermute | solution.py:377
  29.7 2.1 collective-permute-start.9
  31.8 1.3 dynamic-slice_bitcast_fusion.rows
  33.1 3.3 %shard_map.199 = (bf16[208,128]{1,0:T(8,128)(2,1)}, f32[768,8]{1,0:T(8,128)}, f32[8,768]{1,0:T(8,128)}) custom-call(bf16[768,128]{1,0:T(8,128)(2,1)} %kw.3, bf16[768,128]{1,0:T(8,128)(2,1)} %vw.3, bf16[768,128]{1,0:T(8,128)(2,1)} %kn.3, bf16[768,128]{1,0:T(8,128)(2,1)} %vn.3, f32[1,768]{1,0:T(1,128)} %dw.1, f32[2,768]{1,0:T(2,128)} %dn.1, ...), custom_call_target="tpu_custom_call" | custom-call | flops 50331648 | bytes 2359296 | tf_op jit(solution)/shard_map/pallas_call | solution.py:389
  36.4 1.1 collective-permute-start
  37.5 3.2 %collective-permute-done.other = bf16[208,128]{1,0:T(8,128)(2,1)S(1)} collective-permute-done((bf16[208,128]{1,0:T(8,128)(2,1)}, bf16[208,128]{1,0:T(8,128)(2,1)S(1)}, u32[]{:S(2)}, u32[]{:S(2)}) %collective-permute-start) | collective-permute-done | bytes 53280 | tf_op jit(solution)/shard_map/ppermute | solution.py:377
  40.7 1.6 collective-permute-start.24
  43.0 1.5 shard_map.201
  44.5 4.0 %collective-permute-start.1 = (bf16[208,128]{1,0:T(8,128)(2,1)}, bf16[208,128]{1,0:T(8,128)(2,1)S(1)}, u32[]{:S(2)}, u32[]{:S(2)}) collective-permute-start(bf16[208,128]{1,0:T(8,128)(2,1)} %shard_map.201), channel_id=1, source_target_pairs={{0,8},{4,12},{8,16},{12,20},{16,24},{20,28},{1,9},{5,13},{9,17},{1... | collective-permute-start | bytes 159752 | tf_op jit(solution)/shard_map/ppermute | solution.py:377
  48.5 2.4 collective-permute-done.1.refs_0_
  50.9 5.3 %collective-permute-start.2 = (bf16[208,128]{1,0:T(8,128)(2,1)}, bf16[208,128]{1,0:T(8,128)(2,1)S(1)}, u32[]{:S(2)}, u32[]{:S(2)}) collective-permute-start(bf16[208,128]{1,0:T(8,128)(2,1)} %shard_map.201), channel_id=1, source_target_pairs={{0,16},{4,20},{8,24},{12,28},{1,17},{5,21},{9,25},{13,29},{2,18},{... | collective-permute-start | bytes 159752 | tf_op jit(solution)/shard_map/ppermute | solution.py:377
  56.2 2.1 collective-permute-done.2.refs_1_
  58.3 6.8 %collective-permute-start.3 = (bf16[208,128]{1,0:T(8,128)(2,1)}, bf16[208,128]{1,0:T(8,128)(2,1)S(1)}, u32[]{:S(2)}, u32[]{:S(2)}) collective-permute-start(bf16[208,128]{1,0:T(8,128)(2,1)} %shard_map.201), channel_id=1, source_target_pairs={{0,24},{4,28},{1,25},{5,29},{2,26},{6,30},{3,27},{7,31}} | collective-permute-start | bytes 159752 | tf_op jit(solution)/shard_map/ppermute | solution.py:377
  65.1 5.0 %shard_map.200 = (f32[768,128]{1,0:T(8,128)}, f32[768,128]{1,0:T(8,128)}, bf16[768,128]{1,0:T(8,128)(2,1)}, bf16[768,128]{1,0:T(8,128)(2,1)}) custom-call(bf16[768,128]{1,0:T(8,128)(2,1)} %qw.1, bf16[768,128]{1,0:T(8,128)(2,1)} %kw.3, bf16[768,128]{1,0:T(8,128)(2,1)} %vw.3, bf16[768,128]{1,0:T(8,128)(2,1)} %qn.1, bf16[768,128]{1,0:T(8,128)(2,1)} %kn.3, ...), custom_call_target="tpu_custom_call" | custom-call | flops 603979776 | bytes 3932160 | tf_op jit(solution)/shard_map/pallas_call | solution.py:396
  70.7 3.1 %shard_map.202 = (bf16[192,256]{1,0:T(8,128)(2,1)}, bf16[192,256]{1,0:T(8,128)(2,1)}, bf16[192,256]{1,0:T(8,128)(2,1)}, bf16[192,256]{1,0:T(8,128)(2,1)}) custom-call(s32[5]{0:T(128)} %stack.59.late, bf16[208,128]{1,0:T(8,128)(2,1)} %get-tuple-element.26.own, bf16[208,128]{1,0:T(8,128)(2,1)} %copy-done.10, f32[768,128]{1,0:T(8,128)} %get-tuple-element.29.ow, ...), custom_call_target="tpu_custom_call" | custom-call | flops 50331648 | bytes 2359296 | tf_op jit(solution)/shard_map/pallas_call | solution.py:410
  73.8 1.5 collective-permute-done.4.refs_1_
  75.3 1.5 collective-permute-start.5
  76.8 3.6 %collective-permute-done.5.refs_2_ = bf16[192,256]{1,0:T(8,128)(2,1)S(1)} collective-permute-done((bf16[192,256]{1,0:T(8,128)(2,1)}, bf16[192,256]{1,0:T(8,128)(2,1)S(1)}, u32[]{:S(2)}, u32[]{:S(2)}) %collective-permute-start.5) | collective-permute-done | bytes 98336 | tf_op jit(solution)/shard_map/ppermute | solution.py:377
  80.8 4.9 %collective-permute-done.6.refs_3_ = bf16[192,256]{1,0:T(8,128)(2,1)S(1)} collective-permute-done((bf16[192,256]{1,0:T(8,128)(2,1)}, bf16[192,256]{1,0:T(8,128)(2,1)S(1)}, u32[]{:S(2)}, u32[]{:S(2)}) %collective-permute-start.6) | collective-permute-done | bytes 98336 | tf_op jit(solution)/shard_map/ppermute | solution.py:377
  85.7 1.6 collective-permute-start.18
  87.3 1.7 collective-permute-start.20
  90.6 4.9 %shard_map.203 = (bf16[192,2048]{1,0:T(8,128)(2,1)}, bf16[96,2048]{1,0:T(8,128)(2,1)}, bf16[96,2048]{1,0:T(8,128)(2,1)}) custom-call(bf16[192,2048]{1,0:T(8,128)(2,1)} %stream.1, bf16[1,2048]{1,0:T(2,128)(2,1)} %broadcast_in_dim.3.gain, bf16[128,2048]{1,0:T(8,128)(2,1)} %wide.1, bf16[128,2048]{1,0:T(8,128)(2,1)} %narrow.1, ...), custom_call_target="tpu_custom_call" | custom-call | flops 805306368 | bytes 3145728 | tf_op jit(solution)/shard_map/pallas_call | solution.py:430
  96.8 1.3 collective-permute-start.19
  98.1 1.5 collective-permute-start.12
  99.6 1.3 collective-permute-start.22
  100.9 6.0 %collective-permute-done.10.x_a = bf16[96,2048]{1,0:T(8,128)(2,1)S(1)} collective-permute-done((bf16[96,2048]{1,0:T(8,128)(2,1)}, bf16[96,2048]{1,0:T(8,128)(2,1)S(1)}, u32[]{:S(2)}, u32[]{:S(2)}) %collective-permute-start.10) | collective-permute-done | bytes 393248 | tf_op jit(solution)/shard_map/ppermute | solution.py:377
  108.1 1.6 collective-permute-done.12.y_b
  110.8 1.4 collective-permute-start.13
  112.1 10.7 %collective-permute-done.26 = bf16[2048,256]{1,0:T(8,128)(2,1)S(1)} collective-permute-done((bf16[2048,256]{1,0:T(8,128)(2,1)S(1)}, bf16[2048,256]{1,0:T(8,128)(2,1)S(1)}, u32[]{:S(2)}, u32[]{:S(2)}) %collective-permute-start.26) | collective-permute-done | bytes 1048608 | tf_op jit(solution)/shard_map/ppermute | solution.py:377
  123.8 21.6 %collective-permute-done.19 = bf16[256,2048]{1,0:T(8,128)(2,1)} collective-permute-done((bf16[256,2048]{1,0:T(8,128)(2,1)}, bf16[256,2048]{1,0:T(8,128)(2,1)}, u32[]{:S(2)}, u32[]{:S(2)}) %collective-permute-start.19) | collective-permute-done | bytes 1048608 | tf_op jit(solution)/shard_map/ppermute | solution.py:377
  146.2 2.3 broadcast_select_fusion.4.refs_4_
  148.6 1.7 collective-permute-start.33
  150.2 17.2 %collective-permute-done.22 = bf16[256,2048]{1,0:T(8,128)(2,1)} collective-permute-done((bf16[256,2048]{1,0:T(8,128)(2,1)}, bf16[256,2048]{1,0:T(8,128)(2,1)}, u32[]{:S(2)}, u32[]{:S(2)}) %collective-permute-start.22) | collective-permute-done | bytes 1048608 | tf_op jit(solution)/shard_map/ppermute | solution.py:377
  167.4 2.4 broadcast_select_fusion.3.refs_6_
  170.3 1.3 collective-permute-start.32
  172.8 1.5 collective-permute-start.38
  174.3 12.0 %shard_map.204 = bf16[768,2048]{1,0:T(8,128)(2,1)} custom-call(s32[8]{0:T(128)} %stack.53.at, bf16[96,2048]{1,0:T(8,128)(2,1)} %get-tuple-element.38.own_a, bf16[96,2048]{1,0:T(8,128)(2,1)} %get-tuple-element.39.own_b, bf16[96,2048]{1,0:T(8,128)(2,1)} %copy-done.8, bf16[192,2048]{1,0:T(8,128)(2,1)} %collective-permute-done.11.y_a, ...), custom_call_target="tpu_custom_call" | custom-call | flops 6442450944 | bytes 14680064 | tf_op jit(solution)/shard_map/pallas_call | solution.py:321
  186.2 32.9 %collective-permute-done.32 = bf16[2048,256]{1,0:T(8,128)(2,1)} collective-permute-done((bf16[2048,256]{1,0:T(8,128)(2,1)S(1)}, bf16[2048,256]{1,0:T(8,128)(2,1)}, u32[]{:S(2)}, u32[]{:S(2)}) %collective-permute-start.32) | collective-permute-done | bytes 1048608 | tf_op jit(solution)/shard_map/ppermute | solution.py:377
  219.2 1.3 broadcast_select_fusion.1
  220.6 5.9 %fusion.16 = bf16[768,1024]{1,0:T(8,128)(2,1)S(1)} fusion(bf16[768,2048]{1,0:T(8,128)(2,1)} %shard_map.204, bf16[2048,256]{1,0:T(8,128)(2,1)} %collective-permute-done.27, bf16[2048,256]{1,0:T(8,128)(2,1)S(1)} %copy-done.24, bf16[2048,256]{1,0:T(8,128)(2,1)} %collective-permute-done.25, bf16[2048,256]{1,0:T(8,128)(2,1)S(1)} %broadcast_select_fusion.2), kind=kOutput, calls=%fused_computation.16 | convolution fusion | flops 3238789120 | bytes 8912896 | tf_op jit(solution)/shard_map/dot_general | solution.py:519
  227.5 2.0 collective-permute-start.29
  229.5 1.5 collective-permute-start.30
  230.9 1.8 fusion.22
  233.5 1.4 collective-permute-start.35
  234.9 5.5 %collective-permute-done.28.refs_1_ = bf16[192,1024]{1,0:T(8,128)(2,1)S(1)} collective-permute-done((bf16[192,1024]{1,0:T(8,128)(2,1)S(1)}, bf16[192,1024]{1,0:T(8,128)(2,1)S(1)}, u32[]{:S(2)}, u32[]{:S(2)}) %collective-permute-start.28) | collective-permute-done | bytes 393248 | tf_op jit(solution)/shard_map/ppermute | solution.py:377
  240.4 2.0 collective-permute-start.36
  242.4 5.5 %collective-permute-done.29.refs_2_ = bf16[192,1024]{1,0:T(8,128)(2,1)S(1)} collective-permute-done((bf16[192,1024]{1,0:T(8,128)(2,1)S(1)}, bf16[192,1024]{1,0:T(8,128)(2,1)S(1)}, u32[]{:S(2)}, u32[]{:S(2)}) %collective-permute-start.29) | collective-permute-done | bytes 393248 | tf_op jit(solution)/shard_map/ppermute | solution.py:377
  247.9 1.5 collective-permute-start.37
  249.4 3.7 %collective-permute-done.35.refs_5_ = bf16[192,512]{1,0:T(8,128)(2,1)S(1)} collective-permute-done((bf16[192,512]{1,0:T(8,128)(2,1)S(1)}, bf16[192,512]{1,0:T(8,128)(2,1)S(1)}, u32[]{:S(2)}, u32[]{:S(2)}) %collective-permute-start.35) | collective-permute-done | bytes 196640 | tf_op jit(solution)/shard_map/ppermute | solution.py:377
  253.1 3.2 %collective-permute-done.36.refs_6_ = bf16[192,512]{1,0:T(8,128)(2,1)} collective-permute-done((bf16[192,512]{1,0:T(8,128)(2,1)S(1)}, bf16[192,512]{1,0:T(8,128)(2,1)}, u32[]{:S(2)}, u32[]{:S(2)}) %collective-permute-start.36) | collective-permute-done | bytes 196640 | tf_op jit(solution)/shard_map/ppermute | solution.py:377
  256.9 3.2 %shard_map.205.out_in = bf16[192,2048]{1,0:T(8,128)(2,1)} custom-call(s32[8]{0:T(128)} %stack.53.at, bf16[192,2048]{1,0:T(8,128)(2,1)} %get-tuple-element.37.middle, bf16[192,1024]{1,0:T(8,128)(2,1)} %get-tuple-element.50.refs_0_, bf16[192,1024]{1,0:T(8,128)(2,1)} %copy-done.3, bf16[192,1024]{1,0:T(8,128)(2,1)} %copy-done.4, bf16[192,1024]{1,0:T(8,128)(2,1)} %copy-done.5, ...), custom_call_target="tpu_custom_call" | custom-call | flops 393216 | bytes 3145728 | tf_op jit(solution)/shard_map/pallas_call | solution.py:534
  260.3 2.6 collective-permute-done.39
  263.0 1.8 fusion.19
  265.5 2.1 collective-permute-start.40
  267.8 1.2 collective-permute-start.42
  269.0 5.2 %collective-permute-done.40.refs_1_ = bf16[192,512]{1,0:T(8,128)(2,1)S(1)} collective-permute-done((bf16[192,512]{1,0:T(8,128)(2,1)S(1)}, bf16[192,512]{1,0:T(8,128)(2,1)S(1)}, u32[]{:S(2)}, u32[]{:S(2)}) %collective-permute-start.40) | collective-permute-done | bytes 196640 | tf_op jit(solution)/shard_map/ppermute | solution.py:377
  274.2 2.7 collective-permute-done.41.refs_2_
  278.2 2.7 shard_map.206
  (104 shorter events, 16.0 us)
Async XLA Ops:
  0.0 40.7 %copy-start = (bf16[2048,256]{1,0:T(8,128)(2,1)S(1)}, bf16[2048,256]{1,0:T(8,128)(2,1)}, u32[]{:S(2)}) copy-start(bf16[2048,256]{1,0:T(8,128)(2,1)} %param.36) | copy-start | bytes 3145732
  0.0 7.7 %collective-permute-start.14 = (bf16[256,2048]{1,0:T(8,128)(2,1)}, bf16[256,2048]{1,0:T(8,128)(2,1)S(1)}, u32[]{:S(2)}, u32[]{:S(2)}) collective-permute-start(bf16[256,2048]{1,0:T(8,128)(2,1)} %param.35), channel_id=1, source_target_pairs={{1,4},{3,6},{4,1},{6,3},{9,12},{11,14},{12,9},{14,11},{17,20},{19,... | collective-permute-start | bytes 3145736 | tf_op jit(solution)/shard_map/ppermute | solution.py:377
  4.7 25.0 %collective-permute-start.8 = (bf16[256,2048]{1,0:T(8,128)(2,1)}, bf16[256,2048]{1,0:T(8,128)(2,1)}, u32[]{:S(2)}, u32[]{:S(2)}) collective-permute-start(bf16[256,2048]{1,0:T(8,128)(2,1)} %constant_dynamic-update-slice_fusion), channel_id=1, source_target_pairs={{0,2},{1,3},{2,0},{3,1},{4,6},{5,7},{6,4},{7,5},{8,10},{9,11},{10,... | collective-permute-start | bytes 3145736 | tf_op jit(solution)/shard_map/ppermute | solution.py:377
  9.0 113.8 %copy-start.1 = (bf16[256,2048]{1,0:T(8,128)(2,1)}, bf16[256,2048]{1,0:T(8,128)(2,1)S(1)}, u32[]{:S(2)}) copy-start(bf16[256,2048]{1,0:T(8,128)(2,1)S(1)} %broadcast_select_fusion.5.refs_0_) | copy-start | bytes 3145732
  9.0 80.0 %copy-start.21 = (bf16[2048]{0:T(1024)(128)(2,1)S(1)}, bf16[2048]{0:T(1024)(128)(2,1)}, u32[]{:S(2)}) copy-start(bf16[2048]{0:T(1024)(128)(2,1)} %param.34) | copy-start | bytes 12292
  9.0 78.3 %collective-permute-start.16 = (bf16[256,2048]{1,0:T(8,128)(2,1)S(1)}, bf16[256,2048]{1,0:T(8,128)(2,1)}, u32[]{:S(2)}, u32[]{:S(2)}) collective-permute-start(bf16[256,2048]{1,0:T(8,128)(2,1)S(1)} %broadcast_select_fusion.5.refs_0_), channel_id=1, source_target_pairs={{0,8},{4,12},{8,0},{12,4},{16,24},{20,28},{24,16},{28,20},{1,9},{5... | collective-permute-start | bytes 3145736 | tf_op jit(solution)/shard_map/ppermute | solution.py:377
  10.7 78.9 %collective-permute-start.7 = (bf16[256,2048]{1,0:T(8,128)(2,1)}, bf16[256,2048]{1,0:T(8,128)(2,1)S(1)}, u32[]{:S(2)}, u32[]{:S(2)}) collective-permute-start(bf16[256,2048]{1,0:T(8,128)(2,1)} %constant_dynamic-update-slice_fusion), channel_id=1, source_target_pairs={{0,1},{1,0},{2,3},{3,2},{4,5},{5,4},{6,7},{7,6},{8,9},{9,8},{10,11... | collective-permute-start | bytes 3145736 | tf_op jit(solution)/shard_map/ppermute | solution.py:377
  29.7 59.9 %collective-permute-start.9 = (bf16[256,2048]{1,0:T(8,128)(2,1)}, bf16[256,2048]{1,0:T(8,128)(2,1)}, u32[]{:S(2)}, u32[]{:S(2)}) collective-permute-start(bf16[256,2048]{1,0:T(8,128)(2,1)} %collective-permute-done.8.refs_5_), channel_id=1, source_target_pairs={{0,1},{1,0},{2,3},{3,2},{4,5},{5,4},{6,7},{7,6},{8,9},{9,8},{10,11... | collective-permute-start | bytes 3145736 | tf_op jit(solution)/shard_map/ppermute | solution.py:377
  36.4 4.3 %collective-permute-start = (bf16[208,128]{1,0:T(8,128)(2,1)}, bf16[208,128]{1,0:T(8,128)(2,1)S(1)}, u32[]{:S(2)}, u32[]{:S(2)}) collective-permute-start(bf16[208,128]{1,0:T(8,128)(2,1)} %get-tuple-element.26.own), channel_id=1, source_target_pairs={{0,4},{4,0},{8,12},{12,8},{16,20},{20,16},{24,28},{28,24},{1,5},{5... | collective-permute-start | bytes 159752 | tf_op jit(solution)/shard_map/ppermute | solution.py:377
  40.7 2.3 copy-start.10
  40.7 55.8 %collective-permute-start.24 = (bf16[2048,256]{1,0:T(8,128)(2,1)S(1)}, bf16[2048,256]{1,0:T(8,128)(2,1)}, u32[]{:S(2)}, u32[]{:S(2)}) collective-permute-start(bf16[2048,256]{1,0:T(8,128)(2,1)S(1)} %copy-done), channel_id=1, source_target_pairs={{1,4},{3,6},{4,1},{6,3},{9,12},{11,14},{12,9},{14,11},{17,20},{19,... | collective-permute-start | bytes 3145736 | tf_op jit(solution)/shard_map/ppermute | solution.py:377
  44.5 6.4 %collective-permute-start.1 = (bf16[208,128]{1,0:T(8,128)(2,1)}, bf16[208,128]{1,0:T(8,128)(2,1)S(1)}, u32[]{:S(2)}, u32[]{:S(2)}) collective-permute-start(bf16[208,128]{1,0:T(8,128)(2,1)} %shard_map.201), channel_id=1, source_target_pairs={{0,8},{4,12},{8,16},{12,20},{16,24},{20,28},{1,9},{5,13},{9,17},{1... | collective-permute-start | bytes 159752 | tf_op jit(solution)/shard_map/ppermute | solution.py:377
  50.9 19.2 %copy-start.18 = (bf16[208,128]{1,0:T(8,128)(2,1)}, bf16[208,128]{1,0:T(8,128)(2,1)S(1)}, u32[]{:S(2)}) copy-start(bf16[208,128]{1,0:T(8,128)(2,1)S(1)} %collective-permute-done.1.refs_0_) | copy-start | bytes 159748
  50.9 7.4 %collective-permute-start.2 = (bf16[208,128]{1,0:T(8,128)(2,1)}, bf16[208,128]{1,0:T(8,128)(2,1)S(1)}, u32[]{:S(2)}, u32[]{:S(2)}) collective-permute-start(bf16[208,128]{1,0:T(8,128)(2,1)} %shard_map.201), channel_id=1, source_target_pairs={{0,16},{4,20},{8,24},{12,28},{1,17},{5,21},{9,25},{13,29},{2,18},{... | collective-permute-start | bytes 159752 | tf_op jit(solution)/shard_map/ppermute | solution.py:377
  58.3 11.8 %copy-start.19 = (bf16[208,128]{1,0:T(8,128)(2,1)}, bf16[208,128]{1,0:T(8,128)(2,1)S(1)}, u32[]{:S(2)}) copy-start(bf16[208,128]{1,0:T(8,128)(2,1)S(1)} %collective-permute-done.2.refs_1_) | copy-start | bytes 159748
  58.3 11.8 %collective-permute-start.3 = (bf16[208,128]{1,0:T(8,128)(2,1)}, bf16[208,128]{1,0:T(8,128)(2,1)S(1)}, u32[]{:S(2)}, u32[]{:S(2)}) collective-permute-start(bf16[208,128]{1,0:T(8,128)(2,1)} %shard_map.201), channel_id=1, source_target_pairs={{0,24},{4,28},{1,25},{5,29},{2,26},{6,30},{3,27},{7,31}} | collective-permute-start | bytes 159752 | tf_op jit(solution)/shard_map/ppermute | solution.py:377
  73.8 1.5 collective-permute-start.4
  75.3 14.2 %copy-start.15 = (bf16[192,256]{1,0:T(8,128)(2,1)}, bf16[192,256]{1,0:T(8,128)(2,1)S(1)}, u32[]{:S(2)}) copy-start(bf16[192,256]{1,0:T(8,128)(2,1)S(1)} %collective-permute-done.4.refs_1_) | copy-start | bytes 294916
  75.3 5.1 %collective-permute-start.5 = (bf16[192,256]{1,0:T(8,128)(2,1)}, bf16[192,256]{1,0:T(8,128)(2,1)S(1)}, u32[]{:S(2)}, u32[]{:S(2)}) collective-permute-start(bf16[192,256]{1,0:T(8,128)(2,1)} %get-tuple-element.35), channel_id=1, source_target_pairs={{0,2},{1,3},{2,0},{3,1},{4,6},{5,7},{6,4},{7,5},{8,10},{9,11},{10,... | collective-permute-start | bytes 294920 | tf_op jit(solution)/shard_map/ppermute | solution.py:377
  80.4 9.2 %copy-start.16 = (bf16[192,256]{1,0:T(8,128)(2,1)}, bf16[192,256]{1,0:T(8,128)(2,1)S(1)}, u32[]{:S(2)}) copy-start(bf16[192,256]{1,0:T(8,128)(2,1)S(1)} %collective-permute-done.5.refs_2_) | copy-start | bytes 294916
  80.4 5.3 %collective-permute-start.6 = (bf16[192,256]{1,0:T(8,128)(2,1)}, bf16[192,256]{1,0:T(8,128)(2,1)S(1)}, u32[]{:S(2)}, u32[]{:S(2)}) collective-permute-start(bf16[192,256]{1,0:T(8,128)(2,1)} %get-tuple-element.36), channel_id=1, source_target_pairs={{0,3},{1,2},{2,1},{3,0},{4,7},{5,6},{6,5},{7,4},{8,11},{9,10},{10,... | collective-permute-start | bytes 294920 | tf_op jit(solution)/shard_map/ppermute | solution.py:377
  85.7 3.9 %copy-start.17 = (bf16[192,256]{1,0:T(8,128)(2,1)}, bf16[192,256]{1,0:T(8,128)(2,1)S(1)}, u32[]{:S(2)}) copy-start(bf16[192,256]{1,0:T(8,128)(2,1)S(1)} %collective-permute-done.6.refs_3_) | copy-start | bytes 294916
  85.7 11.1 %collective-permute-start.18 = (bf16[256,2048]{1,0:T(8,128)(2,1)S(1)}, bf16[256,2048]{1,0:T(8,128)(2,1)}, u32[]{:S(2)}, u32[]{:S(2)}) collective-permute-start(bf16[256,2048]{1,0:T(8,128)(2,1)S(1)} %broadcast_select_fusion.5.refs_0_), channel_id=1, source_target_pairs={{8,16},{12,20},{16,8},{20,12},{9,17},{13,21},{17,9},{21,13},{10,18... | collective-permute-start | bytes 3145736 | tf_op jit(solution)/shard_map/ppermute | solution.py:377
  87.3 12.3 %collective-permute-start.20 = (bf16[256,2048]{1,0:T(8,128)(2,1)}, bf16[256,2048]{1,0:T(8,128)(2,1)}, u32[]{:S(2)}, u32[]{:S(2)}) collective-permute-start(bf16[256,2048]{1,0:T(8,128)(2,1)} %collective-permute-done.16.refs_2_), channel_id=1, source_target_pairs={{8,16},{12,20},{16,8},{20,12},{9,17},{13,21},{17,9},{21,13},{10,18... | collective-permute-start | bytes 3145736 | tf_op jit(solution)/shard_map/ppermute | solution.py:377
  95.5 2.6 copy-start.7
  95.5 11.4 %copy-start.6 = (bf16[96,2048]{1,0:T(8,128)(2,1)S(1)}, bf16[96,2048]{1,0:T(8,128)(2,1)}, u32[]{:S(2)}) copy-start(bf16[96,2048]{1,0:T(8,128)(2,1)} %get-tuple-element.38.own_a) | copy-start | bytes 1179652
  95.5 11.4 %collective-permute-start.10 = (bf16[96,2048]{1,0:T(8,128)(2,1)}, bf16[96,2048]{1,0:T(8,128)(2,1)S(1)}, u32[]{:S(2)}, u32[]{:S(2)}) collective-permute-start(bf16[96,2048]{1,0:T(8,128)(2,1)} %get-tuple-element.38.own_a), channel_id=1, source_target_pairs={{0,2},{1,3},{2,0},{3,1},{4,6},{5,7},{6,4},{7,5},{8,10},{9,11},{10,... | collective-permute-start | bytes 1179656 | tf_op jit(solution)/shard_map/ppermute | solution.py:377
  96.7 26.1 %collective-permute-start.26 = (bf16[2048,256]{1,0:T(8,128)(2,1)S(1)}, bf16[2048,256]{1,0:T(8,128)(2,1)S(1)}, u32[]{:S(2)}, u32[]{:S(2)}) collective-permute-start(bf16[2048,256]{1,0:T(8,128)(2,1)S(1)} %broadcast_select_fusion.2), channel_id=1, source_target_pairs={{0,8},{4,12},{8,0},{12,4},{16,24},{20,28},{24,16},{28,20},{1,9},{5... | collective-permute-start | bytes 3145736 | tf_op jit(solution)/shard_map/ppermute | solution.py:377
  96.8 48.6 %collective-permute-start.19 = (bf16[256,2048]{1,0:T(8,128)(2,1)}, bf16[256,2048]{1,0:T(8,128)(2,1)}, u32[]{:S(2)}, u32[]{:S(2)}) collective-permute-start(bf16[256,2048]{1,0:T(8,128)(2,1)} %collective-permute-done.18), channel_id=1, source_target_pairs={{8,0},{12,4},{16,24},{20,28},{9,1},{13,5},{17,25},{21,29},{10,2},{... | collective-permute-start | bytes 3145736 | tf_op jit(solution)/shard_map/ppermute | solution.py:377
  98.1 11.6 %collective-permute-start.12 = (bf16[96,2048]{1,0:T(8,128)(2,1)S(1)}, bf16[96,2048]{1,0:T(8,128)(2,1)S(1)}, u32[]{:S(2)}, u32[]{:S(2)}) collective-permute-start(bf16[96,2048]{1,0:T(8,128)(2,1)S(1)} %copy-done.7), channel_id=1, source_target_pairs={{0,4},{4,0},{8,12},{12,8},{16,20},{20,16},{24,28},{28,24},{1,5},{5... | collective-permute-start | bytes 1179656 | tf_op jit(solution)/shard_map/ppermute | solution.py:377
  99.6 67.8 %collective-permute-start.22 = (bf16[256,2048]{1,0:T(8,128)(2,1)}, bf16[256,2048]{1,0:T(8,128)(2,1)}, u32[]{:S(2)}, u32[]{:S(2)}) collective-permute-start(bf16[256,2048]{1,0:T(8,128)(2,1)} %collective-permute-done.20), channel_id=1, source_target_pairs={{8,0},{12,4},{16,24},{20,28},{9,1},{13,5},{17,25},{21,29},{10,2},{... | collective-permute-start | bytes 3145736 | tf_op jit(solution)/shard_map/ppermute | solution.py:377
  106.9 3.9 %copy-start.8 = (bf16[96,2048]{1,0:T(8,128)(2,1)}, bf16[96,2048]{1,0:T(8,128)(2,1)S(1)}, u32[]{:S(2)}) copy-start(bf16[96,2048]{1,0:T(8,128)(2,1)S(1)} %collective-permute-done.10.x_a) | copy-start | bytes 1179652
  107.9 40.6 %collective-permute-start.11 = (bf16[192,2048]{1,0:T(8,128)(2,1)}, bf16[192,2048]{1,0:T(8,128)(2,1)}, u32[]{:S(2)}, u32[]{:S(2)}) collective-permute-start(bf16[192,2048]{1,0:T(8,128)(2,1)} %pad_maximum_fusion), channel_id=1, source_target_pairs={{0,4},{4,0},{8,12},{12,8},{16,20},{20,16},{24,28},{28,24},{1,5},{5... | collective-permute-start | bytes 2359304 | tf_op jit(solution)/shard_map/ppermute | solution.py:377
  110.8 37.8 %collective-permute-start.13 = (bf16[192,2048]{1,0:T(8,128)(2,1)}, bf16[192,2048]{1,0:T(8,128)(2,1)}, u32[]{:S(2)}, u32[]{:S(2)}) collective-permute-start(bf16[192,2048]{1,0:T(8,128)(2,1)} %pad_maximum_fusion.1), channel_id=1, source_target_pairs={{0,2},{1,3},{2,0},{3,1},{4,6},{5,7},{6,4},{7,5},{8,10},{9,11},{10,... | collective-permute-start | bytes 2359304 | tf_op jit(solution)/shard_map/ppermute | solution.py:377
  122.8 49.5 %collective-permute-start.15 = (bf16[256,2048]{1,0:T(8,128)(2,1)S(1)}, bf16[256,2048]{1,0:T(8,128)(2,1)}, u32[]{:S(2)}, u32[]{:S(2)}) collective-permute-start(bf16[256,2048]{1,0:T(8,128)(2,1)S(1)} %broadcast_select_fusion.5.refs_0_), channel_id=1, source_target_pairs={{0,1},{1,0},{2,3},{3,2},{4,5},{5,4},{6,7},{7,6},{8,9},{9,8},{10,11... | collective-permute-start | bytes 3145736 | tf_op jit(solution)/shard_map/ppermute | solution.py:377
  145.4 3.2 %copy-start.23 = (bf16[2048,256]{1,0:T(8,128)(2,1)S(1)}, bf16[2048,256]{1,0:T(8,128)(2,1)}, u32[]{:S(2)}) copy-start(bf16[2048,256]{1,0:T(8,128)(2,1)} %copy-done.22) | copy-start | bytes 3145732
  145.4 24.4 %collective-permute-start.31 = (bf16[2048,256]{1,0:T(8,128)(2,1)S(1)}, bf16[2048,256]{1,0:T(8,128)(2,1)S(1)}, u32[]{:S(2)}, u32[]{:S(2)}) collective-permute-start(bf16[2048,256]{1,0:T(8,128)(2,1)S(1)} %broadcast_select_fusion.2), channel_id=1, source_target_pairs={{8,16},{12,20},{16,8},{20,12},{9,17},{13,21},{17,9},{21,13},{10,18... | collective-permute-start | bytes 3145736 | tf_op jit(solution)/shard_map/ppermute | solution.py:377
  148.5 23.7 %collective-permute-start.17 = (bf16[256,2048]{1,0:T(8,128)(2,1)}, bf16[256,2048]{1,0:T(8,128)(2,1)}, u32[]{:S(2)}, u32[]{:S(2)}) collective-permute-start(bf16[256,2048]{1,0:T(8,128)(2,1)} %collective-permute-done.16.refs_2_), channel_id=1, source_target_pairs={{0,1},{1,0},{2,3},{3,2},{4,5},{5,4},{6,7},{7,6},{8,9},{9,8},{10,11... | collective-permute-start | bytes 3145736 | tf_op jit(solution)/shard_map/ppermute | solution.py:377
  148.6 21.8 %collective-permute-start.33 = (bf16[2048,256]{1,0:T(8,128)(2,1)S(1)}, bf16[2048,256]{1,0:T(8,128)(2,1)}, u32[]{:S(2)}, u32[]{:S(2)}) collective-permute-start(bf16[2048,256]{1,0:T(8,128)(2,1)S(1)} %copy-done.23), channel_id=1, source_target_pairs={{8,16},{12,20},{16,8},{20,12},{9,17},{13,21},{17,9},{21,13},{10,18... | collective-permute-start | bytes 3145736 | tf_op jit(solution)/shard_map/ppermute | solution.py:377
  167.4 5.4 %collective-permute-start.21 = (bf16[256,2048]{1,0:T(8,128)(2,1)}, bf16[256,2048]{1,0:T(8,128)(2,1)}, u32[]{:S(2)}, u32[]{:S(2)}) collective-permute-start(bf16[256,2048]{1,0:T(8,128)(2,1)} %broadcast_select_fusion.4.refs_4_), channel_id=1, source_target_pairs={{0,1},{1,0},{2,3},{3,2},{4,5},{5,4},{6,7},{7,6},{8,9},{9,8},{10,11... | collective-permute-start | bytes 3145736 | tf_op jit(solution)/shard_map/ppermute | solution.py:377
  169.8 4.5 %collective-permute-start.23 = (bf16[256,2048]{1,0:T(8,128)(2,1)}, bf16[256,2048]{1,0:T(8,128)(2,1)}, u32[]{:S(2)}, u32[]{:S(2)}) collective-permute-start(bf16[256,2048]{1,0:T(8,128)(2,1)} %broadcast_select_fusion.3.refs_6_), channel_id=1, source_target_pairs={{0,1},{1,0},{2,3},{3,2},{4,5},{5,4},{6,7},{7,6},{8,9},{9,8},{10,11... | collective-permute-start | bytes 3145736 | tf_op jit(solution)/shard_map/ppermute | solution.py:377
  170.3 48.9 %collective-permute-start.32 = (bf16[2048,256]{1,0:T(8,128)(2,1)S(1)}, bf16[2048,256]{1,0:T(8,128)(2,1)}, u32[]{:S(2)}, u32[]{:S(2)}) collective-permute-start(bf16[2048,256]{1,0:T(8,128)(2,1)S(1)} %collective-permute-done.31), channel_id=1, source_target_pairs={{8,0},{12,4},{16,24},{20,28},{9,1},{13,5},{17,25},{21,29},{10,2},{... | collective-permute-start | bytes 3145736 | tf_op jit(solution)/shard_map/ppermute | solution.py:377
  172.3 48.3 %collective-permute-start.25 = (bf16[2048,256]{1,0:T(8,128)(2,1)S(1)}, bf16[2048,256]{1,0:T(8,128)(2,1)}, u32[]{:S(2)}, u32[]{:S(2)}) collective-permute-start(bf16[2048,256]{1,0:T(8,128)(2,1)S(1)} %broadcast_select_fusion.2), channel_id=1, source_target_pairs={{0,1},{1,0},{2,3},{3,2},{4,5},{5,4},{6,7},{7,6},{8,9},{9,8},{10,11... | collective-permute-start | bytes 3145736 | tf_op jit(solution)/shard_map/ppermute | solution.py:377
  172.3 48.3 %collective-permute-start.27 = (bf16[2048,256]{1,0:T(8,128)(2,1)}, bf16[2048,256]{1,0:T(8,128)(2,1)}, u32[]{:S(2)}, u32[]{:S(2)}) collective-permute-start(bf16[2048,256]{1,0:T(8,128)(2,1)} %copy-done.22), channel_id=1, source_target_pairs={{0,1},{1,0},{2,3},{3,2},{4,5},{5,4},{6,7},{7,6},{8,9},{9,8},{10,11... | collective-permute-start | bytes 3145736 | tf_op jit(solution)/shard_map/ppermute | solution.py:377
  172.8 87.3 %collective-permute-start.38 = (bf16[2048,256]{1,0:T(8,128)(2,1)}, bf16[2048,256]{1,0:T(8,128)(2,1)S(1)}, u32[]{:S(2)}, u32[]{:S(2)}) collective-permute-start(bf16[2048,256]{1,0:T(8,128)(2,1)} %collective-permute-done.33), channel_id=1, source_target_pairs={{8,0},{12,4},{16,24},{20,28},{9,1},{13,5},{17,25},{21,29},{10,2},{... | collective-permute-start | bytes 3145736 | tf_op jit(solution)/shard_map/ppermute | solution.py:377
  186.2 34.4 %copy-start.24 = (bf16[2048,256]{1,0:T(8,128)(2,1)S(1)}, bf16[2048,256]{1,0:T(8,128)(2,1)}, u32[]{:S(2)}) copy-start(bf16[2048,256]{1,0:T(8,128)(2,1)} %copy-done.22) | copy-start | bytes 3145732
  220.5 10.4 %collective-permute-start.34 = (bf16[2048,256]{1,0:T(8,128)(2,1)S(1)}, bf16[2048,256]{1,0:T(8,128)(2,1)S(1)}, u32[]{:S(2)}, u32[]{:S(2)}) collective-permute-start(bf16[2048,256]{1,0:T(8,128)(2,1)S(1)} %broadcast_select_fusion.1), channel_id=1, source_target_pairs={{0,1},{1,0},{2,3},{3,2},{4,5},{5,4},{6,7},{7,6},{8,9},{9,8},{10,11... | collective-permute-start | bytes 3145736 | tf_op jit(solution)/shard_map/ppermute | solution.py:377
  226.5 4.4 %copy-start.25 = (bf16[768,2048]{1,0:T(8,128)(2,1)S(1)}, bf16[768,2048]{1,0:T(8,128)(2,1)}, u32[]{:S(2)}) copy-start(bf16[768,2048]{1,0:T(8,128)(2,1)} %shard_map.204) | copy-start | bytes 9437188
  227.5 12.9 %collective-permute-start.28 = (bf16[192,1024]{1,0:T(8,128)(2,1)S(1)}, bf16[192,1024]{1,0:T(8,128)(2,1)S(1)}, u32[]{:S(2)}, u32[]{:S(2)}) collective-permute-start(bf16[192,1024]{1,0:T(8,128)(2,1)S(1)} %get-tuple-element.49), channel_id=1, source_target_pairs={{0,6},{1,7},{2,4},{3,5},{4,2},{5,3},{6,0},{7,1},{8,14},{9,15},{10,... | collective-permute-start | bytes 1179656 | tf_op jit(solution)/shard_map/ppermute | solution.py:377
  227.5 20.4 %collective-permute-start.29 = (bf16[192,1024]{1,0:T(8,128)(2,1)S(1)}, bf16[192,1024]{1,0:T(8,128)(2,1)S(1)}, u32[]{:S(2)}, u32[]{:S(2)}) collective-permute-start(bf16[192,1024]{1,0:T(8,128)(2,1)S(1)} %get-tuple-element.48), channel_id=1, source_target_pairs={{0,2},{1,3},{2,0},{3,1},{4,6},{5,7},{6,4},{7,5},{8,10},{9,11},{10,... | collective-permute-start | bytes 1179656 | tf_op jit(solution)/shard_map/ppermute | solution.py:377
  229.5 19.9 %collective-permute-start.30 = (bf16[192,1024]{1,0:T(8,128)(2,1)S(1)}, bf16[192,1024]{1,0:T(8,128)(2,1)S(1)}, u32[]{:S(2)}, u32[]{:S(2)}) collective-permute-start(bf16[192,1024]{1,0:T(8,128)(2,1)S(1)} %get-tuple-element.47), channel_id=1, source_target_pairs={{0,4},{4,0},{8,12},{12,8},{16,20},{20,16},{24,28},{28,24},{1,5},{5... | collective-permute-start | bytes 1179656 | tf_op jit(solution)/shard_map/ppermute | solution.py:377
  233.5 19.6 %collective-permute-start.35 = (bf16[192,512]{1,0:T(8,128)(2,1)S(1)}, bf16[192,512]{1,0:T(8,128)(2,1)S(1)}, u32[]{:S(2)}, u32[]{:S(2)}) collective-permute-start(bf16[192,512]{1,0:T(8,128)(2,1)S(1)} %get-tuple-element.57), channel_id=1, source_target_pairs={{0,6},{1,7},{2,4},{3,5},{4,2},{5,3},{6,0},{7,1},{8,14},{9,15},{10,... | collective-permute-start | bytes 589832 | tf_op jit(solution)/shard_map/ppermute | solution.py:377
  240.4 16.5 %copy-start.3 = (bf16[192,1024]{1,0:T(8,128)(2,1)}, bf16[192,1024]{1,0:T(8,128)(2,1)S(1)}, u32[]{:S(2)}) copy-start(bf16[192,1024]{1,0:T(8,128)(2,1)S(1)} %collective-permute-done.28.refs_1_) | copy-start | bytes 1179652
  240.4 15.9 %collective-permute-start.36 = (bf16[192,512]{1,0:T(8,128)(2,1)S(1)}, bf16[192,512]{1,0:T(8,128)(2,1)}, u32[]{:S(2)}, u32[]{:S(2)}) collective-permute-start(bf16[192,512]{1,0:T(8,128)(2,1)S(1)} %get-tuple-element.56), channel_id=1, source_target_pairs={{0,2},{1,3},{2,0},{3,1},{4,6},{5,7},{6,4},{7,5},{8,10},{9,11},{10,... | collective-permute-start | bytes 589832 | tf_op jit(solution)/shard_map/ppermute | solution.py:377
  247.9 9.0 %copy-start.4 = (bf16[192,1024]{1,0:T(8,128)(2,1)}, bf16[192,1024]{1,0:T(8,128)(2,1)S(1)}, u32[]{:S(2)}) copy-start(bf16[192,1024]{1,0:T(8,128)(2,1)S(1)} %collective-permute-done.29.refs_2_) | copy-start | bytes 1179652
  247.9 9.0 %collective-permute-start.37 = (bf16[192,512]{1,0:T(8,128)(2,1)S(1)}, bf16[192,512]{1,0:T(8,128)(2,1)}, u32[]{:S(2)}, u32[]{:S(2)}) collective-permute-start(bf16[192,512]{1,0:T(8,128)(2,1)S(1)} %get-tuple-element.55), channel_id=1, source_target_pairs={{0,4},{4,0},{8,12},{12,8},{16,20},{20,16},{24,28},{28,24},{1,5},{5... | collective-permute-start | bytes 589832 | tf_op jit(solution)/shard_map/ppermute | solution.py:377
  249.4 7.5 %copy-start.5 = (bf16[192,1024]{1,0:T(8,128)(2,1)}, bf16[192,1024]{1,0:T(8,128)(2,1)S(1)}, u32[]{:S(2)}) copy-start(bf16[192,1024]{1,0:T(8,128)(2,1)S(1)} %collective-permute-done.30.refs_3_) | copy-start | bytes 1179652
  253.1 3.8 %copy-start.11 = (bf16[192,512]{1,0:T(8,128)(2,1)}, bf16[192,512]{1,0:T(8,128)(2,1)S(1)}, u32[]{:S(2)}) copy-start(bf16[192,512]{1,0:T(8,128)(2,1)S(1)} %collective-permute-done.35.refs_5_) | copy-start | bytes 589828
  260.1 2.9 %copy-start.26 = (bf16[768,2048]{1,0:T(8,128)(2,1)S(1)}, bf16[768,2048]{1,0:T(8,128)(2,1)}, u32[]{:S(2)}) copy-start(bf16[768,2048]{1,0:T(8,128)(2,1)} %shard_map.204) | copy-start | bytes 9437188
  260.2 2.7 collective-permute-start.39
  265.5 8.7 %collective-permute-start.40 = (bf16[192,512]{1,0:T(8,128)(2,1)S(1)}, bf16[192,512]{1,0:T(8,128)(2,1)S(1)}, u32[]{:S(2)}, u32[]{:S(2)}) collective-permute-start(bf16[192,512]{1,0:T(8,128)(2,1)S(1)} %get-tuple-element.53), channel_id=1, source_target_pairs={{0,6},{1,7},{2,4},{3,5},{4,2},{5,3},{6,0},{7,1},{8,14},{9,15},{10,... | collective-permute-start | bytes 589832 | tf_op jit(solution)/shard_map/ppermute | solution.py:377
  267.5 9.4 %collective-permute-start.41 = (bf16[192,512]{1,0:T(8,128)(2,1)S(1)}, bf16[192,512]{1,0:T(8,128)(2,1)S(1)}, u32[]{:S(2)}, u32[]{:S(2)}) collective-permute-start(bf16[192,512]{1,0:T(8,128)(2,1)S(1)} %get-tuple-element.52), channel_id=1, source_target_pairs={{0,2},{1,3},{2,0},{3,1},{4,6},{5,7},{6,4},{7,5},{8,10},{9,11},{10,... | collective-permute-start | bytes 589832 | tf_op jit(solution)/shard_map/ppermute | solution.py:377
  267.8 9.8 %collective-permute-start.42 = (bf16[192,512]{1,0:T(8,128)(2,1)S(1)}, bf16[192,512]{1,0:T(8,128)(2,1)S(1)}, u32[]{:S(2)}, u32[]{:S(2)}) collective-permute-start(bf16[192,512]{1,0:T(8,128)(2,1)S(1)} %get-tuple-element.51), channel_id=1, source_target_pairs={{0,4},{4,0},{8,12},{12,8},{16,20},{20,16},{24,28},{28,24},{1,5},{5... | collective-permute-start | bytes 589832 | tf_op jit(solution)/shard_map/ppermute | solution.py:377
  274.2 3.3 %copy-start.12 = (bf16[192,512]{1,0:T(8,128)(2,1)}, bf16[192,512]{1,0:T(8,128)(2,1)S(1)}, u32[]{:S(2)}) copy-start(bf16[192,512]{1,0:T(8,128)(2,1)S(1)} %collective-permute-done.40.refs_1_) | copy-start | bytes 589828
  (6 other events, 5.1 us)
where the time goes:
time: 282 us; the launch traced here: 281 us
  waiting for transfers between devices  147 us (52%)
  starting transfers between devices  65.7 us (23%)
  Pallas kernels  35.6 us (13%)
  local copies, waits for them, and re-layouts  12.7 us (5%)
  other arithmetic  9.68 us (3%)
  matrix products  9.5 us (3%)
    ppermute x43, waiting for transfers between devices, exchange(): lax.ppermute(array, axis, [(i, j) for i, j in pairs if j is not None and...  147 us
    ppermute x43, starting transfers between devices, exchange(): lax.ppermute(array, axis, [(i, j) for i, j in pairs if j is not None and...  65.7 us
    pallas_call x1, Pallas kernels, up_project(): return run(at, *pieces, *blocks)  12 us
    dot_general x3, matrix products, down(): jnp.dot(hidden, jnp.concatenate(blocks, axis=1), preferred_element_type=F32)  9.5 us
  transfers between devices with their start and end apart: 43, of which 22 were waited for; matrix products, arithmetic and copies ran while one was open for 9% of the time, Pallas kernels for 12%

commit v1 on v0

--- a/solution.py
+++ b/solution.py
@@ -257,71 +257,93 @@
 
 
 def middle_kernel(stream, gain, wide, narrow, *refs):
-    *inputs, middle, first, second = refs
+    *inputs, middle, normed, turned = refs
     count = (len(inputs) + 1) // 2
     pieces, weights = inputs[:count], inputs[count:]
-    lanes = wide.shape[0]
-    own = pieces[0][...]
-    total = jnp.dot(own[:, :lanes], wide[...], preferred_element_type=F32)
-    total = total + jnp.dot(own[:, lanes:], narrow[...], preferred_element_type=F32)
-    for piece, weight in zip(pieces[1:], weights):
-        total = total + jnp.dot(piece[...], weight[...], preferred_element_type=F32)
+    half = stream.shape[0] // 2
+    total = jnp.dot(
+        jnp.concatenate([piece[...] for piece in pieces], axis=1),
+        jnp.concatenate([weight[...] for weight in (wide, narrow, *weights)], axis=0),
+        preferred_element_type=F32,
+    )
     rounded = (stream[...].astype(F32) + total).astype(BF16)
     middle[...] = rounded
     x = rounded.astype(F32)
     scale = lax.rsqrt(jnp.mean(x * x, axis=-1, keepdims=True) + norm_eps)
-    normed = (x * scale * gain[...].astype(F32)).astype(BF16)
-    half = normed.shape[0] // 2
-    first[...] = normed[:half]
-    second[...] = normed[half:]
-
-
-def up_kernel(at, own_a, own_b, x_a, y_a, y_b, x_b, *refs):
-    *blocks, out, x = refs
+    result = (x * scale * gain[...].astype(F32)).astype(BF16)
+    normed[...] = result
+    turned[0:half, :] = result[half:]
+    turned[half:, :] = result[:half]
+
+
+def up_kernel(at, *refs):
+    pieces, blocks, (partial, rest, x, ordered_x) = refs[:5], refs[5:-4], refs[-4:]
     depth = blocks[0].shape[0]
-    rows = own_a.shape[0]
+
+    def at_block(n):
+        return pl.ds(pl.multiple_of(at[n] * depth, 128), depth)
 
     @pl.when(pl.program_id(0) == 0)
     def _():
-        for n, piece in enumerate(
-            (own_a, own_b, x_a, x_b.at[:rows], y_a.at[:rows], y_b, y_a.at[rows:], x_b.at[rows:])
-        ):
-            x[n * rows : (n + 1) * rows, :] = piece[...]
-
-    total = None
-    for n, block in enumerate(blocks):
-        columns = pl.ds(pl.multiple_of(at[n] * depth, 128), depth)
-        part = jnp.dot(x[:, columns], block[...], preferred_element_type=F32)
-        total = part if total is None else total + part
-    total = jnp.maximum(total, 0.0)
-    out[...] = (total * total).astype(BF16)
-
-
-def up_project(at, pieces, blocks):
+        own, by_x, by_y, low, high = pieces
+        rows, half = own.shape[0], low.shape[0]
+        x[0:rows, :] = own[...]
+        x[rows : 2 * rows, :] = by_x[...]
+        x[2 * rows : 2 * rows + half, :] = by_y[half:rows, :]
+        x[2 * rows + half : 3 * rows, :] = by_y[0:half, :]
+        x[3 * rows : 3 * rows + half, :] = low[...]
+        x[3 * rows + half : 4 * rows, :] = high[...]
+        for n in range(rest.shape[1] // depth):
+            rest[:, n * depth : (n + 1) * depth] = x[:, at_block(len(blocks) + n)]
+
+        for n in range(len(blocks)):
+            ordered_x[:, n * depth : (n + 1) * depth] = x[:, at_block(n)]
+
+    weight = jnp.concatenate([block[...] for block in blocks], axis=0)
+    partial[...] = jnp.dot(ordered_x[...], weight, preferred_element_type=F32)
+
+
+def up_most(at, pieces, blocks):
     width = blocks[0].shape[1]
     rows, depth = sum(p.shape[0] for p in pieces), pieces[0].shape[1]
+    rest = depth - len(blocks) * blocks[0].shape[0]
     tile = 512
     run = pl.pallas_call(
         up_kernel,
-        out_shape=jax.ShapeDtypeStruct((rows, width), BF16),
+        out_shape=(
+            jax.ShapeDtypeStruct((rows, width), F32),
+            jax.ShapeDtypeStruct((rows, rest), BF16),
+        ),
         grid_spec=pltpu.PrefetchScalarGridSpec(
             num_scalar_prefetch=1,
             grid=(width // tile,),
             in_specs=[pl.BlockSpec(p.shape, lambda n, a: (0, 0)) for p in pieces]
             + [pl.BlockSpec((b.shape[0], tile), lambda n, a: (0, n)) for b in blocks],
-            out_specs=pl.BlockSpec((rows, tile), lambda n, a: (0, n)),
-            scratch_shapes=[pltpu.VMEM((rows, depth), BF16)],
+            out_specs=(
+                pl.BlockSpec((rows, tile), lambda n, a: (0, n)),
+                pl.BlockSpec((rows, rest), lambda n, a: (0, 0)),
+            ),
+            scratch_shapes=[
+                pltpu.VMEM((rows, depth), BF16), pltpu.VMEM((rows, depth - rest), BF16)
+            ],
         ),
         cost_estimate=pl.CostEstimate(
-            flops=2 * rows * depth * width,
-            bytes_accessed=2 * (rows * depth + depth * width + rows * width),
+            flops=2 * rows * (depth - rest) * width,
+            bytes_accessed=2 * (rows * depth + depth * width + 2 * rows * width),
             transcendentals=0,
         ),
     )
     return run(at, *pieces, *blocks)
 
 
-SIDE = 256
+def up_rest(partial, x, blocks):
+    total = partial + jnp.dot(
+        x, jnp.concatenate(blocks, axis=0), preferred_element_type=F32
+    )
+    return jnp.square(jax.nn.relu(total)).astype(BF16)
+
+
+UNIT = 128
 
 
 def place_kernel(at, middle, *refs):
@@ -329,14 +351,30 @@
     place = 0
     for n in range(0, len(parts), 4):
         group = parts[n : n + 4]
-        for side in range(group[0].shape[1] // SIDE):
-            here = slice(side * SIDE, (side + 1) * SIDE)
-            columns = pl.ds(pl.multiple_of(at[place] * SIDE, 128), SIDE)
+        side = min(group[0].shape[1] // 2, 2 * UNIT)
+        for m in range(group[0].shape[1] // side):
+            here = slice(m * side, (m + 1) * side)
+            columns = pl.ds(pl.multiple_of(at[place] * UNIT, UNIT), side)
             place += 1
             total = middle[:, columns].astype(F32)
             for part in group:
                 total = total + part[:, here].astype(F32)
             out[:, columns] = total.astype(BF16)
+
+
+def pause_kernel(seen, out):
+    out[...] = seen[0:8, :].astype(F32)
+
+
+def hold(seen):
+    run = pl.pallas_call(
+        pause_kernel,
+        out_shape=jax.ShapeDtypeStruct((8, seen.shape[1]), F32),
+        in_specs=[VM],
+        out_specs=VM,
+        compiler_params=pltpu.CompilerParams(has_side_effects=True),
+    )
+    return run(seen)
 
 
 def last_kernel(at, out_in, middle, *refs):
@@ -349,20 +387,21 @@
 
 def place_last(at, out, middle, parts):
     rows = middle.shape[0]
-    skip = middle.shape[1] // SIDE - parts[0].shape[1] // SIDE
+    side = parts[0].shape[1] // 2
+    skip = at.shape[0] - 2
 
     def column(n, a):
-        return (0, a[skip + n])
+        return (0, a[skip + n] // (side // UNIT))
 
     run = pl.pallas_call(
         last_kernel,
         out_shape=jax.ShapeDtypeStruct(middle.shape, BF16),
         grid_spec=pltpu.PrefetchScalarGridSpec(
             num_scalar_prefetch=1,
-            grid=(parts[0].shape[1] // SIDE,),
-            in_specs=[pl.BlockSpec(memory_space=pl.ANY), pl.BlockSpec((rows, SIDE), column)]
-            + [pl.BlockSpec((rows, SIDE), lambda n, a: (0, n))] * len(parts),
-            out_specs=pl.BlockSpec((rows, SIDE), column),
+            grid=(2,),
+            in_specs=[pl.BlockSpec(memory_space=pl.ANY), pl.BlockSpec((rows, side), column)]
+            + [pl.BlockSpec((rows, side), lambda n, a: (0, n))] * len(parts),
+            out_specs=pl.BlockSpec((rows, side), column),
         ),
         input_output_aliases={1: 0},
         cost_estimate=pl.CostEstimate(
@@ -425,11 +464,10 @@
         low = m & (m - 1)
         weights.append(exchange(weights[low], "tp", tp, lambda i: i ^ (m ^ low)))
         pieces.append(exchange(mixed[m], "tp", tp, lambda i: i ^ m))
-    sds = jax.ShapeDtypeStruct
     rows, depth = stream_in.shape
     return call(
         middle_kernel,
-        (sds((rows, depth), BF16),) + (sds((rows // 2, depth), BF16),) * 2,
+        (jax.ShapeDtypeStruct((rows, depth), BF16),) * 3,
         3 + 2 * tp,
         2 * rows * mixed[0].shape[1] * tp * depth,
         8 * stream_in.size,
@@ -480,7 +518,8 @@
     order = jnp.stack([s * 2 + c for s in slots for c in (core, 1 - core)]).astype(jnp.int32)
 
     def own_block(block, after=()):
-        return jnp.where(y == core, block, swap_y_core(block, after))
+        swapped = swap_y_core(block, after)
+        return jnp.where(y == core, block, swapped)
 
     up_own = own_block(up_weight)
     up_near, up_cross = ends(up_own), middles(up_own)
@@ -494,33 +533,34 @@
     down_cross = middles(tie(down_own, up_near))
     up_last = outwards(up_in)
 
-    middle, first, second = to_middle(mixed, stream_in, output_wide, output_narrow, norm_gain, tp)
-
-    x_a, y_b = by_x(first), by_y(second)
-    down_in = middles(tie(down_near, y_b))
-    y_a = by_y(jnp.concatenate([first, x_a], axis=0))
-    x_b = by_x(jnp.concatenate([second, y_b], axis=0))
-    there = (y_a, x_b)
+    middle, normed, turned = to_middle(
+        mixed, stream_in, output_wide, output_narrow, norm_gain, tp
+    )
+
+    half = normed.shape[0] // 2
+    x_rows, y_rows = by_x(normed), by_y(turned)
+    down_in = middles(down_near)
+    d_low, d_high = by_y(x_rows[:half]), by_x(y_rows[:half])
 
     down_out = outwards(down_cross)
-    up_far = jnp.where(at_end, up_out, up_in)
-    up_final = jnp.where(at_end, tie(up_last, *there), up_cross)
+    up_blocks = both_cores(up_own) + both_cores(up_near)
+    up_far = jnp.where(at_end, tie(up_out, up_blocks[-1]), up_in)
+    up_blocks += both_cores(up_far)
+    down_first = both_cores(down_own) + both_cores(down_near)
+    partial, rest = up_most(order, [normed, x_rows, y_rows, d_low, d_high], up_blocks)
+    up_final = jnp.where(at_end, tie(up_last, partial), up_cross)
     down_last = outwards(tie(down_in, up_final))
-
-    blocks = []
-    for slot in (up_own, up_near, up_far, up_final):
-        blocks += both_cores(slot)
-    hidden = up_project(order, [first, second, x_a, y_a, y_b, x_b], blocks)
-
-    def down(group):
-        blocks = []
-        for d in group:
-            blocks += both_cores(d)
+    hidden = up_rest(partial, rest, both_cores(up_final))
+
+    parts = {}
+
+    def down(n, blocks):
         part = jnp.dot(
             hidden, jnp.concatenate(blocks, axis=1), preferred_element_type=F32
         ).astype(BF16)
         rows = part.shape[0] // 4
         keep, to_x, to_y, across = (part[m * rows : (m + 1) * rows] for m in range(4))
+        parts[n] = part
         return [
             keep,
             exchange(across, ("sp", "tp"), sp * tp, lambda i: i ^ tp ^ 2),
@@ -528,18 +568,22 @@
             by_y(to_y),
         ]
 
-    sums = down([down_own, down_near])
-    down_far = jnp.where(at_end, tie(down_out, hidden), down_in)
-    sums += down([down_far])
+    sums = down(0, down_first)
+    down_far = jnp.where(at_end, tie(down_out, parts[0]), down_in)
+    sums += down(1, both_cores(down_far))
+    pause = hold(stream_in[:16, :128])
+    ends_final = both_cores(tie(down_last, parts[1], pause))
+    middles_final = both_cores(down_cross)
+    sums += down(2, [jnp.where(at_end, a, b) for a, b in zip(ends_final, middles_final)])
+    units = 2 * order
     out = scalar_call(
         place_kernel,
         jax.ShapeDtypeStruct(middle.shape, BF16),
-        1 + len(sums),
+        1 + len(sums[:-4]),
         middle.size,
         8 * middle.size,
-    )(order, middle, *sums)
-    down_final = jnp.where(at_end, tie(down_last, out), down_cross)
-    return place_last(order, out, middle, down([down_final]))
+    )(units, middle, *sums[:-4])
+    return place_last(units, out, middle, sums[-4:])
 
 
 def group_feed_forward(middle, normed):
@@ -567,8 +611,7 @@
             tensors, stream_in, output_wide, output_narrow, norm_gain, up_weight, down_weight, sp, tp
         )
     mixed, _ = retention(tensors, sp, tp)
-    middle, first, second = to_middle(mixed, stream_in, output_wide, output_narrow, norm_gain, tp)
-    normed = jnp.concatenate([first, second], axis=0)
+    middle, normed, _ = to_middle(mixed, stream_in, output_wide, output_narrow, norm_gain, tp)
     return group_feed_forward(middle, normed)(up_weight, down_weight)
 
 

time: 282 us -> 242 us (0.86)
  waiting for transfers between devices: 147 us -> 98.5 us
  matrix products: 9.5 us -> 17.1 us
  local copies, waits for them, and re-layouts: 12.7 us -> 16.2 us
    ppermute x43 -> x44, waiting for transfers between devices: 147 us -> 98.5 us  [exchange(): lax.ppermute(array, axis, [(i, j) for i, j in pairs if j is not None and...]
    dot_general x0 -> x1, matrix products: none -> 4.92 us  [up_rest(): jnp.dot(x, jnp.concatenate(blocks, axis=0), preferred_element_type=F32)]
    slice x0 -> x3, local copies, waits for them, and re-layouts: none -> 3.32 us  [the longest x2 2.04 us: plane_layer(): d_low, d_high = (by_y(x_rows[:half]), by_x(y_rows[:half]))]
    ppermute x43 -> x44, starting transfers between devices: 65.7 us -> 63.7 us  [exchange(): lax.ppermute(array, axis, [(i, j) for i, j in pairs if j is not None and...]
    select_n x6 -> x7, other arithmetic: 7.61 us -> 8.75 us  [the longest x2 2.51 us: own_block(): return jnp.where(y == core, block, swapped)]
    pallas_call x2 -> x3, Pallas kernels: 16.8 us -> 17.5 us  [the longest x1 11.2 us: up_most(): return run(at, *pieces, *blocks)]
  transfers between devices with their start and end apart: 43 -> 44, of which waited for: 22 -> 18; matrix products, arithmetic and copies ran while one was open for 9% -> 16% of each run, Pallas kernels for 12% -> 14%
where the time goes in v1:
time: 242 us; the launch traced here: 241 us
  waiting for transfers between devices  98.5 us (41%)
  starting transfers between devices  63.7 us (26%)
  Pallas kernels  36.2 us (15%)
  matrix products  17.1 us (7%)
  local copies, waits for them, and re-layouts  16.2 us (7%)
  other arithmetic  9.23 us (4%)
    ppermute x44, waiting for transfers between devices, exchange(): lax.ppermute(array, axis, [(i, j) for i, j in pairs if j is not None and...  98.5 us
    ppermute x44, starting transfers between devices, exchange(): lax.ppermute(array, axis, [(i, j) for i, j in pairs if j is not None and...  63.7 us
    dot_general x3, matrix products, down(): jnp.dot(hidden, jnp.concatenate(blocks, axis=1), preferred_element_type=F32)  12.2 us
    pallas_call x1, Pallas kernels, up_most(): return run(at, *pieces, *blocks)  11.2 us
    unnamed x49, local copies, waits for them, and re-layouts  5.32 us
    pallas_call x1, Pallas kernels, to_middle(): call(middle_kernel, (jax.ShapeDtypeStruct((rows, depth), BF16),) * 3, 3 +...  5.01 us
    pallas_call x1, Pallas kernels, retention(): call(local_kernel, (sds((length, lanes), F32),) * 2 + (sds((length, lanes...  4.95 us
    dot_general x1, matrix products, up_rest(): jnp.dot(x, jnp.concatenate(blocks, axis=0), preferred_element_type=F32)  4.92 us
  transfers between devices with their start and end apart: 44, of which 18 were waited for; matrix products, arithmetic and copies ran while one was open for 16% of the time, Pallas kernels for 14%

profile of v1, /device:TPU:0, one launch (start us, length us, event | category | flops | bytes accessed | tf_op | source)
XLA Modules:
  0.0 241.3 jit_solution(5090958540661967780)
XLA Ops:
  0.7 1.9 constant_dynamic-update-slice_fusion.1
  2.6 1.9 constant_dynamic-update-slice_fusion
  4.5 3.0 %collective-permute-start.8 = (bf16[256,2048]{1,0:T(8,128)(2,1)}, bf16[256,2048]{1,0:T(8,128)(2,1)}, u32[]{:S(2)}, u32[]{:S(2)}) collective-permute-start(bf16[256,2048]{1,0:T(8,128)(2,1)} %constant_dynamic-update-slice_fusion), channel_id=1, source_target_pairs={{0,2},{1,3},{2,0},{3,1},{4,6},{5,7},{6,4},{7,5},{8,10},{9,11},{10,... | collective-permute-start | bytes 3145736 | tf_op jit(solution)/shard_map/ppermute | solution.py:416
  7.5 1.4 broadcast_select_fusion.6.refs_5_
  8.9 1.6 collective-permute-start.16
  11.3 1.3 dynamic-slice_bitcast_fusion.rows
  12.6 3.3 %shard_map.199 = (bf16[208,128]{1,0:T(8,128)(2,1)}, f32[768,8]{1,0:T(8,128)}, f32[8,768]{1,0:T(8,128)}) custom-call(bf16[768,128]{1,0:T(8,128)(2,1)} %kw.3, bf16[768,128]{1,0:T(8,128)(2,1)} %vw.3, bf16[768,128]{1,0:T(8,128)(2,1)} %kn.3, bf16[768,128]{1,0:T(8,128)(2,1)} %vn.3, f32[1,768]{1,0:T(1,128)} %dw.1, f32[2,768]{1,0:T(2,128)} %dn.1, ...), custom_call_target="tpu_custom_call" | custom-call | flops 50331648 | bytes 2359296 | tf_op jit(solution)/shard_map/pallas_call | solution.py:428
  15.9 10.5 %collective-permute-start = (bf16[208,128]{1,0:T(8,128)(2,1)}, bf16[208,128]{1,0:T(8,128)(2,1)S(1)}, u32[]{:S(2)}, u32[]{:S(2)}) collective-permute-start(bf16[208,128]{1,0:T(8,128)(2,1)} %get-tuple-element.28.own), channel_id=1, source_target_pairs={{0,4},{4,0},{8,12},{12,8},{16,20},{20,16},{24,28},{28,24},{1,5},{5... | collective-permute-start | bytes 159752 | tf_op jit(solution)/shard_map/ppermute | solution.py:416
  27.1 1.8 collective-permute-done.other
  29.5 1.5 shard_map.201
  31.0 6.1 %collective-permute-start.1 = (bf16[208,128]{1,0:T(8,128)(2,1)}, bf16[208,128]{1,0:T(8,128)(2,1)S(1)}, u32[]{:S(2)}, u32[]{:S(2)}) collective-permute-start(bf16[208,128]{1,0:T(8,128)(2,1)} %shard_map.201), channel_id=1, source_target_pairs={{0,8},{4,12},{8,16},{12,20},{16,24},{20,28},{1,9},{5,13},{9,17},{1... | collective-permute-start | bytes 159752 | tf_op jit(solution)/shard_map/ppermute | solution.py:416
  37.1 1.5 collective-permute-start.2
  39.3 3.0 %collective-permute-start.3 = (bf16[208,128]{1,0:T(8,128)(2,1)}, bf16[208,128]{1,0:T(8,128)(2,1)S(1)}, u32[]{:S(2)}, u32[]{:S(2)}) collective-permute-start(bf16[208,128]{1,0:T(8,128)(2,1)} %shard_map.201), channel_id=1, source_target_pairs={{0,24},{4,28},{1,25},{5,29},{2,26},{6,30},{3,27},{7,31}} | collective-permute-start | bytes 159752 | tf_op jit(solution)/shard_map/ppermute | solution.py:416
  42.3 4.9 %shard_map.200 = (f32[768,128]{1,0:T(8,128)}, f32[768,128]{1,0:T(8,128)}, bf16[768,128]{1,0:T(8,128)(2,1)}, bf16[768,128]{1,0:T(8,128)(2,1)}) custom-call(bf16[768,128]{1,0:T(8,128)(2,1)} %qw.1, bf16[768,128]{1,0:T(8,128)(2,1)} %kw.3, bf16[768,128]{1,0:T(8,128)(2,1)} %vw.3, bf16[768,128]{1,0:T(8,128)(2,1)} %qn.1, bf16[768,128]{1,0:T(8,128)(2,1)} %kn.3, ...), custom_call_target="tpu_custom_call" | custom-call | flops 603979776 | bytes 3932160 | tf_op jit(solution)/shard_map/pallas_call | solution.py:435
  47.9 3.1 %shard_map.202 = (bf16[192,256]{1,0:T(8,128)(2,1)}, bf16[192,256]{1,0:T(8,128)(2,1)}, bf16[192,256]{1,0:T(8,128)(2,1)}, bf16[192,256]{1,0:T(8,128)(2,1)}) custom-call(s32[5]{0:T(128)} %stack.59.late, bf16[208,128]{1,0:T(8,128)(2,1)} %get-tuple-element.28.own, bf16[208,128]{1,0:T(8,128)(2,1)} %copy-done.5, f32[768,128]{1,0:T(8,128)} %get-tuple-element.31.ow, ...), custom_call_target="tpu_custom_call" | custom-call | flops 50331648 | bytes 2359296 | tf_op jit(solution)/shard_map/pallas_call | solution.py:449
  51.0 1.6 collective-permute-start.5
  52.6 1.2 collective-permute-start.6
  53.8 3.2 %collective-permute-done.5.refs_2_ = bf16[192,256]{1,0:T(8,128)(2,1)S(1)} collective-permute-done((bf16[192,256]{1,0:T(8,128)(2,1)}, bf16[192,256]{1,0:T(8,128)(2,1)S(1)}, u32[]{:S(2)}, u32[]{:S(2)}) %collective-permute-start.5) | collective-permute-done | bytes 98336 | tf_op jit(solution)/shard_map/ppermute | solution.py:416
  57.6 1.3 collective-permute-start.19
  58.9 1.6 collective-permute-start.20
  61.1 1.6 collective-permute-start.24
  62.8 2.8 %collective-permute-start.15 = (bf16[256,2048]{1,0:T(8,128)(2,1)S(1)}, bf16[256,2048]{1,0:T(8,128)(2,1)}, u32[]{:S(2)}, u32[]{:S(2)}) collective-permute-start(bf16[256,2048]{1,0:T(8,128)(2,1)S(1)} %broadcast_select_fusion.6.refs_5_), channel_id=1, source_target_pairs={{0,1},{1,0},{2,3},{3,2},{4,5},{5,4},{6,7},{7,6},{8,9},{9,8},{10,11... | collective-permute-start | bytes 3145736 | tf_op jit(solution)/shard_map/ppermute | solution.py:416
  65.6 5.0 %shard_map.203 = (bf16[192,2048]{1,0:T(8,128)(2,1)}, bf16[192,2048]{1,0:T(8,128)(2,1)}, bf16[192,2048]{1,0:T(8,128)(2,1)}) custom-call(bf16[192,2048]{1,0:T(8,128)(2,1)} %stream.1, bf16[1,2048]{1,0:T(2,128)(2,1)} %broadcast_in_dim.3.gain, bf16[128,2048]{1,0:T(8,128)(2,1)} %wide.1, bf16[128,2048]{1,0:T(8,128)(2,1)} %narrow.1, ...), custom_call_target="tpu_custom_call" | custom-call | flops 805306368 | bytes 3145728 | tf_op jit(solution)/shard_map/pallas_call | solution.py:468
  70.6 1.6 collective-permute-start.10
  72.2 12.9 %collective-permute-done.19 = bf16[256,2048]{1,0:T(8,128)(2,1)} collective-permute-done((bf16[256,2048]{1,0:T(8,128)(2,1)S(1)}, bf16[256,2048]{1,0:T(8,128)(2,1)}, u32[]{:S(2)}, u32[]{:S(2)}) %collective-permute-start.19) | collective-permute-done | bytes 1048608 | tf_op jit(solution)/shard_map/ppermute | solution.py:416
  85.1 2.4 collective-permute-start.11
  87.5 2.3 broadcast_select_fusion.5.refs_9_
  90.5 1.3 collective-permute-start.22
  92.5 1.0 slice.60
  93.5 11.5 %collective-permute-done.11.refs_2_ = bf16[192,2048]{1,0:T(8,128)(2,1)} collective-permute-done((bf16[192,2048]{1,0:T(8,128)(2,1)}, bf16[192,2048]{1,0:T(8,128)(2,1)}, u32[]{:S(2)}, u32[]{:S(2)}) %collective-permute-start.11) | collective-permute-done | bytes 786464 | tf_op jit(solution)/shard_map/ppermute | solution.py:416
  105.1 1.7 collective-permute-start.12
  106.8 1.0 slice.61
  107.8 1.6 collective-permute-start.13
  109.4 1.1 broadcast_select_fusion.3
  110.5 4.6 %collective-permute-done.12.refs_3_ = bf16[96,2048]{1,0:T(8,128)(2,1)S(1)} collective-permute-done((bf16[96,2048]{1,0:T(8,128)(2,1)S(1)}, bf16[96,2048]{1,0:T(8,128)(2,1)S(1)}, u32[]{:S(2)}, u32[]{:S(2)}) %collective-permute-start.12) | collective-permute-done | bytes 393248 | tf_op jit(solution)/shard_map/ppermute | solution.py:416
  115.8 1.6 collective-permute-done.13.refs_4_
  118.1 11.2 %shard_map.204 = (f32[768,2048]{1,0:T(8,128)}, bf16[768,512]{1,0:T(8,128)(2,1)}) custom-call(s32[8]{0:T(128)} %stack.53.at, bf16[192,2048]{1,0:T(8,128)(2,1)} %get-tuple-element.40.refs_0_, bf16[192,2048]{1,0:T(8,128)(2,1)} %collective-permute-done.10.refs_1_, bf16[192,2048]{1,0:T(8,128)(2,1)} %collective-permute-done.11.refs_2_, ...), custom_call_target="tpu_custom_call" | custom-call | flops 4831838208 | bytes 17825792 | tf_op jit(solution)/shard_map/pallas_call | solution.py:336
  129.4 1.3 broadcast_select_fusion.4
  131.3 10.0 %collective-permute-done.26 = bf16[2048,256]{1,0:T(8,128)(2,1)} collective-permute-done((bf16[2048,256]{1,0:T(8,128)(2,1)}, bf16[2048,256]{1,0:T(8,128)(2,1)}, u32[]{:S(2)}, u32[]{:S(2)}) %collective-permute-start.26) | collective-permute-done | bytes 1048608 | tf_op jit(solution)/shard_map/ppermute | solution.py:416
  141.3 1.7 collective-permute-start.33
  143.0 1.5 collective-permute-start.32
  144.4 4.9 %multiply_convert_fusion = bf16[768,2048]{1,0:T(8,128)(2,1)S(1)} fusion(f32[768,2048]{1,0:T(8,128)} %get-tuple-element.43, bf16[768,512]{1,0:T(8,128)(2,1)} %get-tuple-element.44, bf16[256,2048]{1,0:T(8,128)(2,1)S(1)} %collective-permute-done.23, bf16[256,2048]{1,0:T(8,128)(2,1)S(1)} %broadcast_select_fusion.4), kind=kOutput, calls=%fused_computation | convolution fusion | flops 1621098496 | bytes 12320768 | tf_op jit(solution)/shard_map/dot_general | solution.py:340
  149.4 6.1 %fusion.19 = bf16[768,1024]{1,0:T(8,128)(2,1)S(1)} fusion(bf16[768,2048]{1,0:T(8,128)(2,1)S(1)} %multiply_convert_fusion, bf16[2048,256]{1,0:T(8,128)(2,1)S(1)} %collective-permute-done.27, bf16[2048,256]{1,0:T(8,128)(2,1)} %collective-permute-done.26, bf16[2048,256]{1,0:T(8,128)(2,1)S(1)} %collective-permute-done.25, ...), kind=kOutput, calls=%fused_computation.20 | convolution fusion | flops 3238789120 | bytes 8912896 | tf_op jit(solution)/shard_map/dot_general | solution.py:558
  155.5 14.9 %collective-permute-done.32 = bf16[2048,256]{1,0:T(8,128)(2,1)S(1)} collective-permute-done((bf16[2048,256]{1,0:T(8,128)(2,1)S(1)}, bf16[2048,256]{1,0:T(8,128)(2,1)S(1)}, u32[]{:S(2)}, u32[]{:S(2)}) %collective-permute-start.32) | collective-permute-done | bytes 1048608 | tf_op jit(solution)/shard_map/ppermute | solution.py:416
  170.4 1.1 broadcast_select_fusion.2
  171.6 1.3 collective-permute-start.38
  172.9 1.3 slice.55.seen
  174.1 1.3 shard_map.206
  175.9 4.3 %fusion.25 = bf16[768,512]{1,0:T(8,128)(2,1)S(1)} fusion(bf16[768,2048]{1,0:T(8,128)(2,1)} %copy-done.22, bf16[2048,256]{1,0:T(8,128)(2,1)} %collective-permute-done.34, bf16[2048,256]{1,0:T(8,128)(2,1)} %broadcast_select_fusion.2), kind=kOutput, calls=%fused_computation.22 | convolution fusion | flops 1615200256 | bytes 6029312 | tf_op jit(solution)/shard_map/dot_general | solution.py:558
  180.2 19.1 %collective-permute-done.38 = bf16[2048,256]{1,0:T(8,128)(2,1)} collective-permute-done((bf16[2048,256]{1,0:T(8,128)(2,1)}, bf16[2048,256]{1,0:T(8,128)(2,1)}, u32[]{:S(2)}, u32[]{:S(2)}) %collective-permute-start.38) | collective-permute-done | bytes 1048608 | tf_op jit(solution)/shard_map/ppermute | solution.py:416
  200.2 2.2 collective-permute-start.28
  204.5 1.3 broadcast_select_fusion.1
  205.8 2.3 collective-permute-start.35
  208.8 1.8 fusion.22
  211.3 1.9 collective-permute-done.28.refs_1_
  213.2 1.3 collective-permute-start.37
  214.4 7.0 %collective-permute-done.29.refs_2_ = bf16[192,1024]{1,0:T(8,128)(2,1)S(1)} collective-permute-done((bf16[192,1024]{1,0:T(8,128)(2,1)S(1)}, bf16[192,1024]{1,0:T(8,128)(2,1)S(1)}, u32[]{:S(2)}, u32[]{:S(2)}) %collective-permute-start.29) | collective-permute-done | bytes 393248 | tf_op jit(solution)/shard_map/ppermute | solution.py:416
  221.4 1.7 collective-permute-start.41
  223.6 2.2 collective-permute-done.35.refs_5_
  225.8 1.3 collective-permute-start.43
  227.6 2.3 collective-permute-done.36.refs_6_
  230.8 3.2 %shard_map.205.out_in = bf16[192,2048]{1,0:T(8,128)(2,1)} custom-call(s32[8]{0:T(128)} %broadcast_multiply_fusion.at, bf16[192,2048]{1,0:T(8,128)(2,1)} %get-tuple-element.39.middle, bf16[192,1024]{1,0:T(8,128)(2,1)} %get-tuple-element.54.refs_0_, bf16[192,1024]{1,0:T(8,128)(2,1)} %copy-done.2, bf16[192,1024]{1,0:T(8,128)(2,1)} %copy-done.3, ...), custom_call_target="tpu_custom_call" | custom-call | flops 393216 | bytes 3145728 | tf_op jit(solution)/shard_map/pallas_call | solution.py:579
  234.3 3.6 %collective-permute-done.42.refs_2_ = bf16[192,512]{1,0:T(8,128)(2,1)S(1)} collective-permute-done((bf16[192,512]{1,0:T(8,128)(2,1)S(1)}, bf16[192,512]{1,0:T(8,128)(2,1)S(1)}, u32[]{:S(2)}, u32[]{:S(2)}) %collective-permute-start.42) | collective-permute-done | bytes 196640 | tf_op jit(solution)/shard_map/ppermute | solution.py:416
  238.7 2.7 %shard_map.207 = bf16[192,2048]{1,0:T(8,128)(2,1)} custom-call(s32[8]{0:T(128)} %broadcast_multiply_fusion.at, bf16[192,2048]{1,0:T(8,128)(2,1)} %shard_map.205.out_in, bf16[192,2048]{1,0:T(8,128)(2,1)} %get-tuple-element.39.middle, bf16[192,512]{1,0:T(8,128)(2,1)} %get-tuple-element.58.refs_0_, ...), custom_call_target="tpu_custom_call", output_to_operand_aliasing={{}: (1, {})} | custom-call | flops 393216 | bytes 1572864 | tf_op jit(solution)/shard_map/pallas_call | solution.py:411
  (105 shorter events, 16.6 us)
Async XLA Ops:
  0.0 7.5 %collective-permute-start.14 = (bf16[256,2048]{1,0:T(8,128)(2,1)}, bf16[256,2048]{1,0:T(8,128)(2,1)S(1)}, u32[]{:S(2)}, u32[]{:S(2)}) collective-permute-start(bf16[256,2048]{1,0:T(8,128)(2,1)} %param.35), channel_id=1, source_target_pairs={{1,4},{3,6},{4,1},{6,3},{9,12},{11,14},{12,9},{14,11},{17,20},{19,... | collective-permute-start | bytes 3145736 | tf_op jit(solution)/shard_map/ppermute | solution.py:416
  4.5 52.5 %collective-permute-start.8 = (bf16[256,2048]{1,0:T(8,128)(2,1)}, bf16[256,2048]{1,0:T(8,128)(2,1)}, u32[]{:S(2)}, u32[]{:S(2)}) collective-permute-start(bf16[256,2048]{1,0:T(8,128)(2,1)} %constant_dynamic-update-slice_fusion), channel_id=1, source_target_pairs={{0,2},{1,3},{2,0},{3,1},{4,6},{5,7},{6,4},{7,5},{8,10},{9,11},{10,... | collective-permute-start | bytes 3145736 | tf_op jit(solution)/shard_map/ppermute | solution.py:416
  7.5 53.0 %copy-start.18 = (bf16[2048]{0:T(1024)(128)(2,1)S(1)}, bf16[2048]{0:T(1024)(128)(2,1)}, u32[]{:S(2)}) copy-start(bf16[2048]{0:T(1024)(128)(2,1)} %param.34) | copy-start | bytes 12292
  7.5 53.6 %copy-start = (bf16[2048,256]{1,0:T(8,128)(2,1)S(1)}, bf16[2048,256]{1,0:T(8,128)(2,1)}, u32[]{:S(2)}) copy-start(bf16[2048,256]{1,0:T(8,128)(2,1)} %param.36) | copy-start | bytes 3145732
  8.9 61.7 %copy-start.1 = (bf16[256,2048]{1,0:T(8,128)(2,1)}, bf16[256,2048]{1,0:T(8,128)(2,1)S(1)}, u32[]{:S(2)}) copy-start(bf16[256,2048]{1,0:T(8,128)(2,1)S(1)} %broadcast_select_fusion.6.refs_5_) | copy-start | bytes 3145732
  8.9 48.6 %collective-permute-start.16 = (bf16[256,2048]{1,0:T(8,128)(2,1)S(1)}, bf16[256,2048]{1,0:T(8,128)(2,1)}, u32[]{:S(2)}, u32[]{:S(2)}) collective-permute-start(bf16[256,2048]{1,0:T(8,128)(2,1)S(1)} %broadcast_select_fusion.6.refs_5_), channel_id=1, source_target_pairs={{0,8},{4,12},{8,0},{12,4},{16,24},{20,28},{24,16},{28,20},{1,9},{5... | collective-permute-start | bytes 3145736 | tf_op jit(solution)/shard_map/ppermute | solution.py:416
  10.6 47.0 %collective-permute-start.18 = (bf16[256,2048]{1,0:T(8,128)(2,1)S(1)}, bf16[256,2048]{1,0:T(8,128)(2,1)S(1)}, u32[]{:S(2)}, u32[]{:S(2)}) collective-permute-start(bf16[256,2048]{1,0:T(8,128)(2,1)S(1)} %broadcast_select_fusion.6.refs_5_), channel_id=1, source_target_pairs={{8,16},{12,20},{16,8},{20,12},{9,17},{13,21},{17,9},{21,13},{10,18... | collective-permute-start | bytes 3145736 | tf_op jit(solution)/shard_map/ppermute | solution.py:416
  15.9 13.0 %collective-permute-start = (bf16[208,128]{1,0:T(8,128)(2,1)}, bf16[208,128]{1,0:T(8,128)(2,1)S(1)}, u32[]{:S(2)}, u32[]{:S(2)}) collective-permute-start(bf16[208,128]{1,0:T(8,128)(2,1)} %get-tuple-element.28.own), channel_id=1, source_target_pairs={{0,4},{4,0},{8,12},{12,8},{16,20},{20,16},{24,28},{28,24},{1,5},{5... | collective-permute-start | bytes 159752 | tf_op jit(solution)/shard_map/ppermute | solution.py:416
  31.0 8.3 %collective-permute-start.1 = (bf16[208,128]{1,0:T(8,128)(2,1)}, bf16[208,128]{1,0:T(8,128)(2,1)S(1)}, u32[]{:S(2)}, u32[]{:S(2)}) collective-permute-start(bf16[208,128]{1,0:T(8,128)(2,1)} %shard_map.201), channel_id=1, source_target_pairs={{0,8},{4,12},{8,16},{12,20},{16,24},{20,28},{1,9},{5,13},{9,17},{1... | collective-permute-start | bytes 159752 | tf_op jit(solution)/shard_map/ppermute | solution.py:416
  37.1 10.2 %collective-permute-start.2 = (bf16[208,128]{1,0:T(8,128)(2,1)}, bf16[208,128]{1,0:T(8,128)(2,1)S(1)}, u32[]{:S(2)}, u32[]{:S(2)}) collective-permute-start(bf16[208,128]{1,0:T(8,128)(2,1)} %shard_map.201), channel_id=1, source_target_pairs={{0,16},{4,20},{8,24},{12,28},{1,17},{5,21},{9,25},{13,29},{2,18},{... | collective-permute-start | bytes 159752 | tf_op jit(solution)/shard_map/ppermute | solution.py:416
  39.3 8.0 %copy-start.15 = (bf16[208,128]{1,0:T(8,128)(2,1)}, bf16[208,128]{1,0:T(8,128)(2,1)S(1)}, u32[]{:S(2)}) copy-start(bf16[208,128]{1,0:T(8,128)(2,1)S(1)} %collective-permute-done.1.refs_0_) | copy-start | bytes 159748
  39.3 8.0 %collective-permute-start.3 = (bf16[208,128]{1,0:T(8,128)(2,1)}, bf16[208,128]{1,0:T(8,128)(2,1)S(1)}, u32[]{:S(2)}, u32[]{:S(2)}) collective-permute-start(bf16[208,128]{1,0:T(8,128)(2,1)} %shard_map.201), channel_id=1, source_target_pairs={{0,24},{4,28},{1,25},{5,29},{2,26},{6,30},{3,27},{7,31}} | collective-permute-start | bytes 159752 | tf_op jit(solution)/shard_map/ppermute | solution.py:416
  51.0 1.6 collective-permute-start.4
  51.0 5.9 %collective-permute-start.5 = (bf16[192,256]{1,0:T(8,128)(2,1)}, bf16[192,256]{1,0:T(8,128)(2,1)S(1)}, u32[]{:S(2)}, u32[]{:S(2)}) collective-permute-start(bf16[192,256]{1,0:T(8,128)(2,1)} %get-tuple-element.37), channel_id=1, source_target_pairs={{0,2},{1,3},{2,0},{3,1},{4,6},{5,7},{6,4},{7,5},{8,10},{9,11},{10,... | collective-permute-start | bytes 294920 | tf_op jit(solution)/shard_map/ppermute | solution.py:416
  52.6 13.0 %copy-start.12 = (bf16[192,256]{1,0:T(8,128)(2,1)}, bf16[192,256]{1,0:T(8,128)(2,1)S(1)}, u32[]{:S(2)}) copy-start(bf16[192,256]{1,0:T(8,128)(2,1)S(1)} %collective-permute-done.4.refs_1_) | copy-start | bytes 294916
  52.6 6.3 %collective-permute-start.6 = (bf16[192,256]{1,0:T(8,128)(2,1)}, bf16[192,256]{1,0:T(8,128)(2,1)S(1)}, u32[]{:S(2)}, u32[]{:S(2)}) collective-permute-start(bf16[192,256]{1,0:T(8,128)(2,1)} %get-tuple-element.38), channel_id=1, source_target_pairs={{0,3},{1,2},{2,1},{3,0},{4,7},{5,6},{6,5},{7,4},{8,11},{9,10},{10,... | collective-permute-start | bytes 294920 | tf_op jit(solution)/shard_map/ppermute | solution.py:416
  57.0 8.6 %copy-start.13 = (bf16[192,256]{1,0:T(8,128)(2,1)}, bf16[192,256]{1,0:T(8,128)(2,1)S(1)}, u32[]{:S(2)}) copy-start(bf16[192,256]{1,0:T(8,128)(2,1)S(1)} %collective-permute-done.5.refs_2_) | copy-start | bytes 294916
  57.0 4.1 %collective-permute-start.7 = (bf16[256,2048]{1,0:T(8,128)(2,1)}, bf16[256,2048]{1,0:T(8,128)(2,1)}, u32[]{:S(2)}, u32[]{:S(2)}) collective-permute-start(bf16[256,2048]{1,0:T(8,128)(2,1)} %constant_dynamic-update-slice_fusion), channel_id=1, source_target_pairs={{0,1},{1,0},{2,3},{3,2},{4,5},{5,4},{6,7},{7,6},{8,9},{9,8},{10,11... | collective-permute-start | bytes 3145736 | tf_op jit(solution)/shard_map/ppermute | solution.py:416
  57.0 5.8 %collective-permute-start.9 = (bf16[256,2048]{1,0:T(8,128)(2,1)}, bf16[256,2048]{1,0:T(8,128)(2,1)}, u32[]{:S(2)}, u32[]{:S(2)}) collective-permute-start(bf16[256,2048]{1,0:T(8,128)(2,1)} %collective-permute-done.8.refs_5_), channel_id=1, source_target_pairs={{0,1},{1,0},{2,3},{3,2},{4,5},{5,4},{6,7},{7,6},{8,9},{9,8},{10,11... | collective-permute-start | bytes 3145736 | tf_op jit(solution)/shard_map/ppermute | solution.py:416
  57.5 13.1 %collective-permute-start.17 = (bf16[256,2048]{1,0:T(8,128)(2,1)}, bf16[256,2048]{1,0:T(8,128)(2,1)}, u32[]{:S(2)}, u32[]{:S(2)}) collective-permute-start(bf16[256,2048]{1,0:T(8,128)(2,1)} %collective-permute-done.16.refs_7_), channel_id=1, source_target_pairs={{0,1},{1,0},{2,3},{3,2},{4,5},{5,4},{6,7},{7,6},{8,9},{9,8},{10,11... | collective-permute-start | bytes 3145736 | tf_op jit(solution)/shard_map/ppermute | solution.py:416
  57.6 27.5 %collective-permute-start.19 = (bf16[256,2048]{1,0:T(8,128)(2,1)S(1)}, bf16[256,2048]{1,0:T(8,128)(2,1)}, u32[]{:S(2)}, u32[]{:S(2)}) collective-permute-start(bf16[256,2048]{1,0:T(8,128)(2,1)S(1)} %collective-permute-done.18), channel_id=1, source_target_pairs={{8,0},{12,4},{16,24},{20,28},{9,1},{13,5},{17,25},{21,29},{10,2},{... | collective-permute-start | bytes 3145736 | tf_op jit(solution)/shard_map/ppermute | solution.py:416
  58.9 6.7 %copy-start.14 = (bf16[192,256]{1,0:T(8,128)(2,1)}, bf16[192,256]{1,0:T(8,128)(2,1)S(1)}, u32[]{:S(2)}) copy-start(bf16[192,256]{1,0:T(8,128)(2,1)S(1)} %collective-permute-done.6.refs_3_) | copy-start | bytes 294916
  58.9 28.6 %collective-permute-start.20 = (bf16[256,2048]{1,0:T(8,128)(2,1)}, bf16[256,2048]{1,0:T(8,128)(2,1)}, u32[]{:S(2)}, u32[]{:S(2)}) collective-permute-start(bf16[256,2048]{1,0:T(8,128)(2,1)} %collective-permute-done.16.refs_7_), channel_id=1, source_target_pairs={{8,16},{12,20},{16,8},{20,12},{9,17},{13,21},{17,9},{21,13},{10,18... | collective-permute-start | bytes 3145736 | tf_op jit(solution)/shard_map/ppermute | solution.py:416
  61.1 46.7 %collective-permute-start.24 = (bf16[2048,256]{1,0:T(8,128)(2,1)S(1)}, bf16[2048,256]{1,0:T(8,128)(2,1)}, u32[]{:S(2)}, u32[]{:S(2)}) collective-permute-start(bf16[2048,256]{1,0:T(8,128)(2,1)S(1)} %copy-done), channel_id=1, source_target_pairs={{1,4},{3,6},{4,1},{6,3},{9,12},{11,14},{12,9},{14,11},{17,20},{19,... | collective-permute-start | bytes 3145736 | tf_op jit(solution)/shard_map/ppermute | solution.py:416
  62.8 47.7 %collective-permute-start.15 = (bf16[256,2048]{1,0:T(8,128)(2,1)S(1)}, bf16[256,2048]{1,0:T(8,128)(2,1)}, u32[]{:S(2)}, u32[]{:S(2)}) collective-permute-start(bf16[256,2048]{1,0:T(8,128)(2,1)S(1)} %broadcast_select_fusion.6.refs_5_), channel_id=1, source_target_pairs={{0,1},{1,0},{2,3},{3,2},{4,5},{5,4},{6,7},{7,6},{8,9},{9,8},{10,11... | collective-permute-start | bytes 3145736 | tf_op jit(solution)/shard_map/ppermute | solution.py:416
  70.6 19.9 %collective-permute-start.10 = (bf16[192,2048]{1,0:T(8,128)(2,1)}, bf16[192,2048]{1,0:T(8,128)(2,1)}, u32[]{:S(2)}, u32[]{:S(2)}) collective-permute-start(bf16[192,2048]{1,0:T(8,128)(2,1)} %get-tuple-element.40.refs_0_), channel_id=1, source_target_pairs={{0,2},{1,3},{2,0},{3,1},{4,6},{5,7},{6,4},{7,5},{8,10},{9,11},{10,... | collective-permute-start | bytes 2359304 | tf_op jit(solution)/shard_map/ppermute | solution.py:416
  85.1 20.0 %collective-permute-start.11 = (bf16[192,2048]{1,0:T(8,128)(2,1)}, bf16[192,2048]{1,0:T(8,128)(2,1)}, u32[]{:S(2)}, u32[]{:S(2)}) collective-permute-start(bf16[192,2048]{1,0:T(8,128)(2,1)} %get-tuple-element.41), channel_id=1, source_target_pairs={{0,4},{4,0},{8,12},{12,8},{16,20},{20,16},{24,28},{28,24},{1,5},{5... | collective-permute-start | bytes 2359304 | tf_op jit(solution)/shard_map/ppermute | solution.py:416
  89.8 28.4 %collective-permute-start.21 = (bf16[256,2048]{1,0:T(8,128)(2,1)}, bf16[256,2048]{1,0:T(8,128)(2,1)}, u32[]{:S(2)}, u32[]{:S(2)}) collective-permute-start(bf16[256,2048]{1,0:T(8,128)(2,1)} %broadcast_select_fusion.5.refs_9_), channel_id=1, source_target_pairs={{0,1},{1,0},{2,3},{3,2},{4,5},{5,4},{6,7},{7,6},{8,9},{9,8},{10,11... | collective-permute-start | bytes 3145736 | tf_op jit(solution)/shard_map/ppermute | solution.py:416
  90.5 38.9 %collective-permute-start.22 = (bf16[256,2048]{1,0:T(8,128)(2,1)}, bf16[256,2048]{1,0:T(8,128)(2,1)}, u32[]{:S(2)}, u32[]{:S(2)}) collective-permute-start(bf16[256,2048]{1,0:T(8,128)(2,1)} %collective-permute-done.20), channel_id=1, source_target_pairs={{8,0},{12,4},{16,24},{20,28},{9,1},{13,5},{17,25},{21,29},{10,2},{... | collective-permute-start | bytes 3145736 | tf_op jit(solution)/shard_map/ppermute | solution.py:416
  105.1 10.0 %collective-permute-start.12 = (bf16[96,2048]{1,0:T(8,128)(2,1)S(1)}, bf16[96,2048]{1,0:T(8,128)(2,1)S(1)}, u32[]{:S(2)}, u32[]{:S(2)}) collective-permute-start(bf16[96,2048]{1,0:T(8,128)(2,1)S(1)} %slice.60), channel_id=1, source_target_pairs={{0,4},{4,0},{8,12},{12,8},{16,20},{20,16},{24,28},{28,24},{1,5},{5... | collective-permute-start | bytes 1179656 | tf_op jit(solution)/shard_map/ppermute | solution.py:416
  107.8 9.5 %collective-permute-start.13 = (bf16[96,2048]{1,0:T(8,128)(2,1)S(1)}, bf16[96,2048]{1,0:T(8,128)(2,1)S(1)}, u32[]{:S(2)}, u32[]{:S(2)}) collective-permute-start(bf16[96,2048]{1,0:T(8,128)(2,1)S(1)} %slice.61), channel_id=1, source_target_pairs={{0,2},{1,3},{2,0},{3,1},{4,6},{5,7},{6,4},{7,5},{8,10},{9,11},{10,... | collective-permute-start | bytes 1179656 | tf_op jit(solution)/shard_map/ppermute | solution.py:416
  110.5 30.8 %collective-permute-start.26 = (bf16[2048,256]{1,0:T(8,128)(2,1)}, bf16[2048,256]{1,0:T(8,128)(2,1)}, u32[]{:S(2)}, u32[]{:S(2)}) collective-permute-start(bf16[2048,256]{1,0:T(8,128)(2,1)} %broadcast_select_fusion.3), channel_id=1, source_target_pairs={{0,8},{4,12},{8,0},{12,4},{16,24},{20,28},{24,16},{28,20},{1,9},{5... | collective-permute-start | bytes 3145736 | tf_op jit(solution)/shard_map/ppermute | solution.py:416
  115.1 3.1 %copy-start.20 = (bf16[96,2048]{1,0:T(8,128)(2,1)}, bf16[96,2048]{1,0:T(8,128)(2,1)S(1)}, u32[]{:S(2)}) copy-start(bf16[96,2048]{1,0:T(8,128)(2,1)S(1)} %collective-permute-done.12.refs_3_) | copy-start | bytes 1179652
  115.1 27.9 %collective-permute-start.31 = (bf16[2048,256]{1,0:T(8,128)(2,1)}, bf16[2048,256]{1,0:T(8,128)(2,1)S(1)}, u32[]{:S(2)}, u32[]{:S(2)}) collective-permute-start(bf16[2048,256]{1,0:T(8,128)(2,1)} %broadcast_select_fusion.3), channel_id=1, source_target_pairs={{8,16},{12,20},{16,8},{20,12},{9,17},{13,21},{17,9},{21,13},{10,18... | collective-permute-start | bytes 3145736 | tf_op jit(solution)/shard_map/ppermute | solution.py:416
  117.4 0.8 copy-start.21
  130.7 13.7 %collective-permute-start.23 = (bf16[256,2048]{1,0:T(8,128)(2,1)S(1)}, bf16[256,2048]{1,0:T(8,128)(2,1)S(1)}, u32[]{:S(2)}, u32[]{:S(2)}) collective-permute-start(bf16[256,2048]{1,0:T(8,128)(2,1)S(1)} %broadcast_select_fusion.4), channel_id=1, source_target_pairs={{0,1},{1,0},{2,3},{3,2},{4,5},{5,4},{6,7},{7,6},{8,9},{9,8},{10,11... | collective-permute-start | bytes 3145736 | tf_op jit(solution)/shard_map/ppermute | solution.py:416
  130.8 18.6 %collective-permute-start.25 = (bf16[2048,256]{1,0:T(8,128)(2,1)}, bf16[2048,256]{1,0:T(8,128)(2,1)S(1)}, u32[]{:S(2)}, u32[]{:S(2)}) collective-permute-start(bf16[2048,256]{1,0:T(8,128)(2,1)} %broadcast_select_fusion.3), channel_id=1, source_target_pairs={{0,1},{1,0},{2,3},{3,2},{4,5},{5,4},{6,7},{7,6},{8,9},{9,8},{10,11... | collective-permute-start | bytes 3145736 | tf_op jit(solution)/shard_map/ppermute | solution.py:416
  141.3 8.1 %collective-permute-start.27 = (bf16[2048,256]{1,0:T(8,128)(2,1)}, bf16[2048,256]{1,0:T(8,128)(2,1)S(1)}, u32[]{:S(2)}, u32[]{:S(2)}) collective-permute-start(bf16[2048,256]{1,0:T(8,128)(2,1)} %collective-permute-done.26), channel_id=1, source_target_pairs={{0,1},{1,0},{2,3},{3,2},{4,5},{5,4},{6,7},{7,6},{8,9},{9,8},{10,11... | collective-permute-start | bytes 3145736 | tf_op jit(solution)/shard_map/ppermute | solution.py:416
  141.3 29.1 %collective-permute-start.33 = (bf16[2048,256]{1,0:T(8,128)(2,1)}, bf16[2048,256]{1,0:T(8,128)(2,1)}, u32[]{:S(2)}, u32[]{:S(2)}) collective-permute-start(bf16[2048,256]{1,0:T(8,128)(2,1)} %collective-permute-done.26), channel_id=1, source_target_pairs={{8,16},{12,20},{16,8},{20,12},{9,17},{13,21},{17,9},{21,13},{10,18... | collective-permute-start | bytes 3145736 | tf_op jit(solution)/shard_map/ppermute | solution.py:416
  143.0 27.5 %collective-permute-start.32 = (bf16[2048,256]{1,0:T(8,128)(2,1)S(1)}, bf16[2048,256]{1,0:T(8,128)(2,1)S(1)}, u32[]{:S(2)}, u32[]{:S(2)}) collective-permute-start(bf16[2048,256]{1,0:T(8,128)(2,1)S(1)} %collective-permute-done.31), channel_id=1, source_target_pairs={{8,0},{12,4},{16,24},{20,28},{9,1},{13,5},{17,25},{21,29},{10,2},{... | collective-permute-start | bytes 3145736 | tf_op jit(solution)/shard_map/ppermute | solution.py:416
  149.4 6.1 %copy-start.22 = (bf16[768,2048]{1,0:T(8,128)(2,1)}, bf16[768,2048]{1,0:T(8,128)(2,1)S(1)}, u32[]{:S(2)}) copy-start(bf16[768,2048]{1,0:T(8,128)(2,1)S(1)} %multiply_convert_fusion) | copy-start | bytes 9437188
  171.6 4.4 %collective-permute-start.34 = (bf16[2048,256]{1,0:T(8,128)(2,1)}, bf16[2048,256]{1,0:T(8,128)(2,1)}, u32[]{:S(2)}, u32[]{:S(2)}) collective-permute-start(bf16[2048,256]{1,0:T(8,128)(2,1)} %broadcast_select_fusion.2), channel_id=1, source_target_pairs={{0,1},{1,0},{2,3},{3,2},{4,5},{5,4},{6,7},{7,6},{8,9},{9,8},{10,11... | collective-permute-start | bytes 3145736 | tf_op jit(solution)/shard_map/ppermute | solution.py:416
  171.6 27.8 %collective-permute-start.38 = (bf16[2048,256]{1,0:T(8,128)(2,1)}, bf16[2048,256]{1,0:T(8,128)(2,1)}, u32[]{:S(2)}, u32[]{:S(2)}) collective-permute-start(bf16[2048,256]{1,0:T(8,128)(2,1)} %collective-permute-done.33), channel_id=1, source_target_pairs={{8,0},{12,4},{16,24},{20,28},{9,1},{13,5},{17,25},{21,29},{10,2},{... | collective-permute-start | bytes 3145736 | tf_op jit(solution)/shard_map/ppermute | solution.py:416
  175.4 30.4 %collective-permute-start.40 = (bf16[2048,256]{1,0:T(8,128)(2,1)S(1)}, bf16[2048,256]{1,0:T(8,128)(2,1)S(1)}, u32[]{:S(2)}, u32[]{:S(2)}) collective-permute-start(bf16[2048,256]{1,0:T(8,128)(2,1)S(1)} %collective-permute-done.31), channel_id=1, source_target_pairs={{0,1},{1,0},{2,3},{3,2},{4,5},{5,4},{6,7},{7,6},{8,9},{9,8},{10,11... | collective-permute-start | bytes 3145736 | tf_op jit(solution)/shard_map/ppermute | solution.py:416
  199.3 8.8 %collective-permute-start.39 = (bf16[2048,256]{1,0:T(8,128)(2,1)}, bf16[2048,256]{1,0:T(8,128)(2,1)S(1)}, u32[]{:S(2)}, u32[]{:S(2)}) collective-permute-start(bf16[2048,256]{1,0:T(8,128)(2,1)} %collective-permute-done.38), channel_id=1, source_target_pairs={{0,1},{1,0},{2,3},{3,2},{4,5},{5,4},{6,7},{7,6},{8,9},{9,8},{10,11... | collective-permute-start | bytes 3145736 | tf_op jit(solution)/shard_map/ppermute | solution.py:416
  200.2 8.5 %copy-start.23 = (bf16[768,2048]{1,0:T(8,128)(2,1)S(1)}, bf16[768,2048]{1,0:T(8,128)(2,1)}, u32[]{:S(2)}) copy-start(bf16[768,2048]{1,0:T(8,128)(2,1)} %copy-done.22) | copy-start | bytes 9437188
  200.2 12.9 %collective-permute-start.28 = (bf16[192,1024]{1,0:T(8,128)(2,1)S(1)}, bf16[192,1024]{1,0:T(8,128)(2,1)S(1)}, u32[]{:S(2)}, u32[]{:S(2)}) collective-permute-start(bf16[192,1024]{1,0:T(8,128)(2,1)S(1)} %get-tuple-element.53), channel_id=1, source_target_pairs={{0,6},{1,7},{2,4},{3,5},{4,2},{5,3},{6,0},{7,1},{8,14},{9,15},{10,... | collective-permute-start | bytes 1179656 | tf_op jit(solution)/shard_map/ppermute | solution.py:416
  202.4 19.0 %collective-permute-start.29 = (bf16[192,1024]{1,0:T(8,128)(2,1)S(1)}, bf16[192,1024]{1,0:T(8,128)(2,1)S(1)}, u32[]{:S(2)}, u32[]{:S(2)}) collective-permute-start(bf16[192,1024]{1,0:T(8,128)(2,1)S(1)} %get-tuple-element.52), channel_id=1, source_target_pairs={{0,2},{1,3},{2,0},{3,1},{4,6},{5,7},{6,4},{7,5},{8,10},{9,11},{10,... | collective-permute-start | bytes 1179656 | tf_op jit(solution)/shard_map/ppermute | solution.py:416
  203.0 20.1 %collective-permute-start.30 = (bf16[192,1024]{1,0:T(8,128)(2,1)S(1)}, bf16[192,1024]{1,0:T(8,128)(2,1)S(1)}, u32[]{:S(2)}, u32[]{:S(2)}) collective-permute-start(bf16[192,1024]{1,0:T(8,128)(2,1)S(1)} %get-tuple-element.51), channel_id=1, source_target_pairs={{0,4},{4,0},{8,12},{12,8},{16,20},{20,16},{24,28},{28,24},{1,5},{5... | collective-permute-start | bytes 1179656 | tf_op jit(solution)/shard_map/ppermute | solution.py:416
  205.8 20.0 %collective-permute-start.35 = (bf16[192,512]{1,0:T(8,128)(2,1)S(1)}, bf16[192,512]{1,0:T(8,128)(2,1)S(1)}, u32[]{:S(2)}, u32[]{:S(2)}) collective-permute-start(bf16[192,512]{1,0:T(8,128)(2,1)S(1)} %get-tuple-element.61), channel_id=1, source_target_pairs={{0,6},{1,7},{2,4},{3,5},{4,2},{5,3},{6,0},{7,1},{8,14},{9,15},{10,... | collective-permute-start | bytes 589832 | tf_op jit(solution)/shard_map/ppermute | solution.py:416
  208.1 21.8 %collective-permute-start.36 = (bf16[192,512]{1,0:T(8,128)(2,1)S(1)}, bf16[192,512]{1,0:T(8,128)(2,1)S(1)}, u32[]{:S(2)}, u32[]{:S(2)}) collective-permute-start(bf16[192,512]{1,0:T(8,128)(2,1)S(1)} %get-tuple-element.60), channel_id=1, source_target_pairs={{0,2},{1,3},{2,0},{3,1},{4,6},{5,7},{6,4},{7,5},{8,10},{9,11},{10,... | collective-permute-start | bytes 589832 | tf_op jit(solution)/shard_map/ppermute | solution.py:416
  208.8 18.4 %copy-start.19 = (s32[8]{0:T(128)S(1)}, s32[8]{0:T(128)}, u32[]{:S(2)}) copy-start(s32[8]{0:T(128)} %stack.53.at) | copy-start | bytes 100
  213.2 16.9 %copy-start.2 = (bf16[192,1024]{1,0:T(8,128)(2,1)}, bf16[192,1024]{1,0:T(8,128)(2,1)S(1)}, u32[]{:S(2)}) copy-start(bf16[192,1024]{1,0:T(8,128)(2,1)S(1)} %collective-permute-done.28.refs_1_) | copy-start | bytes 1179652
  213.2 16.9 %collective-permute-start.37 = (bf16[192,512]{1,0:T(8,128)(2,1)S(1)}, bf16[192,512]{1,0:T(8,128)(2,1)S(1)}, u32[]{:S(2)}, u32[]{:S(2)}) collective-permute-start(bf16[192,512]{1,0:T(8,128)(2,1)S(1)} %get-tuple-element.59), channel_id=1, source_target_pairs={{0,4},{4,0},{8,12},{12,8},{16,20},{20,16},{24,28},{28,24},{1,5},{5... | collective-permute-start | bytes 589832 | tf_op jit(solution)/shard_map/ppermute | solution.py:416
  221.4 8.7 %copy-start.3 = (bf16[192,1024]{1,0:T(8,128)(2,1)}, bf16[192,1024]{1,0:T(8,128)(2,1)S(1)}, u32[]{:S(2)}) copy-start(bf16[192,1024]{1,0:T(8,128)(2,1)S(1)} %collective-permute-done.29.refs_2_) | copy-start | bytes 1179652
  221.4 12.9 %collective-permute-start.41 = (bf16[192,512]{1,0:T(8,128)(2,1)S(1)}, bf16[192,512]{1,0:T(8,128)(2,1)S(1)}, u32[]{:S(2)}, u32[]{:S(2)}) collective-permute-start(bf16[192,512]{1,0:T(8,128)(2,1)S(1)} %get-tuple-element.57), channel_id=1, source_target_pairs={{0,6},{1,7},{2,4},{3,5},{4,2},{5,3},{6,0},{7,1},{8,14},{9,15},{10,... | collective-permute-start | bytes 589832 | tf_op jit(solution)/shard_map/ppermute | solution.py:416
  223.1 7.0 %copy-start.4 = (bf16[192,1024]{1,0:T(8,128)(2,1)}, bf16[192,1024]{1,0:T(8,128)(2,1)S(1)}, u32[]{:S(2)}) copy-start(bf16[192,1024]{1,0:T(8,128)(2,1)S(1)} %collective-permute-done.30.refs_3_) | copy-start | bytes 1179652
  223.1 14.8 %collective-permute-start.42 = (bf16[192,512]{1,0:T(8,128)(2,1)S(1)}, bf16[192,512]{1,0:T(8,128)(2,1)S(1)}, u32[]{:S(2)}, u32[]{:S(2)}) collective-permute-start(bf16[192,512]{1,0:T(8,128)(2,1)S(1)} %get-tuple-element.56), channel_id=1, source_target_pairs={{0,2},{1,3},{2,0},{3,1},{4,6},{5,7},{6,4},{7,5},{8,10},{9,11},{10,... | collective-permute-start | bytes 589832 | tf_op jit(solution)/shard_map/ppermute | solution.py:416
  225.8 4.2 %copy-start.6 = (bf16[192,512]{1,0:T(8,128)(2,1)}, bf16[192,512]{1,0:T(8,128)(2,1)S(1)}, u32[]{:S(2)}) copy-start(bf16[192,512]{1,0:T(8,128)(2,1)S(1)} %collective-permute-done.35.refs_5_) | copy-start | bytes 589828
  225.8 12.1 %collective-permute-start.43 = (bf16[192,512]{1,0:T(8,128)(2,1)S(1)}, bf16[192,512]{1,0:T(8,128)(2,1)S(1)}, u32[]{:S(2)}, u32[]{:S(2)}) collective-permute-start(bf16[192,512]{1,0:T(8,128)(2,1)S(1)} %get-tuple-element.55), channel_id=1, source_target_pairs={{0,4},{4,0},{8,12},{12,8},{16,20},{20,16},{24,28},{28,24},{1,5},{5... | collective-permute-start | bytes 589832 | tf_op jit(solution)/shard_map/ppermute | solution.py:416
  230.1 0.7 copy-start.8
  234.3 3.6 %copy-start.9 = (bf16[192,512]{1,0:T(8,128)(2,1)}, bf16[192,512]{1,0:T(8,128)(2,1)S(1)}, u32[]{:S(2)}) copy-start(bf16[192,512]{1,0:T(8,128)(2,1)S(1)} %collective-permute-done.41.refs_1_) | copy-start | bytes 589828
  237.9 0.7 copy-start.10
  237.9 0.7 copy-start.11
  (4 other events, 2.5 us)

commit v2 on v1

--- a/solution.py
+++ b/solution.py
@@ -377,40 +377,6 @@
     return run(seen)
 
 
-def last_kernel(at, out_in, middle, *refs):
-    *parts, out = refs
-    total = middle[...].astype(F32)
-    for part in parts:
-        total = total + part[...].astype(F32)
-    out[...] = total.astype(BF16)
-
-
-def place_last(at, out, middle, parts):
-    rows = middle.shape[0]
-    side = parts[0].shape[1] // 2
-    skip = at.shape[0] - 2
-
-    def column(n, a):
-        return (0, a[skip + n] // (side // UNIT))
-
-    run = pl.pallas_call(
-        last_kernel,
-        out_shape=jax.ShapeDtypeStruct(middle.shape, BF16),
-        grid_spec=pltpu.PrefetchScalarGridSpec(
-            num_scalar_prefetch=1,
-            grid=(2,),
-            in_specs=[pl.BlockSpec(memory_space=pl.ANY), pl.BlockSpec((rows, side), column)]
-            + [pl.BlockSpec((rows, side), lambda n, a: (0, n))] * len(parts),
-            out_specs=pl.BlockSpec((rows, side), column),
-        ),
-        input_output_aliases={1: 0},
-        cost_estimate=pl.CostEstimate(
-            flops=middle.size, bytes_accessed=4 * middle.size, transcendentals=0
-        ),
-    )
-    return run(at, out, middle, *parts)
-
-
 def exchange(array, axis, size, move):
     pairs = [(i, move(i)) for i in range(size)]
     return lax.ppermute(array, axis, [(i, j) for i, j in pairs if j is not None and 0 <= j < size])
@@ -569,7 +535,8 @@
         ]
 
     sums = down(0, down_first)
-    down_far = jnp.where(at_end, tie(down_out, parts[0]), down_in)
+    wait = hold(stream_in[32:48, :128])
+    down_far = jnp.where(at_end, tie(down_out, parts[0], wait), down_in)
     sums += down(1, both_cores(down_far))
     pause = hold(stream_in[:16, :128])
     ends_final = both_cores(tie(down_last, parts[1], pause))
@@ -583,7 +550,12 @@
         middle.size,
         8 * middle.size,
     )(units, middle, *sums[:-4])
-    return place_last(units, out, middle, sums[-4:])
+    part = sum(p.astype(F32) for p in sums[-4:])
+    width = part.shape[1]
+    part = jnp.where(core == 0, part, jnp.roll(part, width // 2, axis=1))
+    start = slots[3] * width
+    part = part + lax.dynamic_slice_in_dim(middle, start, width, 1).astype(F32)
+    return lax.dynamic_update_slice_in_dim(out, part.astype(BF16), start, 1)
 
 
 def group_feed_forward(middle, normed):

time: 242 us -> 245 us (1.012)
  other arithmetic: 9.23 us -> 12 us
    pallas_call x1 -> x0, Pallas kernels: 2.68 us -> none  [place_last(): return run(at, out, middle, *parts)]
    unnamed x49 -> x43, local copies, waits for them, and re-layouts: 5.32 us -> 4.63 us
  transfers between devices with their start and end apart: 44 -> 44, of which waited for: 18 -> 19; matrix products, arithmetic and copies ran while one was open for 16% -> 16% of each run, Pallas kernels for 14% -> 14%
where the time goes in v2:
time: 245 us; the launch traced here: 243 us
  waiting for transfers between devices  99.9 us (41%)
  starting transfers between devices  63.8 us (26%)
  Pallas kernels  34.9 us (14%)
  matrix products  17.6 us (7%)
  local copies, waits for them, and re-layouts  14.8 us (6%)
  other arithmetic  12 us (5%)
    ppermute x44, waiting for transfers between devices, exchange(): lax.ppermute(array, axis, [(i, j) for i, j in pairs if j is not None and...  99.9 us
    ppermute x44, starting transfers between devices, exchange(): lax.ppermute(array, axis, [(i, j) for i, j in pairs if j is not None and...  63.8 us
    dot_general x3, matrix products, down(): jnp.dot(hidden, jnp.concatenate(blocks, axis=1), preferred_element_type=F32)  12.8 us
    pallas_call x1, Pallas kernels, up_most(): return run(at, *pieces, *blocks)  11.2 us
    pallas_call x1, Pallas kernels, to_middle(): call(middle_kernel, (jax.ShapeDtypeStruct((rows, depth), BF16),) * 3, 3 +...  5 us
    pallas_call x1, Pallas kernels, retention(): call(local_kernel, (sds((length, lanes), F32),) * 2 + (sds((length, lanes...  4.96 us
  transfers between devices with their start and end apart: 44, of which 19 were waited for; matrix products, arithmetic and copies ran while one was open for 16% of the time, Pallas kernels for 14%

profile of v2, /device:TPU:0, one launch (start us, length us, event | category | flops | bytes accessed | tf_op | source)
XLA Modules:
  0.0 243.4 jit_solution(18127199093436986507)
XLA Ops:
  0.7 1.9 constant_dynamic-update-slice_fusion.1
  2.6 1.9 constant_dynamic-update-slice_fusion
  4.5 3.0 %collective-permute-start.8 = (bf16[256,2048]{1,0:T(8,128)(2,1)}, bf16[256,2048]{1,0:T(8,128)(2,1)}, u32[]{:S(2)}, u32[]{:S(2)}) collective-permute-start(bf16[256,2048]{1,0:T(8,128)(2,1)} %constant_dynamic-update-slice_fusion), channel_id=1, source_target_pairs={{0,2},{1,3},{2,0},{3,1},{4,6},{5,7},{6,4},{7,5},{8,10},{9,11},{10,... | collective-permute-start | bytes 3145736 | tf_op jit(solution)/shard_map/ppermute | solution.py:382
  7.5 1.4 broadcast_select_fusion.6.refs_5_
  8.9 1.6 collective-permute-start.16
  11.3 1.3 dynamic-slice_bitcast_fusion.rows
  12.6 3.3 %shard_map.199 = (bf16[208,128]{1,0:T(8,128)(2,1)}, f32[768,8]{1,0:T(8,128)}, f32[8,768]{1,0:T(8,128)}) custom-call(bf16[768,128]{1,0:T(8,128)(2,1)} %kw.3, bf16[768,128]{1,0:T(8,128)(2,1)} %vw.3, bf16[768,128]{1,0:T(8,128)(2,1)} %kn.3, bf16[768,128]{1,0:T(8,128)(2,1)} %vn.3, f32[1,768]{1,0:T(1,128)} %dw.1, f32[2,768]{1,0:T(2,128)} %dn.1, ...), custom_call_target="tpu_custom_call" | custom-call | flops 50331648 | bytes 2359296 | tf_op jit(solution)/shard_map/pallas_call | solution.py:394
  15.9 10.5 %collective-permute-start = (bf16[208,128]{1,0:T(8,128)(2,1)}, bf16[208,128]{1,0:T(8,128)(2,1)S(1)}, u32[]{:S(2)}, u32[]{:S(2)}) collective-permute-start(bf16[208,128]{1,0:T(8,128)(2,1)} %get-tuple-element.28.own), channel_id=1, source_target_pairs={{0,4},{4,0},{8,12},{12,8},{16,20},{20,16},{24,28},{28,24},{1,5},{5... | collective-permute-start | bytes 159752 | tf_op jit(solution)/shard_map/ppermute | solution.py:382
  27.0 1.8 collective-permute-done.other
  29.5 1.5 shard_map.201
  31.0 6.1 %collective-permute-start.1 = (bf16[208,128]{1,0:T(8,128)(2,1)}, bf16[208,128]{1,0:T(8,128)(2,1)S(1)}, u32[]{:S(2)}, u32[]{:S(2)}) collective-permute-start(bf16[208,128]{1,0:T(8,128)(2,1)} %shard_map.201), channel_id=1, source_target_pairs={{0,8},{4,12},{8,16},{12,20},{16,24},{20,28},{1,9},{5,13},{9,17},{1... | collective-permute-start | bytes 159752 | tf_op jit(solution)/shard_map/ppermute | solution.py:382
  37.1 1.5 collective-permute-start.2
  39.3 3.0 %collective-permute-start.3 = (bf16[208,128]{1,0:T(8,128)(2,1)}, bf16[208,128]{1,0:T(8,128)(2,1)S(1)}, u32[]{:S(2)}, u32[]{:S(2)}) collective-permute-start(bf16[208,128]{1,0:T(8,128)(2,1)} %shard_map.201), channel_id=1, source_target_pairs={{0,24},{4,28},{1,25},{5,29},{2,26},{6,30},{3,27},{7,31}} | collective-permute-start | bytes 159752 | tf_op jit(solution)/shard_map/ppermute | solution.py:382
  42.4 5.0 %shard_map.200 = (f32[768,128]{1,0:T(8,128)}, f32[768,128]{1,0:T(8,128)}, bf16[768,128]{1,0:T(8,128)(2,1)}, bf16[768,128]{1,0:T(8,128)(2,1)}) custom-call(bf16[768,128]{1,0:T(8,128)(2,1)} %qw.1, bf16[768,128]{1,0:T(8,128)(2,1)} %kw.3, bf16[768,128]{1,0:T(8,128)(2,1)} %vw.3, bf16[768,128]{1,0:T(8,128)(2,1)} %qn.1, bf16[768,128]{1,0:T(8,128)(2,1)} %kn.3, ...), custom_call_target="tpu_custom_call" | custom-call | flops 603979776 | bytes 3932160 | tf_op jit(solution)/shard_map/pallas_call | solution.py:401
  48.0 3.1 %shard_map.202 = (bf16[192,256]{1,0:T(8,128)(2,1)}, bf16[192,256]{1,0:T(8,128)(2,1)}, bf16[192,256]{1,0:T(8,128)(2,1)}, bf16[192,256]{1,0:T(8,128)(2,1)}) custom-call(s32[5]{0:T(128)} %stack.59.late, bf16[208,128]{1,0:T(8,128)(2,1)} %get-tuple-element.28.own, bf16[208,128]{1,0:T(8,128)(2,1)} %copy-done.5, f32[768,128]{1,0:T(8,128)} %get-tuple-element.31.ow, ...), custom_call_target="tpu_custom_call" | custom-call | flops 50331648 | bytes 2359296 | tf_op jit(solution)/shard_map/pallas_call | solution.py:415
  51.1 1.6 collective-permute-start.5
  52.7 1.2 collective-permute-start.6
  53.9 3.2 %collective-permute-done.5.refs_2_ = bf16[192,256]{1,0:T(8,128)(2,1)S(1)} collective-permute-done((bf16[192,256]{1,0:T(8,128)(2,1)}, bf16[192,256]{1,0:T(8,128)(2,1)S(1)}, u32[]{:S(2)}, u32[]{:S(2)}) %collective-permute-start.5) | collective-permute-done | bytes 98336 | tf_op jit(solution)/shard_map/ppermute | solution.py:382
  57.7 1.3 collective-permute-start.19
  59.0 1.6 collective-permute-start.20
  61.2 1.6 collective-permute-start.24
  62.8 2.8 %collective-permute-start.15 = (bf16[256,2048]{1,0:T(8,128)(2,1)S(1)}, bf16[256,2048]{1,0:T(8,128)(2,1)}, u32[]{:S(2)}, u32[]{:S(2)}) collective-permute-start(bf16[256,2048]{1,0:T(8,128)(2,1)S(1)} %broadcast_select_fusion.6.refs_5_), channel_id=1, source_target_pairs={{0,1},{1,0},{2,3},{3,2},{4,5},{5,4},{6,7},{7,6},{8,9},{9,8},{10,11... | collective-permute-start | bytes 3145736 | tf_op jit(solution)/shard_map/ppermute | solution.py:382
  65.7 5.0 %shard_map.203 = (bf16[192,2048]{1,0:T(8,128)(2,1)}, bf16[192,2048]{1,0:T(8,128)(2,1)}, bf16[192,2048]{1,0:T(8,128)(2,1)}) custom-call(bf16[192,2048]{1,0:T(8,128)(2,1)} %stream.1, bf16[1,2048]{1,0:T(2,128)(2,1)} %broadcast_in_dim.3.gain, bf16[128,2048]{1,0:T(8,128)(2,1)} %wide.1, bf16[128,2048]{1,0:T(8,128)(2,1)} %narrow.1, ...), custom_call_target="tpu_custom_call" | custom-call | flops 805306368 | bytes 3145728 | tf_op jit(solution)/shard_map/pallas_call | solution.py:434
  70.7 1.6 collective-permute-start.10
  72.2 12.9 %collective-permute-done.19 = bf16[256,2048]{1,0:T(8,128)(2,1)} collective-permute-done((bf16[256,2048]{1,0:T(8,128)(2,1)S(1)}, bf16[256,2048]{1,0:T(8,128)(2,1)}, u32[]{:S(2)}, u32[]{:S(2)}) %collective-permute-start.19) | collective-permute-done | bytes 1048608 | tf_op jit(solution)/shard_map/ppermute | solution.py:382
  85.2 2.4 collective-permute-start.11
  87.5 2.3 broadcast_select_fusion.5.refs_9_
  90.6 1.3 collective-permute-start.22
  93.6 11.6 %collective-permute-done.11.refs_2_ = bf16[192,2048]{1,0:T(8,128)(2,1)} collective-permute-done((bf16[192,2048]{1,0:T(8,128)(2,1)}, bf16[192,2048]{1,0:T(8,128)(2,1)}, u32[]{:S(2)}, u32[]{:S(2)}) %collective-permute-start.11) | collective-permute-done | bytes 786464 | tf_op jit(solution)/shard_map/ppermute | solution.py:382
  105.1 1.7 collective-permute-start.12
  107.9 1.6 collective-permute-start.13
  109.5 1.1 broadcast_select_fusion.3
  110.6 4.6 %collective-permute-done.12.refs_3_ = bf16[96,2048]{1,0:T(8,128)(2,1)S(1)} collective-permute-done((bf16[96,2048]{1,0:T(8,128)(2,1)S(1)}, bf16[96,2048]{1,0:T(8,128)(2,1)S(1)}, u32[]{:S(2)}, u32[]{:S(2)}) %collective-permute-start.12) | collective-permute-done | bytes 393248 | tf_op jit(solution)/shard_map/ppermute | solution.py:382
  115.9 1.6 collective-permute-done.13.refs_4_
  118.2 11.2 %shard_map.204 = (f32[768,2048]{1,0:T(8,128)}, bf16[768,512]{1,0:T(8,128)(2,1)}) custom-call(s32[8]{0:T(128)} %stack.53.at, bf16[192,2048]{1,0:T(8,128)(2,1)} %get-tuple-element.40.refs_0_, bf16[192,2048]{1,0:T(8,128)(2,1)} %collective-permute-done.10.refs_1_, bf16[192,2048]{1,0:T(8,128)(2,1)} %collective-permute-done.11.refs_2_, ...), custom_call_target="tpu_custom_call" | custom-call | flops 4831838208 | bytes 17825792 | tf_op jit(solution)/shard_map/pallas_call | solution.py:336
  129.4 1.3 broadcast_select_fusion.4
  131.4 9.9 %collective-permute-done.26 = bf16[2048,256]{1,0:T(8,128)(2,1)} collective-permute-done((bf16[2048,256]{1,0:T(8,128)(2,1)}, bf16[2048,256]{1,0:T(8,128)(2,1)}, u32[]{:S(2)}, u32[]{:S(2)}) %collective-permute-start.26) | collective-permute-done | bytes 1048608 | tf_op jit(solution)/shard_map/ppermute | solution.py:382
  141.3 1.3 fusion.37
  142.6 1.3 shard_map.205
  143.9 1.7 collective-permute-start.33
  145.6 1.5 collective-permute-start.32
  147.0 4.8 %multiply_convert_fusion = bf16[768,2048]{1,0:T(8,128)(2,1)S(1)} fusion(f32[768,2048]{1,0:T(8,128)} %get-tuple-element.43, bf16[768,512]{1,0:T(8,128)(2,1)} %get-tuple-element.44, bf16[256,2048]{1,0:T(8,128)(2,1)S(1)} %collective-permute-done.23, bf16[256,2048]{1,0:T(8,128)(2,1)S(1)} %broadcast_select_fusion.4), kind=kOutput, calls=%fused_computation | convolution fusion | flops 1621098496 | bytes 12320768 | tf_op jit(solution)/shard_map/dot_general | solution.py:340
  151.9 6.7 %fusion.19 = bf16[768,1024]{1,0:T(8,128)(2,1)S(1)} fusion(bf16[768,2048]{1,0:T(8,128)(2,1)S(1)} %multiply_convert_fusion, bf16[2048,256]{1,0:T(8,128)(2,1)} %collective-permute-done.27, bf16[2048,256]{1,0:T(8,128)(2,1)} %collective-permute-done.26, bf16[2048,256]{1,0:T(8,128)(2,1)} %collective-permute-done.25, bf16[2048,256]{1,0:T(8,128)(2,1)} %broadcast_select_fusion.3), kind=kOutput, calls=%fused_computation.20 | convolution fusion | flops 3238789120 | bytes 8912896 | tf_op jit(solution)/shard_map/dot_general | solution.py:524
  158.7 14.4 %collective-permute-done.32 = bf16[2048,256]{1,0:T(8,128)(2,1)S(1)} collective-permute-done((bf16[2048,256]{1,0:T(8,128)(2,1)S(1)}, bf16[2048,256]{1,0:T(8,128)(2,1)S(1)}, u32[]{:S(2)}, u32[]{:S(2)}) %collective-permute-start.32) | collective-permute-done | bytes 1048608 | tf_op jit(solution)/shard_map/ppermute | solution.py:382
  173.0 1.1 broadcast_select_fusion.2
  174.2 1.3 collective-permute-start.38
  175.5 1.3 shard_map.207
  177.3 4.3 %fusion.25 = bf16[768,512]{1,0:T(8,128)(2,1)S(1)} fusion(bf16[768,2048]{1,0:T(8,128)(2,1)} %copy-done.19, bf16[2048,256]{1,0:T(8,128)(2,1)} %collective-permute-done.34, bf16[2048,256]{1,0:T(8,128)(2,1)} %broadcast_select_fusion.2), kind=kOutput, calls=%fused_computation.22 | convolution fusion | flops 1615200256 | bytes 6029312 | tf_op jit(solution)/shard_map/dot_general | solution.py:524
  181.5 20.4 %collective-permute-done.38 = bf16[2048,256]{1,0:T(8,128)(2,1)} collective-permute-done((bf16[2048,256]{1,0:T(8,128)(2,1)}, bf16[2048,256]{1,0:T(8,128)(2,1)}, u32[]{:S(2)}, u32[]{:S(2)}) %collective-permute-start.38) | collective-permute-done | bytes 1048608 | tf_op jit(solution)/shard_map/ppermute | solution.py:382
  202.8 2.3 collective-permute-start.28
  207.1 1.3 broadcast_select_fusion.1
  208.4 2.3 collective-permute-start.35
  211.4 1.8 fusion.22
  213.3 2.5 %collective-permute-done.28.refs_1_ = bf16[192,1024]{1,0:T(8,128)(2,1)S(1)} collective-permute-done((bf16[192,1024]{1,0:T(8,128)(2,1)S(1)}, bf16[192,1024]{1,0:T(8,128)(2,1)S(1)}, u32[]{:S(2)}, u32[]{:S(2)}) %collective-permute-start.28) | collective-permute-done | bytes 393248 | tf_op jit(solution)/shard_map/ppermute | solution.py:382
  215.8 1.3 collective-permute-start.37
  217.1 7.0 %collective-permute-done.29.refs_2_ = bf16[192,1024]{1,0:T(8,128)(2,1)S(1)} collective-permute-done((bf16[192,1024]{1,0:T(8,128)(2,1)S(1)}, bf16[192,1024]{1,0:T(8,128)(2,1)S(1)}, u32[]{:S(2)}, u32[]{:S(2)}) %collective-permute-start.29) | collective-permute-done | bytes 393248 | tf_op jit(solution)/shard_map/ppermute | solution.py:382
  224.1 1.6 collective-permute-start.41
  226.2 2.2 collective-permute-done.35.refs_5_
  228.5 1.3 collective-permute-start.43
  230.3 2.2 collective-permute-done.36.refs_6_
  233.4 3.2 %shard_map.206 = bf16[192,2048]{1,0:T(8,128)(2,1)} custom-call(s32[8]{0:T(128)} %broadcast_multiply_fusion.at, bf16[192,2048]{1,0:T(8,128)(2,1)} %get-tuple-element.39.middle, bf16[192,1024]{1,0:T(8,128)(2,1)} %get-tuple-element.54.refs_0_, bf16[192,1024]{1,0:T(8,128)(2,1)} %copy-done.2, bf16[192,1024]{1,0:T(8,128)(2,1)} %copy-done.3, ...), custom_call_target="tpu_custom_call" | custom-call | flops 393216 | bytes 3145728 | tf_op jit(solution)/shard_map/pallas_call | solution.py:546
  236.9 3.6 %collective-permute-done.42 = bf16[192,512]{1,0:T(8,128)(2,1)S(1)} collective-permute-done((bf16[192,512]{1,0:T(8,128)(2,1)S(1)}, bf16[192,512]{1,0:T(8,128)(2,1)S(1)}, u32[]{:S(2)}, u32[]{:S(2)}) %collective-permute-start.42) | collective-permute-done | bytes 196640 | tf_op jit(solution)/shard_map/ppermute | solution.py:382
  240.7 1.0 convert_add_fusion
  241.7 1.7 fusion.30
  (102 shorter events, 17.1 us)
Async XLA Ops:
  0.0 7.5 %collective-permute-start.14 = (bf16[256,2048]{1,0:T(8,128)(2,1)}, bf16[256,2048]{1,0:T(8,128)(2,1)S(1)}, u32[]{:S(2)}, u32[]{:S(2)}) collective-permute-start(bf16[256,2048]{1,0:T(8,128)(2,1)} %param.35), channel_id=1, source_target_pairs={{1,4},{3,6},{4,1},{6,3},{9,12},{11,14},{12,9},{14,11},{17,20},{19,... | collective-permute-start | bytes 3145736 | tf_op jit(solution)/shard_map/ppermute | solution.py:382
  4.5 52.6 %collective-permute-start.8 = (bf16[256,2048]{1,0:T(8,128)(2,1)}, bf16[256,2048]{1,0:T(8,128)(2,1)}, u32[]{:S(2)}, u32[]{:S(2)}) collective-permute-start(bf16[256,2048]{1,0:T(8,128)(2,1)} %constant_dynamic-update-slice_fusion), channel_id=1, source_target_pairs={{0,2},{1,3},{2,0},{3,1},{4,6},{5,7},{6,4},{7,5},{8,10},{9,11},{10,... | collective-permute-start | bytes 3145736 | tf_op jit(solution)/shard_map/ppermute | solution.py:382
  7.5 53.1 %copy-start.15 = (bf16[2048]{0:T(1024)(128)(2,1)S(1)}, bf16[2048]{0:T(1024)(128)(2,1)}, u32[]{:S(2)}) copy-start(bf16[2048]{0:T(1024)(128)(2,1)} %param.34) | copy-start | bytes 12292
  7.5 53.7 %copy-start = (bf16[2048,256]{1,0:T(8,128)(2,1)S(1)}, bf16[2048,256]{1,0:T(8,128)(2,1)}, u32[]{:S(2)}) copy-start(bf16[2048,256]{1,0:T(8,128)(2,1)} %param.36) | copy-start | bytes 3145732
  8.9 61.8 %copy-start.1 = (bf16[256,2048]{1,0:T(8,128)(2,1)}, bf16[256,2048]{1,0:T(8,128)(2,1)S(1)}, u32[]{:S(2)}) copy-start(bf16[256,2048]{1,0:T(8,128)(2,1)S(1)} %broadcast_select_fusion.6.refs_5_) | copy-start | bytes 3145732
  8.9 48.7 %collective-permute-start.16 = (bf16[256,2048]{1,0:T(8,128)(2,1)S(1)}, bf16[256,2048]{1,0:T(8,128)(2,1)}, u32[]{:S(2)}, u32[]{:S(2)}) collective-permute-start(bf16[256,2048]{1,0:T(8,128)(2,1)S(1)} %broadcast_select_fusion.6.refs_5_), channel_id=1, source_target_pairs={{0,8},{4,12},{8,0},{12,4},{16,24},{20,28},{24,16},{28,20},{1,9},{5... | collective-permute-start | bytes 3145736 | tf_op jit(solution)/shard_map/ppermute | solution.py:382
  10.6 47.1 %collective-permute-start.18 = (bf16[256,2048]{1,0:T(8,128)(2,1)S(1)}, bf16[256,2048]{1,0:T(8,128)(2,1)S(1)}, u32[]{:S(2)}, u32[]{:S(2)}) collective-permute-start(bf16[256,2048]{1,0:T(8,128)(2,1)S(1)} %broadcast_select_fusion.6.refs_5_), channel_id=1, source_target_pairs={{8,16},{12,20},{16,8},{20,12},{9,17},{13,21},{17,9},{21,13},{10,18... | collective-permute-start | bytes 3145736 | tf_op jit(solution)/shard_map/ppermute | solution.py:382
  15.9 13.0 %collective-permute-start = (bf16[208,128]{1,0:T(8,128)(2,1)}, bf16[208,128]{1,0:T(8,128)(2,1)S(1)}, u32[]{:S(2)}, u32[]{:S(2)}) collective-permute-start(bf16[208,128]{1,0:T(8,128)(2,1)} %get-tuple-element.28.own), channel_id=1, source_target_pairs={{0,4},{4,0},{8,12},{12,8},{16,20},{20,16},{24,28},{28,24},{1,5},{5... | collective-permute-start | bytes 159752 | tf_op jit(solution)/shard_map/ppermute | solution.py:382
  28.9 0.6 copy-start.5
  31.0 8.3 %collective-permute-start.1 = (bf16[208,128]{1,0:T(8,128)(2,1)}, bf16[208,128]{1,0:T(8,128)(2,1)S(1)}, u32[]{:S(2)}, u32[]{:S(2)}) collective-permute-start(bf16[208,128]{1,0:T(8,128)(2,1)} %shard_map.201), channel_id=1, source_target_pairs={{0,8},{4,12},{8,16},{12,20},{16,24},{20,28},{1,9},{5,13},{9,17},{1... | collective-permute-start | bytes 159752 | tf_op jit(solution)/shard_map/ppermute | solution.py:382
  37.1 10.2 %collective-permute-start.2 = (bf16[208,128]{1,0:T(8,128)(2,1)}, bf16[208,128]{1,0:T(8,128)(2,1)S(1)}, u32[]{:S(2)}, u32[]{:S(2)}) collective-permute-start(bf16[208,128]{1,0:T(8,128)(2,1)} %shard_map.201), channel_id=1, source_target_pairs={{0,16},{4,20},{8,24},{12,28},{1,17},{5,21},{9,25},{13,29},{2,18},{... | collective-permute-start | bytes 159752 | tf_op jit(solution)/shard_map/ppermute | solution.py:382
  39.3 8.0 %copy-start.12 = (bf16[208,128]{1,0:T(8,128)(2,1)}, bf16[208,128]{1,0:T(8,128)(2,1)S(1)}, u32[]{:S(2)}) copy-start(bf16[208,128]{1,0:T(8,128)(2,1)S(1)} %collective-permute-done.1.refs_0_) | copy-start | bytes 159748
  39.3 8.0 %collective-permute-start.3 = (bf16[208,128]{1,0:T(8,128)(2,1)}, bf16[208,128]{1,0:T(8,128)(2,1)S(1)}, u32[]{:S(2)}, u32[]{:S(2)}) collective-permute-start(bf16[208,128]{1,0:T(8,128)(2,1)} %shard_map.201), channel_id=1, source_target_pairs={{0,24},{4,28},{1,25},{5,29},{2,26},{6,30},{3,27},{7,31}} | collective-permute-start | bytes 159752 | tf_op jit(solution)/shard_map/ppermute | solution.py:382
  47.3 0.6 copy-start.14
  51.1 1.6 collective-permute-start.4
  51.1 5.9 %collective-permute-start.5 = (bf16[192,256]{1,0:T(8,128)(2,1)}, bf16[192,256]{1,0:T(8,128)(2,1)S(1)}, u32[]{:S(2)}, u32[]{:S(2)}) collective-permute-start(bf16[192,256]{1,0:T(8,128)(2,1)} %get-tuple-element.37), channel_id=1, source_target_pairs={{0,2},{1,3},{2,0},{3,1},{4,6},{5,7},{6,4},{7,5},{8,10},{9,11},{10,... | collective-permute-start | bytes 294920 | tf_op jit(solution)/shard_map/ppermute | solution.py:382
  52.7 13.0 %copy-start.9 = (bf16[192,256]{1,0:T(8,128)(2,1)}, bf16[192,256]{1,0:T(8,128)(2,1)S(1)}, u32[]{:S(2)}) copy-start(bf16[192,256]{1,0:T(8,128)(2,1)S(1)} %collective-permute-done.4.refs_1_) | copy-start | bytes 294916
  52.7 6.3 %collective-permute-start.6 = (bf16[192,256]{1,0:T(8,128)(2,1)}, bf16[192,256]{1,0:T(8,128)(2,1)S(1)}, u32[]{:S(2)}, u32[]{:S(2)}) collective-permute-start(bf16[192,256]{1,0:T(8,128)(2,1)} %get-tuple-element.38), channel_id=1, source_target_pairs={{0,3},{1,2},{2,1},{3,0},{4,7},{5,6},{6,5},{7,4},{8,11},{9,10},{10,... | collective-permute-start | bytes 294920 | tf_op jit(solution)/shard_map/ppermute | solution.py:382
  57.1 8.6 %copy-start.10 = (bf16[192,256]{1,0:T(8,128)(2,1)}, bf16[192,256]{1,0:T(8,128)(2,1)S(1)}, u32[]{:S(2)}) copy-start(bf16[192,256]{1,0:T(8,128)(2,1)S(1)} %collective-permute-done.5.refs_2_) | copy-start | bytes 294916
  57.1 4.1 %collective-permute-start.7 = (bf16[256,2048]{1,0:T(8,128)(2,1)}, bf16[256,2048]{1,0:T(8,128)(2,1)}, u32[]{:S(2)}, u32[]{:S(2)}) collective-permute-start(bf16[256,2048]{1,0:T(8,128)(2,1)} %constant_dynamic-update-slice_fusion), channel_id=1, source_target_pairs={{0,1},{1,0},{2,3},{3,2},{4,5},{5,4},{6,7},{7,6},{8,9},{9,8},{10,11... | collective-permute-start | bytes 3145736 | tf_op jit(solution)/shard_map/ppermute | solution.py:382
  57.1 5.8 %collective-permute-start.9 = (bf16[256,2048]{1,0:T(8,128)(2,1)}, bf16[256,2048]{1,0:T(8,128)(2,1)}, u32[]{:S(2)}, u32[]{:S(2)}) collective-permute-start(bf16[256,2048]{1,0:T(8,128)(2,1)} %collective-permute-done.8.refs_5_), channel_id=1, source_target_pairs={{0,1},{1,0},{2,3},{3,2},{4,5},{5,4},{6,7},{7,6},{8,9},{9,8},{10,11... | collective-permute-start | bytes 3145736 | tf_op jit(solution)/shard_map/ppermute | solution.py:382
  57.6 13.1 %collective-permute-start.17 = (bf16[256,2048]{1,0:T(8,128)(2,1)}, bf16[256,2048]{1,0:T(8,128)(2,1)}, u32[]{:S(2)}, u32[]{:S(2)}) collective-permute-start(bf16[256,2048]{1,0:T(8,128)(2,1)} %collective-permute-done.16.refs_7_), channel_id=1, source_target_pairs={{0,1},{1,0},{2,3},{3,2},{4,5},{5,4},{6,7},{7,6},{8,9},{9,8},{10,11... | collective-permute-start | bytes 3145736 | tf_op jit(solution)/shard_map/ppermute | solution.py:382
  57.7 27.5 %collective-permute-start.19 = (bf16[256,2048]{1,0:T(8,128)(2,1)S(1)}, bf16[256,2048]{1,0:T(8,128)(2,1)}, u32[]{:S(2)}, u32[]{:S(2)}) collective-permute-start(bf16[256,2048]{1,0:T(8,128)(2,1)S(1)} %collective-permute-done.18), channel_id=1, source_target_pairs={{8,0},{12,4},{16,24},{20,28},{9,1},{13,5},{17,25},{21,29},{10,2},{... | collective-permute-start | bytes 3145736 | tf_op jit(solution)/shard_map/ppermute | solution.py:382
  59.0 6.7 %copy-start.11 = (bf16[192,256]{1,0:T(8,128)(2,1)}, bf16[192,256]{1,0:T(8,128)(2,1)S(1)}, u32[]{:S(2)}) copy-start(bf16[192,256]{1,0:T(8,128)(2,1)S(1)} %collective-permute-done.6.refs_3_) | copy-start | bytes 294916
  59.0 28.6 %collective-permute-start.20 = (bf16[256,2048]{1,0:T(8,128)(2,1)}, bf16[256,2048]{1,0:T(8,128)(2,1)}, u32[]{:S(2)}, u32[]{:S(2)}) collective-permute-start(bf16[256,2048]{1,0:T(8,128)(2,1)} %collective-permute-done.16.refs_7_), channel_id=1, source_target_pairs={{8,16},{12,20},{16,8},{20,12},{9,17},{13,21},{17,9},{21,13},{10,18... | collective-permute-start | bytes 3145736 | tf_op jit(solution)/shard_map/ppermute | solution.py:382
  61.2 46.7 %collective-permute-start.24 = (bf16[2048,256]{1,0:T(8,128)(2,1)S(1)}, bf16[2048,256]{1,0:T(8,128)(2,1)}, u32[]{:S(2)}, u32[]{:S(2)}) collective-permute-start(bf16[2048,256]{1,0:T(8,128)(2,1)S(1)} %copy-done), channel_id=1, source_target_pairs={{1,4},{3,6},{4,1},{6,3},{9,12},{11,14},{12,9},{14,11},{17,20},{19,... | collective-permute-start | bytes 3145736 | tf_op jit(solution)/shard_map/ppermute | solution.py:382
  62.8 47.7 %collective-permute-start.15 = (bf16[256,2048]{1,0:T(8,128)(2,1)S(1)}, bf16[256,2048]{1,0:T(8,128)(2,1)}, u32[]{:S(2)}, u32[]{:S(2)}) collective-permute-start(bf16[256,2048]{1,0:T(8,128)(2,1)S(1)} %broadcast_select_fusion.6.refs_5_), channel_id=1, source_target_pairs={{0,1},{1,0},{2,3},{3,2},{4,5},{5,4},{6,7},{7,6},{8,9},{9,8},{10,11... | collective-permute-start | bytes 3145736 | tf_op jit(solution)/shard_map/ppermute | solution.py:382
  70.7 19.9 %collective-permute-start.10 = (bf16[192,2048]{1,0:T(8,128)(2,1)}, bf16[192,2048]{1,0:T(8,128)(2,1)}, u32[]{:S(2)}, u32[]{:S(2)}) collective-permute-start(bf16[192,2048]{1,0:T(8,128)(2,1)} %get-tuple-element.40.refs_0_), channel_id=1, source_target_pairs={{0,2},{1,3},{2,0},{3,1},{4,6},{5,7},{6,4},{7,5},{8,10},{9,11},{10,... | collective-permute-start | bytes 2359304 | tf_op jit(solution)/shard_map/ppermute | solution.py:382
  85.2 20.0 %collective-permute-start.11 = (bf16[192,2048]{1,0:T(8,128)(2,1)}, bf16[192,2048]{1,0:T(8,128)(2,1)}, u32[]{:S(2)}, u32[]{:S(2)}) collective-permute-start(bf16[192,2048]{1,0:T(8,128)(2,1)} %get-tuple-element.41), channel_id=1, source_target_pairs={{0,4},{4,0},{8,12},{12,8},{16,20},{20,16},{24,28},{28,24},{1,5},{5... | collective-permute-start | bytes 2359304 | tf_op jit(solution)/shard_map/ppermute | solution.py:382
  89.8 28.4 %collective-permute-start.21 = (bf16[256,2048]{1,0:T(8,128)(2,1)}, bf16[256,2048]{1,0:T(8,128)(2,1)}, u32[]{:S(2)}, u32[]{:S(2)}) collective-permute-start(bf16[256,2048]{1,0:T(8,128)(2,1)} %broadcast_select_fusion.5.refs_9_), channel_id=1, source_target_pairs={{0,1},{1,0},{2,3},{3,2},{4,5},{5,4},{6,7},{7,6},{8,9},{9,8},{10,11... | collective-permute-start | bytes 3145736 | tf_op jit(solution)/shard_map/ppermute | solution.py:382
  90.6 38.9 %collective-permute-start.22 = (bf16[256,2048]{1,0:T(8,128)(2,1)}, bf16[256,2048]{1,0:T(8,128)(2,1)}, u32[]{:S(2)}, u32[]{:S(2)}) collective-permute-start(bf16[256,2048]{1,0:T(8,128)(2,1)} %collective-permute-done.20), channel_id=1, source_target_pairs={{8,0},{12,4},{16,24},{20,28},{9,1},{13,5},{17,25},{21,29},{10,2},{... | collective-permute-start | bytes 3145736 | tf_op jit(solution)/shard_map/ppermute | solution.py:382
  105.1 10.0 %collective-permute-start.12 = (bf16[96,2048]{1,0:T(8,128)(2,1)S(1)}, bf16[96,2048]{1,0:T(8,128)(2,1)S(1)}, u32[]{:S(2)}, u32[]{:S(2)}) collective-permute-start(bf16[96,2048]{1,0:T(8,128)(2,1)S(1)} %slice.74), channel_id=1, source_target_pairs={{0,4},{4,0},{8,12},{12,8},{16,20},{20,16},{24,28},{28,24},{1,5},{5... | collective-permute-start | bytes 1179656 | tf_op jit(solution)/shard_map/ppermute | solution.py:382
  107.9 9.5 %collective-permute-start.13 = (bf16[96,2048]{1,0:T(8,128)(2,1)S(1)}, bf16[96,2048]{1,0:T(8,128)(2,1)S(1)}, u32[]{:S(2)}, u32[]{:S(2)}) collective-permute-start(bf16[96,2048]{1,0:T(8,128)(2,1)S(1)} %slice.75), channel_id=1, source_target_pairs={{0,2},{1,3},{2,0},{3,1},{4,6},{5,7},{6,4},{7,5},{8,10},{9,11},{10,... | collective-permute-start | bytes 1179656 | tf_op jit(solution)/shard_map/ppermute | solution.py:382
  110.6 30.7 %collective-permute-start.26 = (bf16[2048,256]{1,0:T(8,128)(2,1)}, bf16[2048,256]{1,0:T(8,128)(2,1)}, u32[]{:S(2)}, u32[]{:S(2)}) collective-permute-start(bf16[2048,256]{1,0:T(8,128)(2,1)} %broadcast_select_fusion.3), channel_id=1, source_target_pairs={{0,8},{4,12},{8,0},{12,4},{16,24},{20,28},{24,16},{28,20},{1,9},{5... | collective-permute-start | bytes 3145736 | tf_op jit(solution)/shard_map/ppermute | solution.py:382
  115.2 3.0 %copy-start.17 = (bf16[96,2048]{1,0:T(8,128)(2,1)}, bf16[96,2048]{1,0:T(8,128)(2,1)S(1)}, u32[]{:S(2)}) copy-start(bf16[96,2048]{1,0:T(8,128)(2,1)S(1)} %collective-permute-done.12.refs_3_) | copy-start | bytes 1179652
  115.2 30.4 %collective-permute-start.31 = (bf16[2048,256]{1,0:T(8,128)(2,1)}, bf16[2048,256]{1,0:T(8,128)(2,1)S(1)}, u32[]{:S(2)}, u32[]{:S(2)}) collective-permute-start(bf16[2048,256]{1,0:T(8,128)(2,1)} %broadcast_select_fusion.3), channel_id=1, source_target_pairs={{8,16},{12,20},{16,8},{20,12},{9,17},{13,21},{17,9},{21,13},{10,18... | collective-permute-start | bytes 3145736 | tf_op jit(solution)/shard_map/ppermute | solution.py:382
  117.4 0.8 copy-start.18
  130.8 16.2 %collective-permute-start.23 = (bf16[256,2048]{1,0:T(8,128)(2,1)S(1)}, bf16[256,2048]{1,0:T(8,128)(2,1)S(1)}, u32[]{:S(2)}, u32[]{:S(2)}) collective-permute-start(bf16[256,2048]{1,0:T(8,128)(2,1)S(1)} %broadcast_select_fusion.4), channel_id=1, source_target_pairs={{0,1},{1,0},{2,3},{3,2},{4,5},{5,4},{6,7},{7,6},{8,9},{9,8},{10,11... | collective-permute-start | bytes 3145736 | tf_op jit(solution)/shard_map/ppermute | solution.py:382
  130.9 21.0 %collective-permute-start.25 = (bf16[2048,256]{1,0:T(8,128)(2,1)}, bf16[2048,256]{1,0:T(8,128)(2,1)}, u32[]{:S(2)}, u32[]{:S(2)}) collective-permute-start(bf16[2048,256]{1,0:T(8,128)(2,1)} %broadcast_select_fusion.3), channel_id=1, source_target_pairs={{0,1},{1,0},{2,3},{3,2},{4,5},{5,4},{6,7},{7,6},{8,9},{9,8},{10,11... | collective-permute-start | bytes 3145736 | tf_op jit(solution)/shard_map/ppermute | solution.py:382
  141.3 10.6 %collective-permute-start.27 = (bf16[2048,256]{1,0:T(8,128)(2,1)}, bf16[2048,256]{1,0:T(8,128)(2,1)}, u32[]{:S(2)}, u32[]{:S(2)}) collective-permute-start(bf16[2048,256]{1,0:T(8,128)(2,1)} %collective-permute-done.26), channel_id=1, source_target_pairs={{0,1},{1,0},{2,3},{3,2},{4,5},{5,4},{6,7},{7,6},{8,9},{9,8},{10,11... | collective-permute-start | bytes 3145736 | tf_op jit(solution)/shard_map/ppermute | solution.py:382
  143.9 29.1 %collective-permute-start.33 = (bf16[2048,256]{1,0:T(8,128)(2,1)}, bf16[2048,256]{1,0:T(8,128)(2,1)}, u32[]{:S(2)}, u32[]{:S(2)}) collective-permute-start(bf16[2048,256]{1,0:T(8,128)(2,1)} %collective-permute-done.26), channel_id=1, source_target_pairs={{8,16},{12,20},{16,8},{20,12},{9,17},{13,21},{17,9},{21,13},{10,18... | collective-permute-start | bytes 3145736 | tf_op jit(solution)/shard_map/ppermute | solution.py:382
  145.6 27.5 %collective-permute-start.32 = (bf16[2048,256]{1,0:T(8,128)(2,1)S(1)}, bf16[2048,256]{1,0:T(8,128)(2,1)S(1)}, u32[]{:S(2)}, u32[]{:S(2)}) collective-permute-start(bf16[2048,256]{1,0:T(8,128)(2,1)S(1)} %collective-permute-done.31), channel_id=1, source_target_pairs={{8,0},{12,4},{16,24},{20,28},{9,1},{13,5},{17,25},{21,29},{10,2},{... | collective-permute-start | bytes 3145736 | tf_op jit(solution)/shard_map/ppermute | solution.py:382
  151.9 6.8 %copy-start.19 = (bf16[768,2048]{1,0:T(8,128)(2,1)}, bf16[768,2048]{1,0:T(8,128)(2,1)S(1)}, u32[]{:S(2)}) copy-start(bf16[768,2048]{1,0:T(8,128)(2,1)S(1)} %multiply_convert_fusion) | copy-start | bytes 9437188
  174.2 3.1 %collective-permute-start.34 = (bf16[2048,256]{1,0:T(8,128)(2,1)}, bf16[2048,256]{1,0:T(8,128)(2,1)}, u32[]{:S(2)}, u32[]{:S(2)}) collective-permute-start(bf16[2048,256]{1,0:T(8,128)(2,1)} %broadcast_select_fusion.2), channel_id=1, source_target_pairs={{0,1},{1,0},{2,3},{3,2},{4,5},{5,4},{6,7},{7,6},{8,9},{9,8},{10,11... | collective-permute-start | bytes 3145736 | tf_op jit(solution)/shard_map/ppermute | solution.py:382
  174.2 27.8 %collective-permute-start.38 = (bf16[2048,256]{1,0:T(8,128)(2,1)}, bf16[2048,256]{1,0:T(8,128)(2,1)}, u32[]{:S(2)}, u32[]{:S(2)}) collective-permute-start(bf16[2048,256]{1,0:T(8,128)(2,1)} %collective-permute-done.33), channel_id=1, source_target_pairs={{8,0},{12,4},{16,24},{20,28},{9,1},{13,5},{17,25},{21,29},{10,2},{... | collective-permute-start | bytes 3145736 | tf_op jit(solution)/shard_map/ppermute | solution.py:382
  176.7 31.7 %collective-permute-start.40 = (bf16[2048,256]{1,0:T(8,128)(2,1)S(1)}, bf16[2048,256]{1,0:T(8,128)(2,1)S(1)}, u32[]{:S(2)}, u32[]{:S(2)}) collective-permute-start(bf16[2048,256]{1,0:T(8,128)(2,1)S(1)} %collective-permute-done.31), channel_id=1, source_target_pairs={{0,1},{1,0},{2,3},{3,2},{4,5},{5,4},{6,7},{7,6},{8,9},{9,8},{10,11... | collective-permute-start | bytes 3145736 | tf_op jit(solution)/shard_map/ppermute | solution.py:382
  201.9 8.8 %collective-permute-start.39 = (bf16[2048,256]{1,0:T(8,128)(2,1)}, bf16[2048,256]{1,0:T(8,128)(2,1)S(1)}, u32[]{:S(2)}, u32[]{:S(2)}) collective-permute-start(bf16[2048,256]{1,0:T(8,128)(2,1)} %collective-permute-done.38), channel_id=1, source_target_pairs={{0,1},{1,0},{2,3},{3,2},{4,5},{5,4},{6,7},{7,6},{8,9},{9,8},{10,11... | collective-permute-start | bytes 3145736 | tf_op jit(solution)/shard_map/ppermute | solution.py:382
  202.8 8.6 %copy-start.20 = (bf16[768,2048]{1,0:T(8,128)(2,1)S(1)}, bf16[768,2048]{1,0:T(8,128)(2,1)}, u32[]{:S(2)}) copy-start(bf16[768,2048]{1,0:T(8,128)(2,1)} %copy-done.19) | copy-start | bytes 9437188
  202.8 12.9 %collective-permute-start.28 = (bf16[192,1024]{1,0:T(8,128)(2,1)S(1)}, bf16[192,1024]{1,0:T(8,128)(2,1)S(1)}, u32[]{:S(2)}, u32[]{:S(2)}) collective-permute-start(bf16[192,1024]{1,0:T(8,128)(2,1)S(1)} %get-tuple-element.53), channel_id=1, source_target_pairs={{0,6},{1,7},{2,4},{3,5},{4,2},{5,3},{6,0},{7,1},{8,14},{9,15},{10,... | collective-permute-start | bytes 1179656 | tf_op jit(solution)/shard_map/ppermute | solution.py:382
  205.1 19.0 %collective-permute-start.29 = (bf16[192,1024]{1,0:T(8,128)(2,1)S(1)}, bf16[192,1024]{1,0:T(8,128)(2,1)S(1)}, u32[]{:S(2)}, u32[]{:S(2)}) collective-permute-start(bf16[192,1024]{1,0:T(8,128)(2,1)S(1)} %get-tuple-element.52), channel_id=1, source_target_pairs={{0,2},{1,3},{2,0},{3,1},{4,6},{5,7},{6,4},{7,5},{8,10},{9,11},{10,... | collective-permute-start | bytes 1179656 | tf_op jit(solution)/shard_map/ppermute | solution.py:382
  205.7 20.1 %collective-permute-start.30 = (bf16[192,1024]{1,0:T(8,128)(2,1)S(1)}, bf16[192,1024]{1,0:T(8,128)(2,1)S(1)}, u32[]{:S(2)}, u32[]{:S(2)}) collective-permute-start(bf16[192,1024]{1,0:T(8,128)(2,1)S(1)} %get-tuple-element.51), channel_id=1, source_target_pairs={{0,4},{4,0},{8,12},{12,8},{16,20},{20,16},{24,28},{28,24},{1,5},{5... | collective-permute-start | bytes 1179656 | tf_op jit(solution)/shard_map/ppermute | solution.py:382
  208.4 20.0 %collective-permute-start.35 = (bf16[192,512]{1,0:T(8,128)(2,1)S(1)}, bf16[192,512]{1,0:T(8,128)(2,1)S(1)}, u32[]{:S(2)}, u32[]{:S(2)}) collective-permute-start(bf16[192,512]{1,0:T(8,128)(2,1)S(1)} %get-tuple-element.62), channel_id=1, source_target_pairs={{0,6},{1,7},{2,4},{3,5},{4,2},{5,3},{6,0},{7,1},{8,14},{9,15},{10,... | collective-permute-start | bytes 589832 | tf_op jit(solution)/shard_map/ppermute | solution.py:382
  210.8 21.8 %collective-permute-start.36 = (bf16[192,512]{1,0:T(8,128)(2,1)S(1)}, bf16[192,512]{1,0:T(8,128)(2,1)S(1)}, u32[]{:S(2)}, u32[]{:S(2)}) collective-permute-start(bf16[192,512]{1,0:T(8,128)(2,1)S(1)} %get-tuple-element.61), channel_id=1, source_target_pairs={{0,2},{1,3},{2,0},{3,1},{4,6},{5,7},{6,4},{7,5},{8,10},{9,11},{10,... | collective-permute-start | bytes 589832 | tf_op jit(solution)/shard_map/ppermute | solution.py:382
  211.4 18.4 %copy-start.16 = (s32[8]{0:T(128)S(1)}, s32[8]{0:T(128)}, u32[]{:S(2)}) copy-start(s32[8]{0:T(128)} %stack.53.at) | copy-start | bytes 100
  215.8 16.9 %copy-start.2 = (bf16[192,1024]{1,0:T(8,128)(2,1)}, bf16[192,1024]{1,0:T(8,128)(2,1)S(1)}, u32[]{:S(2)}) copy-start(bf16[192,1024]{1,0:T(8,128)(2,1)S(1)} %collective-permute-done.28.refs_1_) | copy-start | bytes 1179652
  215.8 16.9 %collective-permute-start.37 = (bf16[192,512]{1,0:T(8,128)(2,1)S(1)}, bf16[192,512]{1,0:T(8,128)(2,1)S(1)}, u32[]{:S(2)}, u32[]{:S(2)}) collective-permute-start(bf16[192,512]{1,0:T(8,128)(2,1)S(1)} %get-tuple-element.60), channel_id=1, source_target_pairs={{0,4},{4,0},{8,12},{12,8},{16,20},{20,16},{24,28},{28,24},{1,5},{5... | collective-permute-start | bytes 589832 | tf_op jit(solution)/shard_map/ppermute | solution.py:382
  224.1 8.6 %copy-start.3 = (bf16[192,1024]{1,0:T(8,128)(2,1)}, bf16[192,1024]{1,0:T(8,128)(2,1)S(1)}, u32[]{:S(2)}) copy-start(bf16[192,1024]{1,0:T(8,128)(2,1)S(1)} %collective-permute-done.29.refs_2_) | copy-start | bytes 1179652
  224.1 12.8 %collective-permute-start.41 = (bf16[192,512]{1,0:T(8,128)(2,1)S(1)}, bf16[192,512]{1,0:T(8,128)(2,1)S(1)}, u32[]{:S(2)}, u32[]{:S(2)}) collective-permute-start(bf16[192,512]{1,0:T(8,128)(2,1)S(1)} %get-tuple-element.55), channel_id=1, source_target_pairs={{0,6},{1,7},{2,4},{3,5},{4,2},{5,3},{6,0},{7,1},{8,14},{9,15},{10,... | collective-permute-start | bytes 589832 | tf_op jit(solution)/shard_map/ppermute | solution.py:382
  225.7 7.0 %copy-start.4 = (bf16[192,1024]{1,0:T(8,128)(2,1)}, bf16[192,1024]{1,0:T(8,128)(2,1)S(1)}, u32[]{:S(2)}) copy-start(bf16[192,1024]{1,0:T(8,128)(2,1)S(1)} %collective-permute-done.30.refs_3_) | copy-start | bytes 1179652
  225.7 14.8 %collective-permute-start.42 = (bf16[192,512]{1,0:T(8,128)(2,1)S(1)}, bf16[192,512]{1,0:T(8,128)(2,1)S(1)}, u32[]{:S(2)}, u32[]{:S(2)}) collective-permute-start(bf16[192,512]{1,0:T(8,128)(2,1)S(1)} %get-tuple-element.57), channel_id=1, source_target_pairs={{0,2},{1,3},{2,0},{3,1},{4,6},{5,7},{6,4},{7,5},{8,10},{9,11},{10,... | collective-permute-start | bytes 589832 | tf_op jit(solution)/shard_map/ppermute | solution.py:382
  228.5 4.2 %copy-start.6 = (bf16[192,512]{1,0:T(8,128)(2,1)}, bf16[192,512]{1,0:T(8,128)(2,1)S(1)}, u32[]{:S(2)}) copy-start(bf16[192,512]{1,0:T(8,128)(2,1)S(1)} %collective-permute-done.35.refs_5_) | copy-start | bytes 589828
  228.5 12.2 %collective-permute-start.43 = (bf16[192,512]{1,0:T(8,128)(2,1)S(1)}, bf16[192,512]{1,0:T(8,128)(2,1)}, u32[]{:S(2)}, u32[]{:S(2)}) collective-permute-start(bf16[192,512]{1,0:T(8,128)(2,1)S(1)} %get-tuple-element.56), channel_id=1, source_target_pairs={{0,4},{4,0},{8,12},{12,8},{16,20},{20,16},{24,28},{28,24},{1,5},{5... | collective-permute-start | bytes 589832 | tf_op jit(solution)/shard_map/ppermute | solution.py:382
  232.6 0.7 copy-start.7
  232.7 0.7 copy-start.8
  (1 other events, 0.6 us)

commit v3 on v2

--- a/solution.py
+++ b/solution.py
@@ -477,8 +477,11 @@
     def by_y(array):
         return exchange(array, "sp", sp, lambda i: i ^ 1)
 
-    def both_cores(slot):
-        return [slot, exchange(slot, "tp", tp, lambda i: i ^ 1)]
+    def both_cores(slot, planes=range(4)):
+        def move(i):
+            return i ^ 1 if i // tp // 2 in planes else None
+
+        return [slot, exchange(slot, ("sp", "tp"), sp * tp, move)]
 
     slots = [z, z ^ 1, (z + 2) % 4, (z ^ 1) ^ 2]
     order = jnp.stack([s * 2 + c for s in slots for c in (core, 1 - core)]).astype(jnp.int32)
@@ -539,8 +542,8 @@
     down_far = jnp.where(at_end, tie(down_out, parts[0], wait), down_in)
     sums += down(1, both_cores(down_far))
     pause = hold(stream_in[:16, :128])
-    ends_final = both_cores(tie(down_last, parts[1], pause))
-    middles_final = both_cores(down_cross)
+    ends_final = both_cores(tie(down_last, parts[1], pause), (0, 3))
+    middles_final = both_cores(down_cross, (1, 2))
     sums += down(2, [jnp.where(at_end, a, b) for a, b in zip(ends_final, middles_final)])
     units = 2 * order
     out = scalar_call(

time: 245 us -> 246 us (level)
  transfers between devices with their start and end apart: 44 -> 44, of which waited for: 19 -> 19; matrix products, arithmetic and copies ran while one was open for 16% -> 15% of each run, Pallas kernels for 14% -> 14%
where the time goes in v3:
time: 246 us; the launch traced here: 245 us
  waiting for transfers between devices  99.7 us (41%)
  starting transfers between devices  65.9 us (27%)
  Pallas kernels  34.9 us (14%)
  matrix products  17.6 us (7%)
  local copies, waits for them, and re-layouts  14.8 us (6%)
  other arithmetic  12 us (5%)
    ppermute x44, waiting for transfers between devices, exchange(): lax.ppermute(array, axis, [(i, j) for i, j in pairs if j is not None and...  99.7 us
    ppermute x44, starting transfers between devices, exchange(): lax.ppermute(array, axis, [(i, j) for i, j in pairs if j is not None and...  65.9 us
    dot_general x3, matrix products, down(): jnp.dot(hidden, jnp.concatenate(blocks, axis=1), preferred_element_type=F32)  12.8 us
    pallas_call x1, Pallas kernels, up_most(): return run(at, *pieces, *blocks)  11.2 us
    pallas_call x1, Pallas kernels, to_middle(): call(middle_kernel, (jax.ShapeDtypeStruct((rows, depth), BF16),) * 3, 3 +...  5 us
    pallas_call x1, Pallas kernels, retention(): call(local_kernel, (sds((length, lanes), F32),) * 2 + (sds((length, lanes...  4.96 us
  transfers between devices with their start and end apart: 44, of which 19 were waited for; matrix products, arithmetic and copies ran while one was open for 15% of the time, Pallas kernels for 14%

profile of v3, /device:TPU:0, one launch (start us, length us, event | category | flops | bytes accessed | tf_op | source)
XLA Modules:
  0.0 245.3 jit_solution(7124672071278509086)
XLA Ops:
  0.7 1.9 constant_dynamic-update-slice_fusion.1
  2.6 1.9 constant_dynamic-update-slice_fusion
  4.5 3.0 %collective-permute-start.8 = (bf16[256,2048]{1,0:T(8,128)(2,1)}, bf16[256,2048]{1,0:T(8,128)(2,1)}, u32[]{:S(2)}, u32[]{:S(2)}) collective-permute-start(bf16[256,2048]{1,0:T(8,128)(2,1)} %constant_dynamic-update-slice_fusion), channel_id=1, source_target_pairs={{0,2},{1,3},{2,0},{3,1},{4,6},{5,7},{6,4},{7,5},{8,10},{9,11},{10,... | collective-permute-start | bytes 3145736 | tf_op jit(solution)/shard_map/ppermute | solution.py:382
  7.5 1.4 broadcast_select_fusion.6.refs_5_
  8.9 1.6 collective-permute-start.16
  11.3 1.3 dynamic-slice_bitcast_fusion.rows
  12.6 3.3 %shard_map.199 = (bf16[208,128]{1,0:T(8,128)(2,1)}, f32[768,8]{1,0:T(8,128)}, f32[8,768]{1,0:T(8,128)}) custom-call(bf16[768,128]{1,0:T(8,128)(2,1)} %kw.3, bf16[768,128]{1,0:T(8,128)(2,1)} %vw.3, bf16[768,128]{1,0:T(8,128)(2,1)} %kn.3, bf16[768,128]{1,0:T(8,128)(2,1)} %vn.3, f32[1,768]{1,0:T(1,128)} %dw.1, f32[2,768]{1,0:T(2,128)} %dn.1, ...), custom_call_target="tpu_custom_call" | custom-call | flops 50331648 | bytes 2359296 | tf_op jit(solution)/shard_map/pallas_call | solution.py:394
  15.9 10.5 %collective-permute-start = (bf16[208,128]{1,0:T(8,128)(2,1)}, bf16[208,128]{1,0:T(8,128)(2,1)S(1)}, u32[]{:S(2)}, u32[]{:S(2)}) collective-permute-start(bf16[208,128]{1,0:T(8,128)(2,1)} %get-tuple-element.28.own), channel_id=1, source_target_pairs={{0,4},{4,0},{8,12},{12,8},{16,20},{20,16},{24,28},{28,24},{1,5},{5... | collective-permute-start | bytes 159752 | tf_op jit(solution)/shard_map/ppermute | solution.py:382
  27.0 1.8 collective-permute-done.other
  29.5 1.5 shard_map.201
  31.0 6.1 %collective-permute-start.1 = (bf16[208,128]{1,0:T(8,128)(2,1)}, bf16[208,128]{1,0:T(8,128)(2,1)S(1)}, u32[]{:S(2)}, u32[]{:S(2)}) collective-permute-start(bf16[208,128]{1,0:T(8,128)(2,1)} %shard_map.201), channel_id=1, source_target_pairs={{0,8},{4,12},{8,16},{12,20},{16,24},{20,28},{1,9},{5,13},{9,17},{1... | collective-permute-start | bytes 159752 | tf_op jit(solution)/shard_map/ppermute | solution.py:382
  37.1 1.5 collective-permute-start.2
  39.3 3.0 %collective-permute-start.3 = (bf16[208,128]{1,0:T(8,128)(2,1)}, bf16[208,128]{1,0:T(8,128)(2,1)S(1)}, u32[]{:S(2)}, u32[]{:S(2)}) collective-permute-start(bf16[208,128]{1,0:T(8,128)(2,1)} %shard_map.201), channel_id=1, source_target_pairs={{0,24},{4,28},{1,25},{5,29},{2,26},{6,30},{3,27},{7,31}} | collective-permute-start | bytes 159752 | tf_op jit(solution)/shard_map/ppermute | solution.py:382
  42.4 5.0 %shard_map.200 = (f32[768,128]{1,0:T(8,128)}, f32[768,128]{1,0:T(8,128)}, bf16[768,128]{1,0:T(8,128)(2,1)}, bf16[768,128]{1,0:T(8,128)(2,1)}) custom-call(bf16[768,128]{1,0:T(8,128)(2,1)} %qw.1, bf16[768,128]{1,0:T(8,128)(2,1)} %kw.3, bf16[768,128]{1,0:T(8,128)(2,1)} %vw.3, bf16[768,128]{1,0:T(8,128)(2,1)} %qn.1, bf16[768,128]{1,0:T(8,128)(2,1)} %kn.3, ...), custom_call_target="tpu_custom_call" | custom-call | flops 603979776 | bytes 3932160 | tf_op jit(solution)/shard_map/pallas_call | solution.py:401
  48.0 3.1 %shard_map.202 = (bf16[192,256]{1,0:T(8,128)(2,1)}, bf16[192,256]{1,0:T(8,128)(2,1)}, bf16[192,256]{1,0:T(8,128)(2,1)}, bf16[192,256]{1,0:T(8,128)(2,1)}) custom-call(s32[5]{0:T(128)} %stack.59.late, bf16[208,128]{1,0:T(8,128)(2,1)} %get-tuple-element.28.own, bf16[208,128]{1,0:T(8,128)(2,1)} %copy-done.5, f32[768,128]{1,0:T(8,128)} %get-tuple-element.31.ow, ...), custom_call_target="tpu_custom_call" | custom-call | flops 50331648 | bytes 2359296 | tf_op jit(solution)/shard_map/pallas_call | solution.py:415
  51.1 1.6 collective-permute-start.5
  52.7 1.2 collective-permute-start.6
  53.9 3.2 %collective-permute-done.5.refs_2_ = bf16[192,256]{1,0:T(8,128)(2,1)S(1)} collective-permute-done((bf16[192,256]{1,0:T(8,128)(2,1)}, bf16[192,256]{1,0:T(8,128)(2,1)S(1)}, u32[]{:S(2)}, u32[]{:S(2)}) %collective-permute-start.5) | collective-permute-done | bytes 98336 | tf_op jit(solution)/shard_map/ppermute | solution.py:382
  57.7 1.3 collective-permute-start.19
  59.0 1.6 collective-permute-start.20
  61.2 1.6 collective-permute-start.24
  62.8 2.8 %collective-permute-start.15 = (bf16[256,2048]{1,0:T(8,128)(2,1)S(1)}, bf16[256,2048]{1,0:T(8,128)(2,1)}, u32[]{:S(2)}, u32[]{:S(2)}) collective-permute-start(bf16[256,2048]{1,0:T(8,128)(2,1)S(1)} %broadcast_select_fusion.6.refs_5_), channel_id=1, source_target_pairs={{0,1},{1,0},{2,3},{3,2},{4,5},{5,4},{6,7},{7,6},{8,9},{9,8},{10,11... | collective-permute-start | bytes 3145736 | tf_op jit(solution)/shard_map/ppermute | solution.py:382
  65.7 5.0 %shard_map.203 = (bf16[192,2048]{1,0:T(8,128)(2,1)}, bf16[192,2048]{1,0:T(8,128)(2,1)}, bf16[192,2048]{1,0:T(8,128)(2,1)}) custom-call(bf16[192,2048]{1,0:T(8,128)(2,1)} %stream.1, bf16[1,2048]{1,0:T(2,128)(2,1)} %broadcast_in_dim.3.gain, bf16[128,2048]{1,0:T(8,128)(2,1)} %wide.1, bf16[128,2048]{1,0:T(8,128)(2,1)} %narrow.1, ...), custom_call_target="tpu_custom_call" | custom-call | flops 805306368 | bytes 3145728 | tf_op jit(solution)/shard_map/pallas_call | solution.py:434
  70.7 1.6 collective-permute-start.10
  72.2 12.9 %collective-permute-done.19 = bf16[256,2048]{1,0:T(8,128)(2,1)} collective-permute-done((bf16[256,2048]{1,0:T(8,128)(2,1)S(1)}, bf16[256,2048]{1,0:T(8,128)(2,1)}, u32[]{:S(2)}, u32[]{:S(2)}) %collective-permute-start.19) | collective-permute-done | bytes 1048608 | tf_op jit(solution)/shard_map/ppermute | solution.py:382
  85.2 2.4 collective-permute-start.11
  87.5 2.3 broadcast_select_fusion.5.refs_9_
  90.6 1.3 collective-permute-start.22
  93.6 11.6 %collective-permute-done.11.refs_2_ = bf16[192,2048]{1,0:T(8,128)(2,1)} collective-permute-done((bf16[192,2048]{1,0:T(8,128)(2,1)}, bf16[192,2048]{1,0:T(8,128)(2,1)}, u32[]{:S(2)}, u32[]{:S(2)}) %collective-permute-start.11) | collective-permute-done | bytes 786464 | tf_op jit(solution)/shard_map/ppermute | solution.py:382
  105.1 1.7 collective-permute-start.12
  107.9 1.6 collective-permute-start.13
  109.5 1.1 broadcast_select_fusion.3
  110.6 4.6 %collective-permute-done.12.refs_3_ = bf16[96,2048]{1,0:T(8,128)(2,1)S(1)} collective-permute-done((bf16[96,2048]{1,0:T(8,128)(2,1)S(1)}, bf16[96,2048]{1,0:T(8,128)(2,1)S(1)}, u32[]{:S(2)}, u32[]{:S(2)}) %collective-permute-start.12) | collective-permute-done | bytes 393248 | tf_op jit(solution)/shard_map/ppermute | solution.py:382
  115.9 1.6 collective-permute-done.13.refs_4_
  118.2 11.2 %shard_map.204 = (f32[768,2048]{1,0:T(8,128)}, bf16[768,512]{1,0:T(8,128)(2,1)}) custom-call(s32[8]{0:T(128)} %stack.53.at, bf16[192,2048]{1,0:T(8,128)(2,1)} %get-tuple-element.40.refs_0_, bf16[192,2048]{1,0:T(8,128)(2,1)} %collective-permute-done.10.refs_1_, bf16[192,2048]{1,0:T(8,128)(2,1)} %collective-permute-done.11.refs_2_, ...), custom_call_target="tpu_custom_call" | custom-call | flops 4831838208 | bytes 17825792 | tf_op jit(solution)/shard_map/pallas_call | solution.py:336
  129.4 1.3 broadcast_select_fusion.4
  131.4 9.9 %collective-permute-done.26 = bf16[2048,256]{1,0:T(8,128)(2,1)} collective-permute-done((bf16[2048,256]{1,0:T(8,128)(2,1)}, bf16[2048,256]{1,0:T(8,128)(2,1)}, u32[]{:S(2)}, u32[]{:S(2)}) %collective-permute-start.26) | collective-permute-done | bytes 1048608 | tf_op jit(solution)/shard_map/ppermute | solution.py:382
  141.3 1.3 fusion.37
  142.6 1.3 shard_map.205
  143.9 1.7 collective-permute-start.33
  145.6 1.5 collective-permute-start.32
  147.0 4.8 %multiply_convert_fusion = bf16[768,2048]{1,0:T(8,128)(2,1)S(1)} fusion(f32[768,2048]{1,0:T(8,128)} %get-tuple-element.43, bf16[768,512]{1,0:T(8,128)(2,1)} %get-tuple-element.44, bf16[256,2048]{1,0:T(8,128)(2,1)S(1)} %collective-permute-done.23, bf16[256,2048]{1,0:T(8,128)(2,1)S(1)} %broadcast_select_fusion.4), kind=kOutput, calls=%fused_computation | convolution fusion | flops 1621098496 | bytes 12320768 | tf_op jit(solution)/shard_map/dot_general | solution.py:340
  151.9 6.7 %fusion.19 = bf16[768,1024]{1,0:T(8,128)(2,1)S(1)} fusion(bf16[768,2048]{1,0:T(8,128)(2,1)S(1)} %multiply_convert_fusion, bf16[2048,256]{1,0:T(8,128)(2,1)} %collective-permute-done.27, bf16[2048,256]{1,0:T(8,128)(2,1)} %collective-permute-done.26, bf16[2048,256]{1,0:T(8,128)(2,1)} %collective-permute-done.25, bf16[2048,256]{1,0:T(8,128)(2,1)} %broadcast_select_fusion.3), kind=kOutput, calls=%fused_computation.20 | convolution fusion | flops 3238789120 | bytes 8912896 | tf_op jit(solution)/shard_map/dot_general | solution.py:527
  158.7 14.4 %collective-permute-done.32 = bf16[2048,256]{1,0:T(8,128)(2,1)S(1)} collective-permute-done((bf16[2048,256]{1,0:T(8,128)(2,1)S(1)}, bf16[2048,256]{1,0:T(8,128)(2,1)S(1)}, u32[]{:S(2)}, u32[]{:S(2)}) %collective-permute-start.32) | collective-permute-done | bytes 1048608 | tf_op jit(solution)/shard_map/ppermute | solution.py:382
  173.0 1.1 broadcast_select_fusion.2
  174.2 1.3 collective-permute-start.38
  175.5 1.3 shard_map.207
  177.5 4.3 %fusion.25 = bf16[768,512]{1,0:T(8,128)(2,1)S(1)} fusion(bf16[768,2048]{1,0:T(8,128)(2,1)} %copy-done.19, bf16[2048,256]{1,0:T(8,128)(2,1)} %collective-permute-done.34, bf16[2048,256]{1,0:T(8,128)(2,1)} %broadcast_select_fusion.2), kind=kOutput, calls=%fused_computation.22 | convolution fusion | flops 1615200256 | bytes 6029312 | tf_op jit(solution)/shard_map/dot_general | solution.py:527
  181.8 20.2 %collective-permute-done.38 = bf16[2048,256]{1,0:T(8,128)(2,1)} collective-permute-done((bf16[2048,256]{1,0:T(8,128)(2,1)}, bf16[2048,256]{1,0:T(8,128)(2,1)}, u32[]{:S(2)}, u32[]{:S(2)}) %collective-permute-start.38) | collective-permute-done | bytes 1048608 | tf_op jit(solution)/shard_map/ppermute | solution.py:382
  201.9 1.9 collective-permute-start.39
  204.8 2.3 collective-permute-start.28
  209.0 1.3 broadcast_select_fusion.1
  210.4 2.3 collective-permute-start.35
  213.4 1.8 fusion.22
  215.2 2.5 %collective-permute-done.28.refs_1_ = bf16[192,1024]{1,0:T(8,128)(2,1)S(1)} collective-permute-done((bf16[192,1024]{1,0:T(8,128)(2,1)S(1)}, bf16[192,1024]{1,0:T(8,128)(2,1)S(1)}, u32[]{:S(2)}, u32[]{:S(2)}) %collective-permute-start.28) | collective-permute-done | bytes 393248 | tf_op jit(solution)/shard_map/ppermute | solution.py:382
  217.7 1.3 collective-permute-start.37
  219.0 7.0 %collective-permute-done.29.refs_2_ = bf16[192,1024]{1,0:T(8,128)(2,1)S(1)} collective-permute-done((bf16[192,1024]{1,0:T(8,128)(2,1)S(1)}, bf16[192,1024]{1,0:T(8,128)(2,1)S(1)}, u32[]{:S(2)}, u32[]{:S(2)}) %collective-permute-start.29) | collective-permute-done | bytes 393248 | tf_op jit(solution)/shard_map/ppermute | solution.py:382
  226.0 1.6 collective-permute-start.41
  228.2 2.2 collective-permute-done.35.refs_5_
  230.4 1.3 collective-permute-start.43
  232.2 2.2 collective-permute-done.36.refs_6_
  235.3 3.2 %shard_map.206 = bf16[192,2048]{1,0:T(8,128)(2,1)} custom-call(s32[8]{0:T(128)} %broadcast_multiply_fusion.at, bf16[192,2048]{1,0:T(8,128)(2,1)} %get-tuple-element.39.middle, bf16[192,1024]{1,0:T(8,128)(2,1)} %get-tuple-element.54.refs_0_, bf16[192,1024]{1,0:T(8,128)(2,1)} %copy-done.2, bf16[192,1024]{1,0:T(8,128)(2,1)} %copy-done.3, ...), custom_call_target="tpu_custom_call" | custom-call | flops 393216 | bytes 3145728 | tf_op jit(solution)/shard_map/pallas_call | solution.py:549
  238.9 3.6 %collective-permute-done.42 = bf16[192,512]{1,0:T(8,128)(2,1)S(1)} collective-permute-done((bf16[192,512]{1,0:T(8,128)(2,1)S(1)}, bf16[192,512]{1,0:T(8,128)(2,1)S(1)}, u32[]{:S(2)}, u32[]{:S(2)}) %collective-permute-start.42) | collective-permute-done | bytes 196640 | tf_op jit(solution)/shard_map/ppermute | solution.py:382
  243.6 1.7 fusion.30
  (102 shorter events, 18.4 us)
Async XLA Ops:
  0.0 7.5 %collective-permute-start.14 = (bf16[256,2048]{1,0:T(8,128)(2,1)}, bf16[256,2048]{1,0:T(8,128)(2,1)S(1)}, u32[]{:S(2)}, u32[]{:S(2)}) collective-permute-start(bf16[256,2048]{1,0:T(8,128)(2,1)} %param.35), channel_id=1, source_target_pairs={{1,4},{3,6},{4,1},{6,3},{9,12},{11,14},{12,9},{14,11},{17,20},{19,... | collective-permute-start | bytes 3145736 | tf_op jit(solution)/shard_map/ppermute | solution.py:382
  4.5 52.6 %collective-permute-start.8 = (bf16[256,2048]{1,0:T(8,128)(2,1)}, bf16[256,2048]{1,0:T(8,128)(2,1)}, u32[]{:S(2)}, u32[]{:S(2)}) collective-permute-start(bf16[256,2048]{1,0:T(8,128)(2,1)} %constant_dynamic-update-slice_fusion), channel_id=1, source_target_pairs={{0,2},{1,3},{2,0},{3,1},{4,6},{5,7},{6,4},{7,5},{8,10},{9,11},{10,... | collective-permute-start | bytes 3145736 | tf_op jit(solution)/shard_map/ppermute | solution.py:382
  7.5 53.1 %copy-start.15 = (bf16[2048]{0:T(1024)(128)(2,1)S(1)}, bf16[2048]{0:T(1024)(128)(2,1)}, u32[]{:S(2)}) copy-start(bf16[2048]{0:T(1024)(128)(2,1)} %param.34) | copy-start | bytes 12292
  7.5 53.7 %copy-start = (bf16[2048,256]{1,0:T(8,128)(2,1)S(1)}, bf16[2048,256]{1,0:T(8,128)(2,1)}, u32[]{:S(2)}) copy-start(bf16[2048,256]{1,0:T(8,128)(2,1)} %param.36) | copy-start | bytes 3145732
  8.9 61.8 %copy-start.1 = (bf16[256,2048]{1,0:T(8,128)(2,1)}, bf16[256,2048]{1,0:T(8,128)(2,1)S(1)}, u32[]{:S(2)}) copy-start(bf16[256,2048]{1,0:T(8,128)(2,1)S(1)} %broadcast_select_fusion.6.refs_5_) | copy-start | bytes 3145732
  8.9 48.7 %collective-permute-start.16 = (bf16[256,2048]{1,0:T(8,128)(2,1)S(1)}, bf16[256,2048]{1,0:T(8,128)(2,1)}, u32[]{:S(2)}, u32[]{:S(2)}) collective-permute-start(bf16[256,2048]{1,0:T(8,128)(2,1)S(1)} %broadcast_select_fusion.6.refs_5_), channel_id=1, source_target_pairs={{0,8},{4,12},{8,0},{12,4},{16,24},{20,28},{24,16},{28,20},{1,9},{5... | collective-permute-start | bytes 3145736 | tf_op jit(solution)/shard_map/ppermute | solution.py:382
  10.6 47.1 %collective-permute-start.18 = (bf16[256,2048]{1,0:T(8,128)(2,1)S(1)}, bf16[256,2048]{1,0:T(8,128)(2,1)S(1)}, u32[]{:S(2)}, u32[]{:S(2)}) collective-permute-start(bf16[256,2048]{1,0:T(8,128)(2,1)S(1)} %broadcast_select_fusion.6.refs_5_), channel_id=1, source_target_pairs={{8,16},{12,20},{16,8},{20,12},{9,17},{13,21},{17,9},{21,13},{10,18... | collective-permute-start | bytes 3145736 | tf_op jit(solution)/shard_map/ppermute | solution.py:382
  15.9 13.0 %collective-permute-start = (bf16[208,128]{1,0:T(8,128)(2,1)}, bf16[208,128]{1,0:T(8,128)(2,1)S(1)}, u32[]{:S(2)}, u32[]{:S(2)}) collective-permute-start(bf16[208,128]{1,0:T(8,128)(2,1)} %get-tuple-element.28.own), channel_id=1, source_target_pairs={{0,4},{4,0},{8,12},{12,8},{16,20},{20,16},{24,28},{28,24},{1,5},{5... | collective-permute-start | bytes 159752 | tf_op jit(solution)/shard_map/ppermute | solution.py:382
  28.9 0.6 copy-start.5
  31.0 8.3 %collective-permute-start.1 = (bf16[208,128]{1,0:T(8,128)(2,1)}, bf16[208,128]{1,0:T(8,128)(2,1)S(1)}, u32[]{:S(2)}, u32[]{:S(2)}) collective-permute-start(bf16[208,128]{1,0:T(8,128)(2,1)} %shard_map.201), channel_id=1, source_target_pairs={{0,8},{4,12},{8,16},{12,20},{16,24},{20,28},{1,9},{5,13},{9,17},{1... | collective-permute-start | bytes 159752 | tf_op jit(solution)/shard_map/ppermute | solution.py:382
  37.1 10.2 %collective-permute-start.2 = (bf16[208,128]{1,0:T(8,128)(2,1)}, bf16[208,128]{1,0:T(8,128)(2,1)S(1)}, u32[]{:S(2)}, u32[]{:S(2)}) collective-permute-start(bf16[208,128]{1,0:T(8,128)(2,1)} %shard_map.201), channel_id=1, source_target_pairs={{0,16},{4,20},{8,24},{12,28},{1,17},{5,21},{9,25},{13,29},{2,18},{... | collective-permute-start | bytes 159752 | tf_op jit(solution)/shard_map/ppermute | solution.py:382
  39.3 8.0 %copy-start.12 = (bf16[208,128]{1,0:T(8,128)(2,1)}, bf16[208,128]{1,0:T(8,128)(2,1)S(1)}, u32[]{:S(2)}) copy-start(bf16[208,128]{1,0:T(8,128)(2,1)S(1)} %collective-permute-done.1.refs_0_) | copy-start | bytes 159748
  39.3 8.0 %collective-permute-start.3 = (bf16[208,128]{1,0:T(8,128)(2,1)}, bf16[208,128]{1,0:T(8,128)(2,1)S(1)}, u32[]{:S(2)}, u32[]{:S(2)}) collective-permute-start(bf16[208,128]{1,0:T(8,128)(2,1)} %shard_map.201), channel_id=1, source_target_pairs={{0,24},{4,28},{1,25},{5,29},{2,26},{6,30},{3,27},{7,31}} | collective-permute-start | bytes 159752 | tf_op jit(solution)/shard_map/ppermute | solution.py:382
  47.3 0.6 copy-start.14
  51.1 1.6 collective-permute-start.4
  51.1 5.9 %collective-permute-start.5 = (bf16[192,256]{1,0:T(8,128)(2,1)}, bf16[192,256]{1,0:T(8,128)(2,1)S(1)}, u32[]{:S(2)}, u32[]{:S(2)}) collective-permute-start(bf16[192,256]{1,0:T(8,128)(2,1)} %get-tuple-element.37), channel_id=1, source_target_pairs={{0,2},{1,3},{2,0},{3,1},{4,6},{5,7},{6,4},{7,5},{8,10},{9,11},{10,... | collective-permute-start | bytes 294920 | tf_op jit(solution)/shard_map/ppermute | solution.py:382
  52.7 13.0 %copy-start.9 = (bf16[192,256]{1,0:T(8,128)(2,1)}, bf16[192,256]{1,0:T(8,128)(2,1)S(1)}, u32[]{:S(2)}) copy-start(bf16[192,256]{1,0:T(8,128)(2,1)S(1)} %collective-permute-done.4.refs_1_) | copy-start | bytes 294916
  52.7 6.3 %collective-permute-start.6 = (bf16[192,256]{1,0:T(8,128)(2,1)}, bf16[192,256]{1,0:T(8,128)(2,1)S(1)}, u32[]{:S(2)}, u32[]{:S(2)}) collective-permute-start(bf16[192,256]{1,0:T(8,128)(2,1)} %get-tuple-element.38), channel_id=1, source_target_pairs={{0,3},{1,2},{2,1},{3,0},{4,7},{5,6},{6,5},{7,4},{8,11},{9,10},{10,... | collective-permute-start | bytes 294920 | tf_op jit(solution)/shard_map/ppermute | solution.py:382
  57.1 8.6 %copy-start.10 = (bf16[192,256]{1,0:T(8,128)(2,1)}, bf16[192,256]{1,0:T(8,128)(2,1)S(1)}, u32[]{:S(2)}) copy-start(bf16[192,256]{1,0:T(8,128)(2,1)S(1)} %collective-permute-done.5.refs_2_) | copy-start | bytes 294916
  57.1 4.1 %collective-permute-start.7 = (bf16[256,2048]{1,0:T(8,128)(2,1)}, bf16[256,2048]{1,0:T(8,128)(2,1)}, u32[]{:S(2)}, u32[]{:S(2)}) collective-permute-start(bf16[256,2048]{1,0:T(8,128)(2,1)} %constant_dynamic-update-slice_fusion), channel_id=1, source_target_pairs={{0,1},{1,0},{2,3},{3,2},{4,5},{5,4},{6,7},{7,6},{8,9},{9,8},{10,11... | collective-permute-start | bytes 3145736 | tf_op jit(solution)/shard_map/ppermute | solution.py:382
  57.1 5.8 %collective-permute-start.9 = (bf16[256,2048]{1,0:T(8,128)(2,1)}, bf16[256,2048]{1,0:T(8,128)(2,1)}, u32[]{:S(2)}, u32[]{:S(2)}) collective-permute-start(bf16[256,2048]{1,0:T(8,128)(2,1)} %collective-permute-done.8.refs_5_), channel_id=1, source_target_pairs={{0,1},{1,0},{2,3},{3,2},{4,5},{5,4},{6,7},{7,6},{8,9},{9,8},{10,11... | collective-permute-start | bytes 3145736 | tf_op jit(solution)/shard_map/ppermute | solution.py:382
  57.6 13.1 %collective-permute-start.17 = (bf16[256,2048]{1,0:T(8,128)(2,1)}, bf16[256,2048]{1,0:T(8,128)(2,1)}, u32[]{:S(2)}, u32[]{:S(2)}) collective-permute-start(bf16[256,2048]{1,0:T(8,128)(2,1)} %collective-permute-done.16.refs_7_), channel_id=1, source_target_pairs={{0,1},{1,0},{2,3},{3,2},{4,5},{5,4},{6,7},{7,6},{8,9},{9,8},{10,11... | collective-permute-start | bytes 3145736 | tf_op jit(solution)/shard_map/ppermute | solution.py:382
  57.7 27.5 %collective-permute-start.19 = (bf16[256,2048]{1,0:T(8,128)(2,1)S(1)}, bf16[256,2048]{1,0:T(8,128)(2,1)}, u32[]{:S(2)}, u32[]{:S(2)}) collective-permute-start(bf16[256,2048]{1,0:T(8,128)(2,1)S(1)} %collective-permute-done.18), channel_id=1, source_target_pairs={{8,0},{12,4},{16,24},{20,28},{9,1},{13,5},{17,25},{21,29},{10,2},{... | collective-permute-start | bytes 3145736 | tf_op jit(solution)/shard_map/ppermute | solution.py:382
  59.0 6.7 %copy-start.11 = (bf16[192,256]{1,0:T(8,128)(2,1)}, bf16[192,256]{1,0:T(8,128)(2,1)S(1)}, u32[]{:S(2)}) copy-start(bf16[192,256]{1,0:T(8,128)(2,1)S(1)} %collective-permute-done.6.refs_3_) | copy-start | bytes 294916
  59.0 28.6 %collective-permute-start.20 = (bf16[256,2048]{1,0:T(8,128)(2,1)}, bf16[256,2048]{1,0:T(8,128)(2,1)}, u32[]{:S(2)}, u32[]{:S(2)}) collective-permute-start(bf16[256,2048]{1,0:T(8,128)(2,1)} %collective-permute-done.16.refs_7_), channel_id=1, source_target_pairs={{8,16},{12,20},{16,8},{20,12},{9,17},{13,21},{17,9},{21,13},{10,18... | collective-permute-start | bytes 3145736 | tf_op jit(solution)/shard_map/ppermute | solution.py:382
  61.2 46.7 %collective-permute-start.24 = (bf16[2048,256]{1,0:T(8,128)(2,1)S(1)}, bf16[2048,256]{1,0:T(8,128)(2,1)}, u32[]{:S(2)}, u32[]{:S(2)}) collective-permute-start(bf16[2048,256]{1,0:T(8,128)(2,1)S(1)} %copy-done), channel_id=1, source_target_pairs={{1,4},{3,6},{4,1},{6,3},{9,12},{11,14},{12,9},{14,11},{17,20},{19,... | collective-permute-start | bytes 3145736 | tf_op jit(solution)/shard_map/ppermute | solution.py:382
  62.8 47.7 %collective-permute-start.15 = (bf16[256,2048]{1,0:T(8,128)(2,1)S(1)}, bf16[256,2048]{1,0:T(8,128)(2,1)}, u32[]{:S(2)}, u32[]{:S(2)}) collective-permute-start(bf16[256,2048]{1,0:T(8,128)(2,1)S(1)} %broadcast_select_fusion.6.refs_5_), channel_id=1, source_target_pairs={{0,1},{1,0},{2,3},{3,2},{4,5},{5,4},{6,7},{7,6},{8,9},{9,8},{10,11... | collective-permute-start | bytes 3145736 | tf_op jit(solution)/shard_map/ppermute | solution.py:382
  70.7 19.9 %collective-permute-start.10 = (bf16[192,2048]{1,0:T(8,128)(2,1)}, bf16[192,2048]{1,0:T(8,128)(2,1)}, u32[]{:S(2)}, u32[]{:S(2)}) collective-permute-start(bf16[192,2048]{1,0:T(8,128)(2,1)} %get-tuple-element.40.refs_0_), channel_id=1, source_target_pairs={{0,2},{1,3},{2,0},{3,1},{4,6},{5,7},{6,4},{7,5},{8,10},{9,11},{10,... | collective-permute-start | bytes 2359304 | tf_op jit(solution)/shard_map/ppermute | solution.py:382
  85.2 20.0 %collective-permute-start.11 = (bf16[192,2048]{1,0:T(8,128)(2,1)}, bf16[192,2048]{1,0:T(8,128)(2,1)}, u32[]{:S(2)}, u32[]{:S(2)}) collective-permute-start(bf16[192,2048]{1,0:T(8,128)(2,1)} %get-tuple-element.41), channel_id=1, source_target_pairs={{0,4},{4,0},{8,12},{12,8},{16,20},{20,16},{24,28},{28,24},{1,5},{5... | collective-permute-start | bytes 2359304 | tf_op jit(solution)/shard_map/ppermute | solution.py:382
  89.8 28.4 %collective-permute-start.21 = (bf16[256,2048]{1,0:T(8,128)(2,1)}, bf16[256,2048]{1,0:T(8,128)(2,1)}, u32[]{:S(2)}, u32[]{:S(2)}) collective-permute-start(bf16[256,2048]{1,0:T(8,128)(2,1)} %broadcast_select_fusion.5.refs_9_), channel_id=1, source_target_pairs={{0,1},{1,0},{2,3},{3,2},{4,5},{5,4},{6,7},{7,6},{8,9},{9,8},{10,11... | collective-permute-start | bytes 3145736 | tf_op jit(solution)/shard_map/ppermute | solution.py:382
  90.6 38.9 %collective-permute-start.22 = (bf16[256,2048]{1,0:T(8,128)(2,1)}, bf16[256,2048]{1,0:T(8,128)(2,1)}, u32[]{:S(2)}, u32[]{:S(2)}) collective-permute-start(bf16[256,2048]{1,0:T(8,128)(2,1)} %collective-permute-done.20), channel_id=1, source_target_pairs={{8,0},{12,4},{16,24},{20,28},{9,1},{13,5},{17,25},{21,29},{10,2},{... | collective-permute-start | bytes 3145736 | tf_op jit(solution)/shard_map/ppermute | solution.py:382
  105.1 10.0 %collective-permute-start.12 = (bf16[96,2048]{1,0:T(8,128)(2,1)S(1)}, bf16[96,2048]{1,0:T(8,128)(2,1)S(1)}, u32[]{:S(2)}, u32[]{:S(2)}) collective-permute-start(bf16[96,2048]{1,0:T(8,128)(2,1)S(1)} %slice.74), channel_id=1, source_target_pairs={{0,4},{4,0},{8,12},{12,8},{16,20},{20,16},{24,28},{28,24},{1,5},{5... | collective-permute-start | bytes 1179656 | tf_op jit(solution)/shard_map/ppermute | solution.py:382
  107.9 9.5 %collective-permute-start.13 = (bf16[96,2048]{1,0:T(8,128)(2,1)S(1)}, bf16[96,2048]{1,0:T(8,128)(2,1)S(1)}, u32[]{:S(2)}, u32[]{:S(2)}) collective-permute-start(bf16[96,2048]{1,0:T(8,128)(2,1)S(1)} %slice.75), channel_id=1, source_target_pairs={{0,2},{1,3},{2,0},{3,1},{4,6},{5,7},{6,4},{7,5},{8,10},{9,11},{10,... | collective-permute-start | bytes 1179656 | tf_op jit(solution)/shard_map/ppermute | solution.py:382
  110.6 30.7 %collective-permute-start.26 = (bf16[2048,256]{1,0:T(8,128)(2,1)}, bf16[2048,256]{1,0:T(8,128)(2,1)}, u32[]{:S(2)}, u32[]{:S(2)}) collective-permute-start(bf16[2048,256]{1,0:T(8,128)(2,1)} %broadcast_select_fusion.3), channel_id=1, source_target_pairs={{0,8},{4,12},{8,0},{12,4},{16,24},{20,28},{24,16},{28,20},{1,9},{5... | collective-permute-start | bytes 3145736 | tf_op jit(solution)/shard_map/ppermute | solution.py:382
  115.2 3.0 %copy-start.17 = (bf16[96,2048]{1,0:T(8,128)(2,1)}, bf16[96,2048]{1,0:T(8,128)(2,1)S(1)}, u32[]{:S(2)}) copy-start(bf16[96,2048]{1,0:T(8,128)(2,1)S(1)} %collective-permute-done.12.refs_3_) | copy-start | bytes 1179652
  115.2 30.4 %collective-permute-start.31 = (bf16[2048,256]{1,0:T(8,128)(2,1)}, bf16[2048,256]{1,0:T(8,128)(2,1)S(1)}, u32[]{:S(2)}, u32[]{:S(2)}) collective-permute-start(bf16[2048,256]{1,0:T(8,128)(2,1)} %broadcast_select_fusion.3), channel_id=1, source_target_pairs={{8,16},{12,20},{16,8},{20,12},{9,17},{13,21},{17,9},{21,13},{10,18... | collective-permute-start | bytes 3145736 | tf_op jit(solution)/shard_map/ppermute | solution.py:382
  117.4 0.8 copy-start.18
  130.8 16.2 %collective-permute-start.23 = (bf16[256,2048]{1,0:T(8,128)(2,1)S(1)}, bf16[256,2048]{1,0:T(8,128)(2,1)S(1)}, u32[]{:S(2)}, u32[]{:S(2)}) collective-permute-start(bf16[256,2048]{1,0:T(8,128)(2,1)S(1)} %broadcast_select_fusion.4), channel_id=1, source_target_pairs={{0,1},{1,0},{2,3},{3,2},{4,5},{5,4},{6,7},{7,6},{8,9},{9,8},{10,11... | collective-permute-start | bytes 3145736 | tf_op jit(solution)/shard_map/ppermute | solution.py:382
  130.9 21.0 %collective-permute-start.25 = (bf16[2048,256]{1,0:T(8,128)(2,1)}, bf16[2048,256]{1,0:T(8,128)(2,1)}, u32[]{:S(2)}, u32[]{:S(2)}) collective-permute-start(bf16[2048,256]{1,0:T(8,128)(2,1)} %broadcast_select_fusion.3), channel_id=1, source_target_pairs={{0,1},{1,0},{2,3},{3,2},{4,5},{5,4},{6,7},{7,6},{8,9},{9,8},{10,11... | collective-permute-start | bytes 3145736 | tf_op jit(solution)/shard_map/ppermute | solution.py:382
  141.3 10.6 %collective-permute-start.27 = (bf16[2048,256]{1,0:T(8,128)(2,1)}, bf16[2048,256]{1,0:T(8,128)(2,1)}, u32[]{:S(2)}, u32[]{:S(2)}) collective-permute-start(bf16[2048,256]{1,0:T(8,128)(2,1)} %collective-permute-done.26), channel_id=1, source_target_pairs={{0,1},{1,0},{2,3},{3,2},{4,5},{5,4},{6,7},{7,6},{8,9},{9,8},{10,11... | collective-permute-start | bytes 3145736 | tf_op jit(solution)/shard_map/ppermute | solution.py:382
  143.9 29.1 %collective-permute-start.33 = (bf16[2048,256]{1,0:T(8,128)(2,1)}, bf16[2048,256]{1,0:T(8,128)(2,1)}, u32[]{:S(2)}, u32[]{:S(2)}) collective-permute-start(bf16[2048,256]{1,0:T(8,128)(2,1)} %collective-permute-done.26), channel_id=1, source_target_pairs={{8,16},{12,20},{16,8},{20,12},{9,17},{13,21},{17,9},{21,13},{10,18... | collective-permute-start | bytes 3145736 | tf_op jit(solution)/shard_map/ppermute | solution.py:382
  145.6 27.5 %collective-permute-start.32 = (bf16[2048,256]{1,0:T(8,128)(2,1)S(1)}, bf16[2048,256]{1,0:T(8,128)(2,1)S(1)}, u32[]{:S(2)}, u32[]{:S(2)}) collective-permute-start(bf16[2048,256]{1,0:T(8,128)(2,1)S(1)} %collective-permute-done.31), channel_id=1, source_target_pairs={{8,0},{12,4},{16,24},{20,28},{9,1},{13,5},{17,25},{21,29},{10,2},{... | collective-permute-start | bytes 3145736 | tf_op jit(solution)/shard_map/ppermute | solution.py:382
  151.9 6.8 %copy-start.19 = (bf16[768,2048]{1,0:T(8,128)(2,1)}, bf16[768,2048]{1,0:T(8,128)(2,1)S(1)}, u32[]{:S(2)}) copy-start(bf16[768,2048]{1,0:T(8,128)(2,1)S(1)} %multiply_convert_fusion) | copy-start | bytes 9437188
  174.2 3.3 %collective-permute-start.34 = (bf16[2048,256]{1,0:T(8,128)(2,1)}, bf16[2048,256]{1,0:T(8,128)(2,1)}, u32[]{:S(2)}, u32[]{:S(2)}) collective-permute-start(bf16[2048,256]{1,0:T(8,128)(2,1)} %broadcast_select_fusion.2), channel_id=1, source_target_pairs={{0,1},{1,0},{2,3},{3,2},{4,5},{5,4},{6,7},{7,6},{8,9},{9,8},{10,11... | collective-permute-start | bytes 3145736 | tf_op jit(solution)/shard_map/ppermute | solution.py:382
  174.2 27.8 %collective-permute-start.38 = (bf16[2048,256]{1,0:T(8,128)(2,1)}, bf16[2048,256]{1,0:T(8,128)(2,1)}, u32[]{:S(2)}, u32[]{:S(2)}) collective-permute-start(bf16[2048,256]{1,0:T(8,128)(2,1)} %collective-permute-done.33), channel_id=1, source_target_pairs={{8,0},{12,4},{16,24},{20,28},{9,1},{13,5},{17,25},{21,29},{10,2},{... | collective-permute-start | bytes 3145736 | tf_op jit(solution)/shard_map/ppermute | solution.py:382
  176.7 33.6 %collective-permute-start.40 = (bf16[2048,256]{1,0:T(8,128)(2,1)S(1)}, bf16[2048,256]{1,0:T(8,128)(2,1)S(1)}, u32[]{:S(2)}, u32[]{:S(2)}) collective-permute-start(bf16[2048,256]{1,0:T(8,128)(2,1)S(1)} %collective-permute-done.31), channel_id=1, source_target_pairs={{8,9},{9,8},{10,11},{11,10},{12,13},{13,12},{14,15},{15,14},{16,17... | collective-permute-start | bytes 3145736 | tf_op jit(solution)/shard_map/ppermute | solution.py:382
  201.9 10.8 %collective-permute-start.39 = (bf16[2048,256]{1,0:T(8,128)(2,1)}, bf16[2048,256]{1,0:T(8,128)(2,1)S(1)}, u32[]{:S(2)}, u32[]{:S(2)}) collective-permute-start(bf16[2048,256]{1,0:T(8,128)(2,1)} %collective-permute-done.38), channel_id=1, source_target_pairs={{0,1},{1,0},{2,3},{3,2},{4,5},{5,4},{6,7},{7,6},{24,25},{25,24},{2... | collective-permute-start | bytes 3145736 | tf_op jit(solution)/shard_map/ppermute | solution.py:382
  204.8 8.6 %copy-start.20 = (bf16[768,2048]{1,0:T(8,128)(2,1)S(1)}, bf16[768,2048]{1,0:T(8,128)(2,1)}, u32[]{:S(2)}) copy-start(bf16[768,2048]{1,0:T(8,128)(2,1)} %copy-done.19) | copy-start | bytes 9437188
  204.8 12.9 %collective-permute-start.28 = (bf16[192,1024]{1,0:T(8,128)(2,1)S(1)}, bf16[192,1024]{1,0:T(8,128)(2,1)S(1)}, u32[]{:S(2)}, u32[]{:S(2)}) collective-permute-start(bf16[192,1024]{1,0:T(8,128)(2,1)S(1)} %get-tuple-element.53), channel_id=1, source_target_pairs={{0,6},{1,7},{2,4},{3,5},{4,2},{5,3},{6,0},{7,1},{8,14},{9,15},{10,... | collective-permute-start | bytes 1179656 | tf_op jit(solution)/shard_map/ppermute | solution.py:382
  207.0 19.0 %collective-permute-start.29 = (bf16[192,1024]{1,0:T(8,128)(2,1)S(1)}, bf16[192,1024]{1,0:T(8,128)(2,1)S(1)}, u32[]{:S(2)}, u32[]{:S(2)}) collective-permute-start(bf16[192,1024]{1,0:T(8,128)(2,1)S(1)} %get-tuple-element.52), channel_id=1, source_target_pairs={{0,2},{1,3},{2,0},{3,1},{4,6},{5,7},{6,4},{7,5},{8,10},{9,11},{10,... | collective-permute-start | bytes 1179656 | tf_op jit(solution)/shard_map/ppermute | solution.py:382
  207.6 20.1 %collective-permute-start.30 = (bf16[192,1024]{1,0:T(8,128)(2,1)S(1)}, bf16[192,1024]{1,0:T(8,128)(2,1)S(1)}, u32[]{:S(2)}, u32[]{:S(2)}) collective-permute-start(bf16[192,1024]{1,0:T(8,128)(2,1)S(1)} %get-tuple-element.51), channel_id=1, source_target_pairs={{0,4},{4,0},{8,12},{12,8},{16,20},{20,16},{24,28},{28,24},{1,5},{5... | collective-permute-start | bytes 1179656 | tf_op jit(solution)/shard_map/ppermute | solution.py:382
  210.4 20.0 %collective-permute-start.35 = (bf16[192,512]{1,0:T(8,128)(2,1)S(1)}, bf16[192,512]{1,0:T(8,128)(2,1)S(1)}, u32[]{:S(2)}, u32[]{:S(2)}) collective-permute-start(bf16[192,512]{1,0:T(8,128)(2,1)S(1)} %get-tuple-element.62), channel_id=1, source_target_pairs={{0,6},{1,7},{2,4},{3,5},{4,2},{5,3},{6,0},{7,1},{8,14},{9,15},{10,... | collective-permute-start | bytes 589832 | tf_op jit(solution)/shard_map/ppermute | solution.py:382
  212.7 21.8 %collective-permute-start.36 = (bf16[192,512]{1,0:T(8,128)(2,1)S(1)}, bf16[192,512]{1,0:T(8,128)(2,1)S(1)}, u32[]{:S(2)}, u32[]{:S(2)}) collective-permute-start(bf16[192,512]{1,0:T(8,128)(2,1)S(1)} %get-tuple-element.61), channel_id=1, source_target_pairs={{0,2},{1,3},{2,0},{3,1},{4,6},{5,7},{6,4},{7,5},{8,10},{9,11},{10,... | collective-permute-start | bytes 589832 | tf_op jit(solution)/shard_map/ppermute | solution.py:382
  213.4 18.4 %copy-start.16 = (s32[8]{0:T(128)S(1)}, s32[8]{0:T(128)}, u32[]{:S(2)}) copy-start(s32[8]{0:T(128)} %stack.53.at) | copy-start | bytes 100
  217.7 16.9 %copy-start.2 = (bf16[192,1024]{1,0:T(8,128)(2,1)}, bf16[192,1024]{1,0:T(8,128)(2,1)S(1)}, u32[]{:S(2)}) copy-start(bf16[192,1024]{1,0:T(8,128)(2,1)S(1)} %collective-permute-done.28.refs_1_) | copy-start | bytes 1179652
  217.7 16.9 %collective-permute-start.37 = (bf16[192,512]{1,0:T(8,128)(2,1)S(1)}, bf16[192,512]{1,0:T(8,128)(2,1)S(1)}, u32[]{:S(2)}, u32[]{:S(2)}) collective-permute-start(bf16[192,512]{1,0:T(8,128)(2,1)S(1)} %get-tuple-element.60), channel_id=1, source_target_pairs={{0,4},{4,0},{8,12},{12,8},{16,20},{20,16},{24,28},{28,24},{1,5},{5... | collective-permute-start | bytes 589832 | tf_op jit(solution)/shard_map/ppermute | solution.py:382
  226.0 8.6 %copy-start.3 = (bf16[192,1024]{1,0:T(8,128)(2,1)}, bf16[192,1024]{1,0:T(8,128)(2,1)S(1)}, u32[]{:S(2)}) copy-start(bf16[192,1024]{1,0:T(8,128)(2,1)S(1)} %collective-permute-done.29.refs_2_) | copy-start | bytes 1179652
  226.0 12.8 %collective-permute-start.41 = (bf16[192,512]{1,0:T(8,128)(2,1)S(1)}, bf16[192,512]{1,0:T(8,128)(2,1)S(1)}, u32[]{:S(2)}, u32[]{:S(2)}) collective-permute-start(bf16[192,512]{1,0:T(8,128)(2,1)S(1)} %get-tuple-element.55), channel_id=1, source_target_pairs={{0,6},{1,7},{2,4},{3,5},{4,2},{5,3},{6,0},{7,1},{8,14},{9,15},{10,... | collective-permute-start | bytes 589832 | tf_op jit(solution)/shard_map/ppermute | solution.py:382
  227.6 7.0 %copy-start.4 = (bf16[192,1024]{1,0:T(8,128)(2,1)}, bf16[192,1024]{1,0:T(8,128)(2,1)S(1)}, u32[]{:S(2)}) copy-start(bf16[192,1024]{1,0:T(8,128)(2,1)S(1)} %collective-permute-done.30.refs_3_) | copy-start | bytes 1179652
  227.6 14.8 %collective-permute-start.42 = (bf16[192,512]{1,0:T(8,128)(2,1)S(1)}, bf16[192,512]{1,0:T(8,128)(2,1)S(1)}, u32[]{:S(2)}, u32[]{:S(2)}) collective-permute-start(bf16[192,512]{1,0:T(8,128)(2,1)S(1)} %get-tuple-element.57), channel_id=1, source_target_pairs={{0,2},{1,3},{2,0},{3,1},{4,6},{5,7},{6,4},{7,5},{8,10},{9,11},{10,... | collective-permute-start | bytes 589832 | tf_op jit(solution)/shard_map/ppermute | solution.py:382
  230.4 4.2 %copy-start.6 = (bf16[192,512]{1,0:T(8,128)(2,1)}, bf16[192,512]{1,0:T(8,128)(2,1)S(1)}, u32[]{:S(2)}) copy-start(bf16[192,512]{1,0:T(8,128)(2,1)S(1)} %collective-permute-done.35.refs_5_) | copy-start | bytes 589828
  230.4 12.2 %collective-permute-start.43 = (bf16[192,512]{1,0:T(8,128)(2,1)S(1)}, bf16[192,512]{1,0:T(8,128)(2,1)}, u32[]{:S(2)}, u32[]{:S(2)}) collective-permute-start(bf16[192,512]{1,0:T(8,128)(2,1)S(1)} %get-tuple-element.56), channel_id=1, source_target_pairs={{0,4},{4,0},{8,12},{12,8},{16,20},{20,16},{24,28},{28,24},{1,5},{5... | collective-permute-start | bytes 589832 | tf_op jit(solution)/shard_map/ppermute | solution.py:382
  234.5 0.7 copy-start.7
  234.6 0.7 copy-start.8
  (1 other events, 0.6 us)
